TPU v7x, 32 devices: a whole 2x2x4 slice. The times are simulated.
32 devices in a mesh: ep: 8 (over z, x), tp: 4 (over y, core).
Axes of the slice: x: 2, y: 2, z: 4, core: 2. Of those that a mesh axis runs over, the one named last changes fastest.
Arguments:
- receptance: bfloat16 [4096, 2048], P('ep', 'tp'), may hold values from -6 to 6
- key_rows: bfloat16 [4096, 2048], P('ep', 'tp'), may hold values from -6 to 6
- value_rows: bfloat16 [4096, 2048], P('ep', 'tp'), may hold values from -6 to 6
- decay_input: bfloat16 [4096, 2048], P('ep', 'tp'), may hold values from -2.796875 to 2.796875
- learn_input: bfloat16 [4096, 2048], P('ep', 'tp'), may hold values from -12 to 4
- decay_base: float32 [2048], P('tp'), may hold values from -20 to -2
- decay_shift: float32 [4096, 32], P('ep', 'tp'), may hold values from -1 to 20
- channel_gain: float32 [2048], P('tp'), may hold values from 0.1 to 1.9
- out_weight: bfloat16 [2048, 2048], P('tp'), may hold values from -0.125 to 0.125
- expert_input: bfloat16 [4096, 2048], P(('ep', 'tp')), may hold values from -6 to 6
- expert_gain: float32 [2048], replicated, may hold values from 0.1 to 1.9
- routes: int32 [4096, 2], P(('ep', 'tp')), may hold values from 0 to 7, all different within a row; in each aligned block of 128 rows (0 to 127, 128 to 255, ...) at most 64 rows name the same one
- route_weight: float32 [4096, 2], P(('ep', 'tp')), may hold values from 0.1 to 1
- gate_weight: bfloat16 [8, 2048, 1024], P('ep', None, 'tp'), may hold values from -0.125 to 0.125
- up_weight: bfloat16 [8, 2048, 1024], P('ep', None, 'tp'), may hold values from -0.125 to 0.125
- down_weight: bfloat16 [8, 1024, 2048], P('ep', 'tp'), may hold values from -0.1875 to 0.1875
Outputs:
- mixer_out: bfloat16 [4096, 2048], P(('ep', 'tp'))
- expert_out: bfloat16 [4096, 2048], P(('ep', 'tp'))
Inputs may be any that keep to these rules, and one draw needn't show every extreme that they name: `routes`: within the rows of one device (aligned blocks of 128 rows) no expert is named by more than 64 rows, and in every draw some block names some expert exactly 64 times. Each row names 2 different experts.
All inputs are finite; a program needn't handle non-finite values.
Results may differ from a plain program's by a relative error of at most 0.024.
Values may be sent and summed in bfloat16 or wider, within the bound.
A program may use at most 128 MiB of HBM per device.

v0:
```python
import functools

import jax
import jax.numpy as jnp
from jax import lax
from jax.experimental import pallas as pl
from jax.experimental.pallas import tpu as pltpu
from jax.sharding import PartitionSpec as P

SPAN = 128
STACK = 2
LANES = 128

NORM_EPS = 1e-06
GROUP_EPS = 0.00064
KEY_EPS = 1e-06
F32 = jnp.float32
BF16 = jnp.bfloat16


def mm(a, b):
    return lax.dot_general(
        a.astype(BF16), b.astype(BF16), (((1,), (0,)), ((), ())), preferred_element_type=F32
    )


def mm_nt(a, b):
    return lax.dot_general(
        a.astype(BF16), b.astype(BF16), (((1,), (1,)), ((), ())), preferred_element_type=F32
    )


def mm_tn(a, b):
    return lax.dot_general(
        a.astype(BF16), b.astype(BF16), (((0,), (0,)), ((), ())), preferred_element_type=F32
    )


def split_two(x):
    high = x.astype(BF16)
    return high, (x - high.astype(F32)).astype(BF16)


def grid_index(shape, axis):
    return lax.broadcasted_iota(jnp.int32, shape, axis)


def same_head(head_size):
    rows = grid_index((LANES, LANES), 0) // head_size
    cols = grid_index((LANES, LANES), 1) // head_size
    return rows == cols


def head_sums(x, block):
    high, low = split_two(x)
    return mm(
        jnp.concatenate([high, low], axis=1), jnp.concatenate([block, block], axis=0)
    )


def lower_inverses(strict_parts, rows, cols):
    eye = jnp.where(rows == cols, 1.0, 0.0)
    size = 1
    inverses = None
    while size < SPAN:
        off = (rows // (2 * size) == cols // (2 * size)) & (rows // size != cols // size)
        parts = [jnp.where(off, part, 0.0) for part in strict_parts]
        if inverses is None:
            inverses = [eye - part for part in parts]
        else:
            firsts = [mm(part, inv) for part, inv in zip(parts, inverses)]
            inverses = [inv - mm(inv, first) for inv, first in zip(inverses, firsts)]
        size *= 2
    return inverses


def local_kernel(
    head_size,
    r_ref,
    k_ref,
    v_ref,
    d_ref,
    l_ref,
    base_ref,
    shift_ref,
    reader_ref,
    local_ref,
    summary_ref,
    state,
):
    pair = pl.program_id(0)
    half = LANES // 2

    rows = grid_index((SPAN, SPAN), 0)
    cols = grid_index((SPAN, SPAN), 1)
    strict = rows > cols
    inclusive = rows >= cols
    first = grid_index((SPAN, LANES), 1) < half
    matched = same_head(head_size)
    block = matched.astype(BF16)
    diagonal = grid_index((LANES, LANES), 0) == grid_index((LANES, LANES), 1)
    tri = inclusive.astype(BF16)
    tri_two = jnp.concatenate([tri, tri], axis=1)

    state[:LANES] = jnp.zeros((LANES, LANES), F32)
    state[LANES:] = jnp.where(diagonal, 1.0, 0.0)

    heads = shift_ref.shape[1]
    chosen = grid_index((heads, LANES), 0) == 2 * pair + grid_index((heads, LANES), 1) // half
    def advance(step, nothing):
        start = pl.multiple_of(step * (STACK * SPAN), STACK * SPAN)
        rows_here = pl.ds(start, STACK * SPAN)
        shift = lax.dot_general(
            shift_ref[rows_here],
            chosen.astype(F32),
            (((1,), (0,)), ((), ())),
            precision=lax.Precision.HIGHEST,
            preferred_element_type=F32,
        )
        pre = d_ref[rows_here].astype(F32) + base_ref[0] + shift
        log_all = -0.6065306597126334 / (1.0 + jnp.exp(-pre))
        rates = 1.0 / (1.0 + jnp.exp(-l_ref[rows_here].astype(F32)))
        key_all = k_ref[rows_here].astype(F32)
        unit_all = key_all * lax.rsqrt(head_sums(key_all * key_all, block) + KEY_EPS)
        removal_all = unit_all * rates

        spans = STACK
        items = []
        strict_parts = []
        for j in range(spans):
            here = slice(j * SPAN, (j + 1) * SPAN)
            log_decay = log_all[here]
            high, low = split_two(log_decay)
            cum = mm(tri_two, jnp.concatenate([high, low], axis=0))
            middle = cum[SPAN // 2 - 1 : SPAN // 2]
            ending = cum[SPAN - 1 :]
            e_cm = jnp.exp(cum - middle)
            e_pm = jnp.exp(cum - log_decay - middle)
            shrink = jnp.exp(middle - cum)
            e_mid = jnp.exp(middle)
            e_tail = jnp.exp(ending - middle)
            unit, key = unit_all[here], key_all[here]
            value = v_ref[pl.ds(start + j * SPAN, SPAN)]
            turned = jnp.concatenate([value[:, half:], value[:, :half]], axis=1)
            recept = r_ref[pl.ds(start + j * SPAN, SPAN)].astype(F32)
            probes = unit * e_pm
            queries = recept * e_cm
            back_removal = removal_all[here] * shrink
            back_keys = key * shrink
            left = jnp.concatenate(
                [
                    jnp.where(first, probes, 0.0),
                    jnp.where(first, 0.0, probes),
                    jnp.where(first, queries, 0.0),
                    jnp.where(first, 0.0, queries),
                ],
                axis=0,
            )
            products = mm_nt(left, jnp.concatenate([back_removal, back_keys], axis=0))
            for h in range(2):
                strict_parts.append(
                    jnp.where(strict, products[h * SPAN : (h + 1) * SPAN, :SPAN], 0.0)
                )
            items.append(
                dict(
                    products=products,
                    turned=turned,
                    carrying=probes * e_mid,
                    reading=queries * e_mid,
                    removal_tail=back_removal * e_tail,
                    key_tail=back_keys * e_tail,
                    fade=jnp.exp(ending),
                )
            )
        inverses = lower_inverses(strict_parts, rows, cols)
        for j in range(spans):
            item = items[j]
            products, turned = item["products"], item["turned"]
            solved, removed, kept = [], [], []
            for h in range(2):
                top = slice(h * SPAN, (h + 1) * SPAN)
                bottom = slice((2 + h) * SPAN, (3 + h) * SPAN)
                pair_keys = jnp.where(strict, products[top, SPAN:], 0.0)
                read_removal = jnp.where(inclusive, products[bottom, :SPAN], 0.0)
                read_keys = jnp.where(inclusive, products[bottom, SPAN:], 0.0)
                both = mm(jnp.concatenate([pair_keys, read_keys], axis=0), turned)
                own = first if h == 0 else jnp.logical_not(first)
                right = jnp.where(own, item["carrying"], both[:SPAN])
                answer = mm(inverses[2 * j + h], right)
                solved.append(answer)
                removed.append(mm(read_removal, answer))
                kept.append(both[SPAN:])
            carried = jnp.where(first, solved[0], solved[1])
            local_turned = jnp.where(first, solved[1], solved[0])
            reader = item["reading"] - jnp.where(first, removed[0], removed[1])
            read_turned = jnp.where(first, kept[1] - removed[1], kept[0] - removed[0])
            local_read = jnp.concatenate([read_turned[:, half:], read_turned[:, :half]], axis=1)
            taken = mm_tn(
                jnp.concatenate([carried, local_turned], axis=1), item["removal_tail"]
            )
            offset_turned = mm_tn(turned, item["key_tail"]) - taken[LANES:]
            offset = jnp.concatenate([offset_turned[half:], offset_turned[:half]], axis=0)
            offset = jnp.where(matched, offset, 0.0)
            transition = jnp.where(diagonal, item["fade"], 0.0) - jnp.where(
                matched, taken[:LANES], 0.0
            )
            now = state[...]
            reads = mm_nt(reader, now)
            here = pl.ds(start + j * SPAN, SPAN)
            local_ref[here] = local_read + reads[:, :LANES]
            reader_ref[pl.ds(start + j * SPAN, SPAN)] = reads[:, LANES:].astype(BF16)
            now_high, now_low = split_two(now)
            step_high, step_low = split_two(transition)
            moved = mm(now_high, step_high) + mm(now_low, step_high) + mm(now_high, step_low)
            state[:LANES] = moved[:LANES] + offset
            state[LANES:] = moved[LANES:]
        return nothing

    lax.fori_loop(0, r_ref.shape[0] // (STACK * SPAN), advance, 0)
    summary_ref[1] = (state[:half] + state[half:LANES]).astype(BF16)
    summary_ref[0] = (state[LANES : LANES + half] + state[LANES + half :]).astype(BF16)


def mixer_local(receptance, keys, values, decay, learn, base, shift, head_size):
    rows, channels = receptance.shape
    pairs = channels // LANES
    heads = shift.shape[1]
    half = LANES // 2
    tile = pl.BlockSpec((rows, LANES), lambda p: (0, p))
    small = pl.BlockSpec((2, half, LANES), lambda p: (0, p, 0))
    return pl.pallas_call(
        functools.partial(local_kernel, head_size),
        grid=(pairs,),
        in_specs=[tile] * 5
        + [
            pl.BlockSpec((1, 1, LANES), lambda p: (p, 0, 0)),
            pl.BlockSpec((rows, heads), lambda p: (0, 0)),
        ],
        out_specs=[tile, tile, small],
        out_shape=[
            jax.ShapeDtypeStruct((rows, channels), BF16),
            jax.ShapeDtypeStruct((rows, channels), F32),
            jax.ShapeDtypeStruct((2, pairs * half, LANES), BF16),
        ],
        scratch_shapes=[pltpu.VMEM((2 * LANES, LANES), F32)],
        compiler_params=pltpu.CompilerParams(
            dimension_semantics=("arbitrary",), vmem_limit_bytes=24 * 2**20
        ),
        cost_estimate=pl.CostEstimate(
            flops=20 * 10**9, bytes_accessed=6 * 2**20, transcendentals=10**6
        ),
        name="mixer_local",
    )(receptance, keys, values, decay, learn, base.reshape(pairs, 1, LANES), shift)


def finish_kernel(
    head_size,
    summary_ref,
    reader_ref,
    local_ref,
    gain_ref,
    out_ref,
    landed,
    send_sems,
    recv_sems,
):
    here = lax.axis_index("ep")
    count = lax.axis_size("ep")
    half = LANES // 2
    rows, channels = reader_ref.shape
    pairs = channels // LANES
    matched = same_head(head_size)
    block = matched.astype(BF16)

    def transfer(distance, target):
        return pltpu.make_async_remote_copy(
            src_ref=summary_ref,
            dst_ref=landed.at[distance - 1],
            send_sem=send_sems.at[distance - 1],
            recv_sem=recv_sems.at[distance - 1],
            device_id={"ep": target},
            device_id_type=pl.DeviceIdType.MESH,
        )

    barrier = pltpu.get_barrier_semaphore()

    def greet(distance, nothing):
        pl.semaphore_signal(
            barrier,
            inc=1,
            device_id={"ep": lax.rem(here + distance, count)},
            device_id_type=pl.DeviceIdType.MESH,
        )
        return nothing

    lax.fori_loop(1, count, greet, 0)
    pl.semaphore_wait(barrier, count - 1)

    def launch(distance, nothing):
        transfer(distance, here + distance).start()
        return nothing

    lax.fori_loop(1, count - here, launch, 0)

    def wide(place, kind, p):
        part = landed[place, kind, p * half : (p + 1) * half].astype(F32)
        return jnp.where(matched, jnp.concatenate([part, part], axis=0), 0.0)

    def turn(k, states):
        distance = here - k
        transfer(distance, k).wait_recv()
        after = []
        for p in range(pairs):
            high, low = split_two(states[p])
            moved = mm(jnp.concatenate([high, low], axis=0), wide(distance - 1, 0, p))
            after.append(moved[:LANES] + moved[LANES:] + wide(distance - 1, 1, p))
        return tuple(after)

    nothing = tuple(jnp.zeros((LANES, LANES), F32) for _ in range(pairs))
    entering = lax.fori_loop(0, here, turn, nothing)
    for p in range(pairs):
        lanes = slice(p * LANES, (p + 1) * LANES)
        read = mm_nt(reader_ref[:, lanes], entering[p]) + local_ref[:, lanes]
        centred = read - head_sums(read, block) * (1.0 / head_size)
        variance = head_sums(centred * centred, block) * (1.0 / head_size)
        scaled = centred * lax.rsqrt(variance + GROUP_EPS) * gain_ref[:, lanes]
        out_ref[:, lanes] = scaled.astype(BF16)

    def settle(distance, nothing):
        transfer(distance, here + distance).wait_send()
        return nothing

    lax.fori_loop(1, count - here, settle, 0)


def mixer_finish(summary, reader, local_read, gain, head_size):
    rows, channels = reader.shape
    count = lax.axis_size("ep")
    return pl.pallas_call(
        functools.partial(finish_kernel, head_size),
        in_specs=[pl.BlockSpec(memory_space=pltpu.VMEM)] * 4,
        out_specs=pl.BlockSpec(memory_space=pltpu.VMEM),
        out_shape=jax.ShapeDtypeStruct((rows, channels), BF16),
        scratch_shapes=[
            pltpu.VMEM((count - 1,) + summary.shape, BF16),
            pltpu.SemaphoreType.DMA((count - 1,)),
            pltpu.SemaphoreType.DMA((count - 1,)),
        ],
        compiler_params=pltpu.CompilerParams(
            vmem_limit_bytes=32 * 2**20, collective_id=0, has_side_effects=True
        ),
        cost_estimate=pl.CostEstimate(
            flops=10 * 10**9, bytes_accessed=4 * 2**20, transcendentals=10**5
        ),
        name="mixer_finish",
    )(summary, reader, local_read, gain.reshape(1, channels))


def hidden_kernel(x_ref, gate_ref, up_ref, out_ref):
    gates = mm(x_ref[...], gate_ref[0])
    uppers = mm(x_ref[...], up_ref[0])
    out_ref[...] = (gates / (1.0 + jnp.exp(-gates)) * uppers).astype(BF16)


def expert_hidden(incoming, all_gate, all_up):
    rows, width = incoming.shape
    shards, _, units = all_gate.shape
    weight = pl.BlockSpec((1, width, units), lambda t: (t, 0, 0))
    return pl.pallas_call(
        hidden_kernel,
        grid=(shards,),
        in_specs=[pl.BlockSpec((rows, width), lambda t: (0, 0)), weight, weight],
        out_specs=pl.BlockSpec((rows, units), lambda t: (0, t)),
        out_shape=jax.ShapeDtypeStruct((rows, shards * units), BF16),
        compiler_params=pltpu.CompilerParams(
            dimension_semantics=("arbitrary",), vmem_limit_bytes=32 * 2**20
        ),
        cost_estimate=pl.CostEstimate(
            flops=4 * rows * width * units * shards,
            bytes_accessed=2 * (rows * width + 2 * shards * units * width),
            transcendentals=rows * units * shards,
        ),
        name="expert_hidden",
    )(incoming, all_gate, all_up)


def slot_targets(block_routes, experts, capacity):
    flat_routes = block_routes.reshape(-1)
    count = flat_routes.shape[0]
    order = jnp.arange(count, dtype=jnp.int32)
    before = (order[:, None] > order[None, :]) & (flat_routes[:, None] == flat_routes[None, :])
    slots = jnp.sum(before.astype(jnp.int32), axis=1).reshape(block_routes.shape)
    return block_routes * capacity + slots


def dispersal_table(targets, places):
    marks = (jnp.arange(places, dtype=jnp.int32)[:, None, None] == targets[None, :, :]).astype(
        jnp.int32
    )
    return jnp.sum(marks, axis=2).astype(jnp.bfloat16)


def on_device(
    receptance,
    key_rows,
    value_rows,
    decay_input,
    learn_input,
    decay_base,
    decay_shift,
    channel_gain,
    out_weight,
    expert_input,
    expert_gain,
    routes,
    route_weight,
    gate_weight,
    up_weight,
    down_weight,
):
    ep_count = lax.axis_size("ep")
    channels = receptance.shape[1]
    head_size = channels // decay_shift.shape[1]
    token_rows, model_width = expert_input.shape
    top_count = routes.shape[1]
    experts = gate_weight.shape[0] * ep_count
    capacity = max(2, 2 * token_rows * top_count // experts)
    slab_rows = ep_count * capacity

    all_gate = lax.all_gather(gate_weight[0], "tp")
    all_up = lax.all_gather(up_weight[0], "tp")
    all_down = lax.all_gather(down_weight[0], "tp")

    inputs = expert_input.astype(F32)
    expert_normed = (
        inputs
        * lax.rsqrt(jnp.mean(inputs * inputs, axis=1, keepdims=True) + NORM_EPS)
        * expert_gain
    ).astype(BF16)
    own_targets = slot_targets(routes, experts, capacity)
    outgoing = jnp.dot(
        dispersal_table(own_targets, experts * capacity),
        expert_normed,
        preferred_element_type=F32,
    ).astype(BF16)
    arrived = lax.all_to_all(
        outgoing.reshape(experts, capacity, model_width),
        "ep",
        split_axis=0,
        concat_axis=0,
        tiled=True,
    ).reshape(slab_rows, model_width)

    reader, local_read, summary = mixer_local(
        receptance,
        key_rows,
        value_rows,
        decay_input,
        learn_input,
        decay_base,
        decay_shift,
        head_size,
    )
    mixed = mixer_finish(summary, reader, local_read, channel_gain, head_size)
    mixer_term = jnp.dot(mixed, out_weight, preferred_element_type=F32)
    mixer_out = lax.psum_scatter(
        mixer_term.astype(BF16), "tp", scatter_dimension=0, tiled=True
    )

    hidden = expert_hidden(arrived, all_gate, all_up)
    total = jnp.dot(
        hidden, all_down.reshape(hidden.shape[1], model_width), preferred_element_type=F32
    )
    returned = lax.all_to_all(
        total.astype(BF16).reshape(ep_count, capacity, model_width),
        "ep",
        split_axis=0,
        concat_axis=0,
        tiled=True,
    )
    flat_rows = returned.reshape(experts * capacity, model_width)
    places = jnp.arange(experts * capacity, dtype=jnp.int32)
    combined = jnp.zeros((token_rows, model_width), F32)
    for picked in range(top_count):
        table = (own_targets[:, picked : picked + 1] == places[None, :]).astype(BF16)
        chosen = jnp.dot(table, flat_rows, preferred_element_type=F32)
        combined = combined + chosen * route_weight[:, picked : picked + 1]
    return (mixer_out, combined.astype(BF16))


def solution(mesh):
    return jax.shard_map(
        on_device,
        mesh=mesh,
        in_specs=(
            P("ep", "tp"),
            P("ep", "tp"),
            P("ep", "tp"),
            P("ep", "tp"),
            P("ep", "tp"),
            P("tp"),
            P("ep", "tp"),
            P("tp"),
            P("tp", None),
            P(("ep", "tp"), None),
            P(),
            P(("ep", "tp"), None),
            P(("ep", "tp"), None),
            P("ep", None, "tp"),
            P("ep", None, "tp"),
            P("ep", "tp", None),
        ),
        out_specs=(P(("ep", "tp"), None), P(("ep", "tp"), None)),
        check_vma=False,
    )
```

profile of v0, /device:TPU:0, one launch (start us, length us, event | category | flops | bytes accessed | tf_op | source)
XLA Modules:
  0.0 190.9 jit_solution(5834312436922276781)
XLA Ops:
  7.2 0.0 copy-start
  7.2 0.0 copy-start.14
  7.2 0.0 copy-start.11
  7.2 0.0 copy-start.13
  7.2 0.0 all-gather.4.cloned.1.call-start
  7.3 0.7 all-gather.4.cloned.1.call-update
  7.9 0.0 all-gather.6.cloned.1.call-start
  8.0 0.7 all-gather.6.cloned.1.call-update
  8.7 0.0 all-gather.8.cloned.1.call-start
  8.7 0.7 all-gather.8.cloned.1.call-update
  9.4 0.0 copy-done.14
  9.4 0.1 copy.38
  9.6 0.1 eq.58
  9.7 0.2 convert_reduce_fusion.1
  9.9 0.1 reshape.42
  10.0 0.1 copy.39
  10.1 0.1 convert_reduce_fusion
  10.2 0.0 copy-done.11
  10.2 0.2 fusion.2
  10.4 0.0 copy-done.13
  10.4 2.1 %convolution_convert_fusion.1 = bf16[512,2048]{1,0:T(8,128)(2,1)} fusion(bf16[128,2048]{1,0:T(8,128)(2,1)S(1)} %copy-done.11, f32[2048]{0:T(1024)S(1)} %copy-done.13, f32[128]{0:T(128)S(1)} %add_rsqrt_fusion, s32[512,128]{1,0:T(8,128)S(1)} %convert_reduce_fusion), kind=kOutput, calls=%fused_computation.1 | convolution fusion | flops 270598144 | bytes 2892288 | tf_op jit(solution)/shard_map/dot_general | solution.py:441
  12.5 0.0 copy-start.12
  12.5 0.0 copy-start.3
  12.5 0.0 copy-start.4
  12.5 0.0 copy-start.8
  12.5 7.4 %all-to-all-start = ((bf16[8,64,2048]{2,1,0:T(8,128)(2,1)}), bf16[8,64,2048]{2,1,0:T(8,128)(2,1)}, u32[]{:S(2)}, u32[]{:S(2)}) async-start(bf16[8,64,2048]{2,1,0:T(8,128)(2,1)} %bitcast.23), calls=%async_computation.1 | async-start | bytes 4194304 | tf_op jit(solution)/shard_map/all_to_all | solution.py:446
  20.0 0.0 copy-done.12
  20.0 0.1 copy.37.shift_ref
  20.1 0.0 copy-done.3
  20.1 0.0 copy-done.4
  20.1 0.0 copy-done.8
  20.1 0.0 copy-start.5
  20.1 1.0 copy-done.5
  21.2 0.0 copy-start.6
  21.2 1.1 copy-done.6
  22.3 0.0 copy-start.7
  22.3 1.0 copy-done.7
  23.3 0.0 copy-start.9
  23.3 30.2 %mixer_local.1 = (bf16[512,512]{1,0:T(8,128)(2,1)S(1)}, f32[512,512]{1,0:T(8,128)S(1)}, bf16[2,256,128]{2,1,0:T(8,128)(2,1)S(1)}) custom-call(bf16[512,512]{1,0:T(8,128)(2,1)S(1)} %copy-done.3, bf16[512,512]{1,0:T(8,128)(2,1)S(1)} %copy-done.4, bf16[512,512]{1,0:T(8,128)(2,1)S(1)} %copy-done.5, bf16[512,512]{1,0:T(8,128)(2,1)S(1)} %copy-done.6, ...), custom_call_target="tpu_custom_call" | custom-call | flops 20000000000 | bytes 6291456 | tf_op jit(solution)/shard_map/mixer_local/pallas_call | solution.py:231
  53.5 0.0 copy-done.9
  53.5 21.4 %mixer_finish.1 = bf16[512,512]{1,0:T(8,128)(2,1)S(1)} custom-call(bf16[2,256,128]{2,1,0:T(8,128)(2,1)S(1)} %get-tuple-element.5.summary_ref, bf16[512,512]{1,0:T(8,128)(2,1)S(1)} %get-tuple-element.6.reader_ref, f32[512,512]{1,0:T(8,128)S(1)} %get-tuple-element.7.local_ref, f32[1,512]{1,0:T(1,128)S(1)} %bitcast.22), custom_call_target="tpu_custom_call" | custom-call | flops 10000000000 | bytes 4194304 | tf_op jit(solution)/shard_map/mixer_finish/pallas_call | solution.py:339
  74.9 0.0 all-to-all-done
  74.9 0.0 all-gather.4.cloned.1.call-done.gate_ref
  74.9 7.9 %all-gather.6.cloned.1.call-done.up_ref = bf16[4,2048,256]{2,1,0:T(8,128)(2,1)} async-done(((bf16[1,2048,256]{2,1,0:T(8,128)(2,1)}), bf16[4,2048,256]{2,1,0:T(8,128)(2,1)}) %all-gather.6.cloned.1.call-update) | async-done | bytes 4194320 | tf_op jit(solution)/shard_map/all_gather | solution.py:431
  82.9 0.0 copy-start.1
  82.9 2.2 %copy-done.1 = bf16[4,2048,256]{2,1,0:T(8,128)(2,1)S(1)} copy-done((bf16[4,2048,256]{2,1,0:T(8,128)(2,1)S(1)}, bf16[4,2048,256]{2,1,0:T(8,128)(2,1)}, u32[]{:S(2)}) %copy-start.1) | copy-done | bytes 4194328
  85.1 0.0 copy-start.2
  85.1 2.2 %copy-done.2 = bf16[4,2048,256]{2,1,0:T(8,128)(2,1)S(1)} copy-done((bf16[4,2048,256]{2,1,0:T(8,128)(2,1)S(1)}, bf16[4,2048,256]{2,1,0:T(8,128)(2,1)}, u32[]{:S(2)}) %copy-start.2) | copy-done | bytes 4194328
  87.3 6.8 %expert_hidden.1 = bf16[512,1024]{1,0:T(8,128)(2,1)S(1)} custom-call(bf16[512,2048]{1,0:T(8,128)(2,1)} %bitcast.4.x_ref, bf16[4,2048,256]{2,1,0:T(8,128)(2,1)S(1)} %copy-done.1, bf16[4,2048,256]{2,1,0:T(8,128)(2,1)S(1)} %copy-done.2), custom_call_target="tpu_custom_call" | custom-call | flops 4294967296 | bytes 10485760 | tf_op jit(solution)/shard_map/expert_hidden/pallas_call | solution.py:369
  94.0 0.0 copy-start.10
  94.1 1.0 copy-done.10
  95.0 24.0 %all-gather.8.cloned.1.call-done = bf16[4,256,2048]{2,1,0:T(8,128)(2,1)} async-done(((bf16[1,256,2048]{2,1,0:T(8,128)(2,1)}), bf16[4,256,2048]{2,1,0:T(8,128)(2,1)}) %all-gather.8.cloned.1.call-update) | async-done | bytes 4194320 | tf_op jit(solution)/shard_map/all_gather | solution.py:432
  119.0 6.2 %convolution_convert_fusion = bf16[512,2048]{1,0:T(8,128)(2,1)} fusion(bf16[512,1024]{1,0:T(8,128)(2,1)} %copy-done.10, bf16[1024,2048]{1,0:T(8,128)(2,1)} %bitcast.25), kind=kOutput, calls=%fused_computation | convolution fusion | flops 2148532224 | bytes 7340032 | tf_op jit(solution)/shard_map/dot_general | solution.py:471
  125.2 5.5 %all-to-all-start.1 = ((bf16[8,64,2048]{2,1,0:T(8,128)(2,1)}), bf16[8,64,2048]{2,1,0:T(8,128)(2,1)}, u32[]{:S(2)}, u32[]{:S(2)}) async-start(bf16[8,64,2048]{2,1,0:T(8,128)(2,1)} %bitcast.24), calls=%async_computation.2 | async-start | bytes 4194304 | tf_op jit(solution)/shard_map/all_to_all | solution.py:474
  130.7 0.0 reduce-scatter.2.cloned.1.call-start
  130.8 0.0 copy-done
  130.8 2.6 %convolution_convert_fusion.2 = bf16[512,2048]{1,0:T(8,128)(2,1)} fusion(bf16[512,512]{1,0:T(8,128)(2,1)S(1)} %mixer_finish.1, bf16[512,2048]{1,0:T(8,128)(2,1)S(1)} %copy-done), kind=kOutput, calls=%fused_computation.2 | convolution fusion | flops 1074790400 | bytes 4718592 | tf_op jit(solution)/shard_map/dot_general | solution.py:465
  133.3 0.0 copy-start.15
  133.3 0.0 reduce-scatter.2.cloned.1.call-update
  133.4 0.6 copy-done.15
  134.0 45.5 %all-to-all-done.1 = bf16[8,64,2048]{2,1,0:T(8,128)(2,1)} async-done(((bf16[8,64,2048]{2,1,0:T(8,128)(2,1)}), bf16[8,64,2048]{2,1,0:T(8,128)(2,1)}, u32[]{:S(2)}, u32[]{:S(2)}) %all-to-all-start.1) | async-done | bytes 2097184 | tf_op jit(solution)/shard_map/all_to_all | solution.py:474
  179.5 2.1 %convolution_multiply_fusion.1 = f32[128,2048]{1,0:T(8,128)S(1)} fusion(bf16[512,2048]{1,0:T(8,128)(2,1)} %bitcast.7, f32[128]{0:T(128)S(1)} %get-tuple-element.11, s32[128]{0:T(128)S(1)} %get-tuple-element.9), kind=kOutput, calls=%fused_computation.5 | convolution fusion | flops 268763136 | bytes 3146752 | tf_op jit(solution)/shard_map/dot_general | solution.py:486
  181.5 2.9 %fusion.1 = bf16[128,2048]{1,0:T(8,128)(2,1)} fusion(f32[128,2048]{1,0:T(8,128)S(1)} %convolution_multiply_fusion.1, bf16[512,2048]{1,0:T(8,128)(2,1)} %bitcast.7, f32[128]{0:T(128)S(1)} %get-tuple-element.10, s32[128]{0:T(128)S(1)} %get-tuple-element.8), kind=kOutput, calls=%fused_computation.6 | convolution fusion | flops 269287424 | bytes 3671040 | tf_op jit(solution)/shard_map/dot_general | solution.py:486
  184.4 0.0 reduce-scatter.2.cloned.1.call-done
  (4 shorter events, 0.0 us)
Async XLA Ops:
  7.2 123.6 %copy-start = (bf16[512,2048]{1,0:T(8,128)(2,1)S(1)}, bf16[512,2048]{1,0:T(8,128)(2,1)}, u32[]{:S(2)}) copy-start(bf16[512,2048]{1,0:T(8,128)(2,1)} %param.24) | copy-start | bytes 6291460
  7.2 2.3 %copy-start.14 = (s32[128,2]{0,1:T(2,128)S(1)}, s32[128,2]{0,1:T(2,128)}, u32[]{:S(2)}) copy-start(s32[128,2]{0,1:T(2,128)} %param.27) | copy-start | bytes 3076
  7.2 3.0 %copy-start.11 = (bf16[128,2048]{1,0:T(8,128)(2,1)S(1)}, bf16[128,2048]{1,0:T(8,128)(2,1)}, u32[]{:S(2)}) copy-start(bf16[128,2048]{1,0:T(8,128)(2,1)} %param.25) | copy-start | bytes 1572868
  7.2 3.2 %copy-start.13 = (f32[2048]{0:T(1024)S(1)}, f32[2048]{0:T(1024)}, u32[]{:S(2)}) copy-start(f32[2048]{0:T(1024)} %param.26) | copy-start | bytes 24580
  7.2 67.7 %all-gather.4.cloned.1.call-start = ((), (), s32[]{:S(2)}) async-start(), calls=%async_computation.4 | async-start | bytes 5242880 | tf_op jit(solution)/shard_map/all_gather | solution.py:430
  7.9 74.9 %all-gather.6.cloned.1.call-start = ((), (), s32[]{:S(2)}) async-start(), calls=%async_computation.5 | async-start | bytes 5242880 | tf_op jit(solution)/shard_map/all_gather | solution.py:431
  8.7 110.3 %all-gather.8.cloned.1.call-start = ((), (), s32[]{:S(2)}) async-start(), calls=%async_computation.6 | async-start | bytes 5242880 | tf_op jit(solution)/shard_map/all_gather | solution.py:432
  12.5 7.4 %copy-start.12 = (f32[512,8]{0,1:T(8,128)S(1)}, f32[512,8]{0,1:T(8,128)}, u32[]{:S(2)}) copy-start(f32[512,8]{0,1:T(8,128)} %param.22) | copy-start | bytes 49156
  12.5 7.6 %copy-start.3 = (bf16[512,512]{1,0:T(8,128)(2,1)S(1)}, bf16[512,512]{1,0:T(8,128)(2,1)}, u32[]{:S(2)}) copy-start(bf16[512,512]{1,0:T(8,128)(2,1)} %r_ref.1) | copy-start | bytes 1572868
  12.5 7.6 %copy-start.4 = (bf16[512,512]{1,0:T(8,128)(2,1)S(1)}, bf16[512,512]{1,0:T(8,128)(2,1)}, u32[]{:S(2)}) copy-start(bf16[512,512]{1,0:T(8,128)(2,1)} %k_ref.1) | copy-start | bytes 1572868
  12.5 7.6 %copy-start.8 = (f32[512]{0:T(512)S(1)}, f32[512]{0:T(512)}, u32[]{:S(2)}) copy-start(f32[512]{0:T(512)} %param.21) | copy-start | bytes 6148
  12.5 62.4 %all-to-all-start = ((bf16[8,64,2048]{2,1,0:T(8,128)(2,1)}), bf16[8,64,2048]{2,1,0:T(8,128)(2,1)}, u32[]{:S(2)}, u32[]{:S(2)}) async-start(bf16[8,64,2048]{2,1,0:T(8,128)(2,1)} %bitcast.23), calls=%async_computation.1 | async-start | bytes 4194304 | tf_op jit(solution)/shard_map/all_to_all | solution.py:446
  20.1 1.1 copy-start.5
  21.2 1.1 copy-start.6
  22.3 1.0 copy-start.7
  23.3 30.2 %copy-start.9 = (f32[512]{0:T(512)S(1)}, f32[512]{0:T(512)}, u32[]{:S(2)}) copy-start(f32[512]{0:T(512)} %param.23) | copy-start | bytes 6148
  82.9 2.2 %copy-start.1 = (bf16[4,2048,256]{2,1,0:T(8,128)(2,1)S(1)}, bf16[4,2048,256]{2,1,0:T(8,128)(2,1)}, u32[]{:S(2)}) copy-start(bf16[4,2048,256]{2,1,0:T(8,128)(2,1)} %all-gather.4.cloned.1.call-done.gate_ref) | copy-start | bytes 12582916
  85.1 2.2 %copy-start.2 = (bf16[4,2048,256]{2,1,0:T(8,128)(2,1)S(1)}, bf16[4,2048,256]{2,1,0:T(8,128)(2,1)}, u32[]{:S(2)}) copy-start(bf16[4,2048,256]{2,1,0:T(8,128)(2,1)} %all-gather.6.cloned.1.call-done.up_ref) | copy-start | bytes 12582916
  94.0 1.0 copy-start.10
  125.2 54.3 %all-to-all-start.1 = ((bf16[8,64,2048]{2,1,0:T(8,128)(2,1)}), bf16[8,64,2048]{2,1,0:T(8,128)(2,1)}, u32[]{:S(2)}, u32[]{:S(2)}) async-start(bf16[8,64,2048]{2,1,0:T(8,128)(2,1)} %bitcast.24), calls=%async_computation.2 | async-start | bytes 4194304 | tf_op jit(solution)/shard_map/all_to_all | solution.py:474
  130.7 53.7 %reduce-scatter.2.cloned.1.call-start = ((), (), s32[]{:S(2)}) async-start(), calls=%async_computation.3 | async-start | bytes 2621440 | tf_op jit(solution)/shard_map/reduce_scatter | solution.py:466
  133.3 0.7 copy-start.15
Sparse Core Ops, SparseCore 0:
  9.6 37.2 all-gather.3
  48.4 34.4 all-gather.5
  84.5 34.5 all-gather.7
  134.3 31.6 reduce-scatter.1
where the time goes:
time: 192 us; the launch traced here: 191 us
  waiting for transfers between devices  79.5 us (41%)
  Pallas kernels  58.3 us (30%)
  matrix products  15.8 us (8%)
  between operations  14 us (7%)
  starting transfers between devices  13.1 us (7%)
  local copies, waits for them, and re-layouts  9.78 us (5%)
    all_to_all x1, waiting for transfers between devices, on_device(): lax.all_to_all(total.astype(BF16).reshape(ep_count, capacity, model_width...  45.5 us
    pallas_call x1, Pallas kernels, mixer_local(): pl.pallas_call(functools.partial(local_kernel, head_size), grid=(pairs,),...  30.2 us
    all_gather x1, waiting for transfers between devices, on_device(): all_down = lax.all_gather(down_weight[0], 'tp')  24 us
    pallas_call x1, Pallas kernels, mixer_finish(): pl.pallas_call(functools.partial(finish_kernel, head_size), in_specs=[pl....  21.4 us
    unnamed x34, local copies, waits for them, and re-layouts  9.44 us
    all_gather x1, waiting for transfers between devices, on_device(): all_up = lax.all_gather(up_weight[0], 'tp')  7.94 us
    all_to_all x1, starting transfers between devices, on_device(): lax.all_to_all(outgoing.reshape(experts, capacity, model_width), 'ep', sp...  7.43 us
    pallas_call x1, Pallas kernels, expert_hidden(): pl.pallas_call(hidden_kernel, grid=(shards,), in_specs=[pl.BlockSpec((row...  6.78 us
  transfers between devices with their start and end apart: 6, of which 3 were waited for; matrix products, arithmetic and copies ran while one was open for 6% of the time, Pallas kernels for 31%

commit v1 on v0

--- a/solution.py
+++ b/solution.py
@@ -6,6 +6,7 @@
 from jax.experimental import pallas as pl
 from jax.experimental.pallas import tpu as pltpu
 from jax.sharding import PartitionSpec as P
+
 
 SPAN = 128
 STACK = 2
@@ -107,6 +108,7 @@
 
     heads = shift_ref.shape[1]
     chosen = grid_index((heads, LANES), 0) == 2 * pair + grid_index((heads, LANES), 1) // half
+
     def advance(step, nothing):
         start = pl.multiple_of(step * (STACK * SPAN), STACK * SPAN)
         rows_here = pl.ds(start, STACK * SPAN)
@@ -267,7 +269,7 @@
     here = lax.axis_index("ep")
     count = lax.axis_size("ep")
     half = LANES // 2
-    rows, channels = reader_ref.shape
+    _, channels = reader_ref.shape
     pairs = channels // LANES
     matched = same_head(head_size)
     block = matched.astype(BF16)
@@ -356,35 +358,75 @@
     )(summary, reader, local_read, gain.reshape(1, channels))
 
 
-def hidden_kernel(x_ref, gate_ref, up_ref, out_ref):
-    gates = mm(x_ref[...], gate_ref[0])
-    uppers = mm(x_ref[...], up_ref[0])
-    out_ref[...] = (gates / (1.0 + jnp.exp(-gates)) * uppers).astype(BF16)
-
-
-def expert_hidden(incoming, all_gate, all_up):
+def part_kernel(shards, started, *refs):
+    x_ref = refs[0]
+    weights = refs[1 : 1 + 3 * shards]
+    total_ref = refs[1 + 3 * shards] if started else None
+    out_ref = refs[-1]
+    rows = x_ref.shape[0]
+    piece = min(rows, 256)
+
+    def block(step, nothing):
+        here = pl.ds(pl.multiple_of(step * piece, piece), piece)
+        x = x_ref[here]
+        total = total_ref[here] if started else None
+        for s in range(shards):
+            gate, up, down = weights[3 * s : 3 * s + 3]
+            gates = mm(x, gate[...])
+            uppers = mm(x, up[...])
+            hidden = (gates / (1.0 + jnp.exp(-gates)) * uppers).astype(BF16)
+            term = mm(hidden, down[...])
+            total = term if total is None else total + term
+        out_ref[here] = total.astype(out_ref.dtype)
+        return nothing
+
+    lax.fori_loop(0, rows // piece, block, 0)
+
+
+def expert_part(incoming, weights, total, out_type):
     rows, width = incoming.shape
-    shards, _, units = all_gate.shape
-    weight = pl.BlockSpec((1, width, units), lambda t: (t, 0, 0))
+    shards = len(weights)
+    units = weights[0][0].shape[1]
+    started = total is not None
+    flat = [array for shard in weights for array in shard]
+    operands = [incoming] + flat + ([total] if started else [])
     return pl.pallas_call(
-        hidden_kernel,
-        grid=(shards,),
-        in_specs=[pl.BlockSpec((rows, width), lambda t: (0, 0)), weight, weight],
-        out_specs=pl.BlockSpec((rows, units), lambda t: (0, t)),
-        out_shape=jax.ShapeDtypeStruct((rows, shards * units), BF16),
-        compiler_params=pltpu.CompilerParams(
-            dimension_semantics=("arbitrary",), vmem_limit_bytes=32 * 2**20
-        ),
+        functools.partial(part_kernel, shards, started),
+        in_specs=[pl.BlockSpec(memory_space=pltpu.VMEM)] * len(operands),
+        out_specs=pl.BlockSpec(memory_space=pltpu.VMEM),
+        out_shape=jax.ShapeDtypeStruct((rows, width), out_type),
+        compiler_params=pltpu.CompilerParams(vmem_limit_bytes=32 * 2**20),
         cost_estimate=pl.CostEstimate(
-            flops=4 * rows * width * units * shards,
-            bytes_accessed=2 * (rows * width + 2 * shards * units * width),
+            flops=6 * rows * width * units * shards,
+            bytes_accessed=2 * (rows * width + 3 * shards * units * width),
             transcendentals=rows * units * shards,
         ),
-        name="expert_hidden",
-    )(incoming, all_gate, all_up)
-
-
-def slot_targets(block_routes, experts, capacity):
+        name="expert_part",
+    )(*operands)
+
+
+def swap(x, distance):
+    count = lax.axis_size("tp")
+    return lax.ppermute(x, "tp", [(i, i ^ distance) for i in range(count)])
+
+
+def spread_sum(term):
+    rows, width = term.shape
+    count = lax.axis_size("tp")
+    place = lax.axis_index("tp")
+    block = rows // count
+    parts = term.reshape(count // 2, 2, block, width)
+    low = place % 2
+    kept = lax.dynamic_index_in_dim(parts, low, 1, keepdims=False)
+    sent = lax.dynamic_index_in_dim(parts, 1 - low, 1, keepdims=False)
+    pair = (kept.astype(F32) + swap(sent, 1).astype(F32)).astype(BF16)
+    high = place // 2
+    kept = lax.dynamic_index_in_dim(pair, high, 0, keepdims=False)
+    sent = lax.dynamic_index_in_dim(pair, 1 - high, 0, keepdims=False)
+    return (kept.astype(F32) + swap(sent, 2).astype(F32)).astype(BF16)
+
+
+def slot_targets(block_routes, capacity):
     flat_routes = block_routes.reshape(-1)
     count = flat_routes.shape[0]
     order = jnp.arange(count, dtype=jnp.int32)
@@ -400,7 +442,7 @@
     return jnp.sum(marks, axis=2).astype(jnp.bfloat16)
 
 
-def on_device(
+def one_device(
     receptance,
     key_rows,
     value_rows,
@@ -427,9 +469,9 @@
     capacity = max(2, 2 * token_rows * top_count // experts)
     slab_rows = ep_count * capacity
 
-    all_gate = lax.all_gather(gate_weight[0], "tp")
-    all_up = lax.all_gather(up_weight[0], "tp")
-    all_down = lax.all_gather(down_weight[0], "tp")
+    own = (gate_weight[0], up_weight[0], down_weight[0])
+    far = tuple(swap(array, 2) for array in own)
+    near = tuple(swap(array, 1) for array in own)
 
     inputs = expert_input.astype(F32)
     expert_normed = (
@@ -437,7 +479,7 @@
         * lax.rsqrt(jnp.mean(inputs * inputs, axis=1, keepdims=True) + NORM_EPS)
         * expert_gain
     ).astype(BF16)
-    own_targets = slot_targets(routes, experts, capacity)
+    own_targets = slot_targets(routes, capacity)
     outgoing = jnp.dot(
         dispersal_table(own_targets, experts * capacity),
         expert_normed,
@@ -462,17 +504,24 @@
         head_size,
     )
     mixed = mixer_finish(summary, reader, local_read, channel_gain, head_size)
+    far_gate, far_up, arrived, mixed = lax.optimization_barrier(
+        (far[0], far[1], arrived, mixed)
+    )
+    cross_gate, cross_up = swap(far_gate, 1), swap(far_up, 1)
     mixer_term = jnp.dot(mixed, out_weight, preferred_element_type=F32)
-    mixer_out = lax.psum_scatter(
-        mixer_term.astype(BF16), "tp", scatter_dimension=0, tiled=True
-    )
-
-    hidden = expert_hidden(arrived, all_gate, all_up)
-    total = jnp.dot(
-        hidden, all_down.reshape(hidden.shape[1], model_width), preferred_element_type=F32
-    )
+    first = expert_part(arrived, (own, near), None, F32)
+    far_down, first, mixer_term = lax.optimization_barrier((far[2], first, mixer_term))
+    cross_down = swap(far_down, 1)
+    total = expert_part(
+        arrived,
+        ((far_gate, far_up, far_down), (cross_gate, cross_up, cross_down)),
+        first,
+        BF16,
+    )
+    total, mixer_term = lax.optimization_barrier((total, mixer_term))
+    mixer_out = spread_sum(mixer_term.astype(BF16))
     returned = lax.all_to_all(
-        total.astype(BF16).reshape(ep_count, capacity, model_width),
+        total.reshape(ep_count, capacity, model_width),
         "ep",
         split_axis=0,
         concat_axis=0,
@@ -490,7 +539,7 @@
 
 def solution(mesh):
     return jax.shard_map(
-        on_device,
+        one_device,
         mesh=mesh,
         in_specs=(
             P("ep", "tp"),

time: 192 us -> 173 us (0.901)
  waiting for transfers between devices: 79.5 us -> 46.3 us
  starting transfers between devices: 13.1 us -> 29.9 us
  between operations: 14 us -> 0.86 us
  Pallas kernels: 58.3 us -> 64.9 us
  other arithmetic: 0.47 us -> 6.09 us
  matrix products: 15.8 us -> 10.7 us
  local copies, waits for them, and re-layouts: 9.78 us -> 13.3 us
    all_gather x3 -> x0, waiting for transfers between devices: 32 us -> none  [the longest x1 24 us: on_device(): all_down = lax.all_gather(down_weight[0], 'tp')]
    ppermute x0 -> x11, waiting for transfers between devices: none -> 20.9 us  [swap(): return lax.ppermute(x, 'tp', [(i, i ^ distance) for i in range(count)])]
    all_to_all x2, waiting for transfers between devices: 45.5 us -> 25.5 us  [the longest x1 25.5 us: one_device(): lax.all_to_all(total.reshape(ep_count, capacity, model_width), 'ep', spli...]
    all_to_all x2, starting transfers between devices: 12.9 us -> 23.7 us  [the longest x1 16.3 us: one_device(): lax.all_to_all(total.reshape(ep_count, capacity, model_width), 'ep', spli...]
    ppermute x0 -> x11, starting transfers between devices: none -> 6.23 us  [swap(): return lax.ppermute(x, 'tp', [(i, i ^ distance) for i in range(count)])]
    pallas_call x1 -> x2, Pallas kernels: 6.78 us -> 12.9 us  [expert_part(): pl.pallas_call(functools.partial(part_kernel, shards, started), in_specs=...]
    dot_general x5 -> x4, matrix products: 15.8 us -> 10.7 us  [the longest x2 4.95 us: one_device(): chosen = jnp.dot(table, flat_rows, preferred_element_type=F32)]
    convert_element_type x0 -> x2, other arithmetic: none -> 3.89 us  [the longest x1 1.96 us: spread_sum(): return (kept.astype(F32) + swap(sent, 2).astype(F32)).astype(BF16)]
  transfers between devices with their start and end apart: 6 -> 13, of which waited for: 3 -> 6; matrix products, arithmetic and copies ran while one was open for 6% -> 5% of each run, Pallas kernels for 31% -> 34%
where the time goes in v1:
time: 173 us; the launch traced here: 172 us
  Pallas kernels  64.9 us (38%)
  waiting for transfers between devices  46.3 us (27%)
  starting transfers between devices  29.9 us (17%)
  local copies, waits for them, and re-layouts  13.3 us (8%)
  matrix products  10.7 us (6%)
  other arithmetic  6.09 us (4%)
    pallas_call x1, Pallas kernels, mixer_local(): pl.pallas_call(functools.partial(local_kernel, head_size), grid=(pairs,),...  30.2 us
    all_to_all x1, waiting for transfers between devices, one_device(): lax.all_to_all(total.reshape(ep_count, capacity, model_width), 'ep', spli...  25.5 us
    pallas_call x1, Pallas kernels, mixer_finish(): pl.pallas_call(functools.partial(finish_kernel, head_size), in_specs=[pl....  21.8 us
    ppermute x11, waiting for transfers between devices, swap(): return lax.ppermute(x, 'tp', [(i, i ^ distance) for i in range(count)])  20.9 us
    all_to_all x1, starting transfers between devices, one_device(): lax.all_to_all(total.reshape(ep_count, capacity, model_width), 'ep', spli...  16.3 us
    pallas_call x2, Pallas kernels, expert_part(): pl.pallas_call(functools.partial(part_kernel, shards, started), in_specs=...  12.9 us
    unnamed x32, local copies, waits for them, and re-layouts  10.8 us
    all_to_all x1, starting transfers between devices, one_device(): lax.all_to_all(outgoing.reshape(experts, capacity, model_width), 'ep', sp...  7.41 us
  transfers between devices with their start and end apart: 13, of which 6 were waited for; matrix products, arithmetic and copies ran while one was open for 5% of the time, Pallas kernels for 34%

profile of v1, /device:TPU:0, one launch (start us, length us, event | category | flops | bytes accessed | tf_op | source)
XLA Modules:
  0.0 172.1 jit_solution(65853278420049171)
XLA Ops:
  0.6 0.0 copy-start
  0.6 0.9 copy.37
  1.6 0.1 eq.61
  1.7 0.2 convert_reduce_fusion.1
  1.9 0.1 reshape.44
  2.1 0.1 copy.38
  2.1 0.7 multiply_add_fusion
  2.8 0.1 convert_reduce_fusion
  2.9 1.2 fusion.3
  4.1 3.2 %convolution_convert_fusion = bf16[512,2048]{1,0:T(8,128)(2,1)} fusion(bf16[128,2048]{1,0:T(8,128)(2,1)} %param.25, f32[2048]{0:T(1024)} %param.26, f32[128]{0:T(128)S(1)} %add_rsqrt_fusion, s32[512,128]{1,0:T(8,128)S(1)} %convert_reduce_fusion), kind=kOutput, calls=%fused_computation | convolution fusion | flops 270598144 | bytes 2892288 | tf_op jit(solution)/shard_map/dot_general | solution.py:483
  7.3 7.4 %all-to-all-start = ((bf16[8,64,2048]{2,1,0:T(8,128)(2,1)}), bf16[8,64,2048]{2,1,0:T(8,128)(2,1)}, u32[]{:S(2)}, u32[]{:S(2)}) async-start(bf16[8,64,2048]{2,1,0:T(8,128)(2,1)} %bitcast.43), calls=%async_computation | async-start | bytes 4194304 | tf_op jit(solution)/shard_map/all_to_all | solution.py:488
  14.7 1.5 collective-permute-start
  16.2 0.0 collective-permute-start.3
  16.2 0.5 collective-permute-start.1
  16.7 0.2 collective-permute-start.4
  17.0 0.3 collective-permute-start.5
  17.2 0.0 copy-done.13
  17.2 0.1 copy.39.shift_ref
  17.4 0.0 copy-start.4
  17.4 1.0 copy-done.4
  18.4 1.0 copy-done.5
  19.5 1.0 copy-done.6
  20.5 1.0 copy-done.7
  21.6 1.0 copy-done.8
  22.6 30.2 %mixer_local.1 = (bf16[512,512]{1,0:T(8,128)(2,1)S(1)}, f32[512,512]{1,0:T(8,128)S(1)}, bf16[2,256,128]{2,1,0:T(8,128)(2,1)S(1)}) custom-call(bf16[512,512]{1,0:T(8,128)(2,1)S(1)} %copy-done.4, bf16[512,512]{1,0:T(8,128)(2,1)S(1)} %copy-done.5, bf16[512,512]{1,0:T(8,128)(2,1)S(1)} %copy-done.6, bf16[512,512]{1,0:T(8,128)(2,1)S(1)} %copy-done.7, ...), custom_call_target="tpu_custom_call" | custom-call | flops 20000000000 | bytes 6291456 | tf_op jit(solution)/shard_map/mixer_local/pallas_call | solution.py:233
  52.8 0.0 collective-permute-done.refs_1_
  52.8 1.6 collective-permute-start.2
  54.4 0.0 copy-done.10
  54.4 21.8 %mixer_finish.1 = bf16[512,512]{1,0:T(8,128)(2,1)S(1)} custom-call(bf16[2,256,128]{2,1,0:T(8,128)(2,1)S(1)} %get-tuple-element.14.summary_ref, bf16[512,512]{1,0:T(8,128)(2,1)S(1)} %get-tuple-element.15.reader_ref, f32[512,512]{1,0:T(8,128)S(1)} %get-tuple-element.16.local_ref, f32[1,512]{1,0:T(1,128)S(1)} %bitcast.42), custom_call_target="tpu_custom_call" | custom-call | flops 10000000000 | bytes 4194304 | tf_op jit(solution)/shard_map/mixer_finish/pallas_call | solution.py:341
  76.3 0.0 copy-start.11
  76.3 0.8 copy-done.11
  77.1 0.0 collective-permute-done.1.refs_2_
  77.1 0.0 all-to-all-done
  77.1 0.0 collective-permute-done.3.refs_4_
  77.1 0.0 collective-permute-done.4.refs_5_
  77.1 0.0 collective-permute-done.5.refs_6_
  77.1 0.0 copy-start.2
  77.1 1.2 copy-done.2
  78.3 1.2 copy-done.3
  79.5 6.7 %expert_part.2.refs_7_ = f32[512,2048]{1,0:T(8,128)S(1)} custom-call(bf16[512,2048]{1,0:T(8,128)(2,1)} %bitcast.3.refs_0_, bf16[2048,256]{1,0:T(8,128)(2,1)S(1)} %bitcast.37, bf16[2048,256]{1,0:T(8,128)(2,1)S(1)} %bitcast.40, bf16[256,2048]{1,0:T(8,128)(2,1)} %bitcast.6.refs_3_, bf16[2048,256]{1,0:T(8,128)(2,1)} %collective-permute-done.3.refs_4_, ...), custom_call_target="tpu_custom_call" | custom-call | flops 3221225472 | bytes 8388608 | tf_op jit(solution)/shard_map/expert_part/pallas_call | solution.py:393
  86.2 2.6 %fusion.14 = bf16[512,2048]{1,0:T(8,128)(2,1)} fusion(bf16[512,512]{1,0:T(8,128)(2,1)S(1)} %copy-done.12, bf16[512,2048]{1,0:T(8,128)(2,1)S(1)} %copy-done), kind=kOutput, calls=%fused_computation.34 | convolution fusion | flops 1073741824 | bytes 4718592 | tf_op jit(solution)/shard_map/dot_general | solution.py:511
  88.8 0.0 collective-permute-done.2.refs_3_
  88.8 0.0 collective-permute-start.8
  88.8 0.5 collective-permute-start.6
  89.3 0.0 collective-permute-start.7
  89.3 2.4 %collective-permute-done.8.refs_6_ = bf16[256,2048]{1,0:T(8,128)(2,1)S(1)} collective-permute-done((bf16[256,2048]{1,0:T(8,128)(2,1)}, bf16[256,2048]{1,0:T(8,128)(2,1)S(1)}, u32[]{:S(2)}, u32[]{:S(2)}) %collective-permute-start.8) | collective-permute-done | bytes 1048608 | tf_op jit(solution)/shard_map/ppermute | solution.py:410
  91.7 1.5 collective-permute-done.6.refs_4_
  93.2 1.5 collective-permute-done.7.refs_5_
  94.7 6.2 %expert_part.3 = bf16[512,2048]{1,0:T(8,128)(2,1)S(1)} custom-call(bf16[512,2048]{1,0:T(8,128)(2,1)} %bitcast.3.refs_0_, bf16[2048,256]{1,0:T(8,128)(2,1)S(1)} %collective-permute-done.refs_1_, bf16[2048,256]{1,0:T(8,128)(2,1)} %collective-permute-done.1.refs_2_, bf16[256,2048]{1,0:T(8,128)(2,1)} %collective-permute-done.2.refs_3_, ...), custom_call_target="tpu_custom_call" | custom-call | flops 3221225472 | bytes 8388608 | tf_op jit(solution)/shard_map/expert_part/pallas_call | solution.py:393
  100.9 0.0 copy-start.1
  100.9 1.3 copy-done.1
  102.2 16.3 %all-to-all-start.1 = ((bf16[8,64,2048]{2,1,0:T(8,128)(2,1)}), bf16[8,64,2048]{2,1,0:T(8,128)(2,1)}, u32[]{:S(2)}, u32[]{:S(2)}) async-start(bf16[8,64,2048]{2,1,0:T(8,128)(2,1)} %bitcast.34), calls=%async_computation.1 | async-start | bytes 4194304 | tf_op jit(solution)/shard_map/all_to_all | solution.py:523
  118.5 1.3 dynamic-slice_bitcast_fusion
  119.8 0.1 collective-permute-start.9
  119.9 0.0 copy-start.14
  119.9 2.7 %collective-permute-done.9 = bf16[2,128,2048]{2,1,0:T(8,128)(2,1)} collective-permute-done((bf16[2,128,2048]{2,1,0:T(8,128)(2,1)S(1)}, bf16[2,128,2048]{2,1,0:T(8,128)(2,1)}, u32[]{:S(2)}, u32[]{:S(2)}) %collective-permute-start.9) | collective-permute-done | bytes 1048608 | tf_op jit(solution)/shard_map/ppermute | solution.py:410
  122.7 1.9 %fusion.2 = bf16[2,128,2048]{2,1,0:T(8,128)(2,1)S(1)} fusion(bf16[2,128,2048]{2,1,0:T(8,128)(2,1)} %collective-permute-done.9, bf16[2,2,128,2048]{3,2,1,0:T(8,128)(2,1)} %bitcast.45, s32[]{:T(128)S(6)} %select_n.26), kind=kLoop, calls=%fused_computation.6 | loop fusion | flops 2097152 | bytes 3145732 | tf_op jit(solution)/shard_map/convert_element_type | solution.py:422
  124.6 0.8 dynamic-slice_bitcast_fusion.1
  125.4 1.5 collective-permute-start.10
  127.0 12.7 %collective-permute-done.10 = bf16[128,2048]{1,0:T(8,128)(2,1)} collective-permute-done((bf16[128,2048]{1,0:T(8,128)(2,1)}, bf16[128,2048]{1,0:T(8,128)(2,1)}, u32[]{:S(2)}, u32[]{:S(2)}) %collective-permute-start.10) | collective-permute-done | bytes 524320 | tf_op jit(solution)/shard_map/ppermute | solution.py:410
  139.7 2.0 %fusion.6 = bf16[128,2048]{1,0:T(8,128)(2,1)} fusion(bf16[128,2048]{1,0:T(8,128)(2,1)} %collective-permute-done.10, bf16[2,128,2048]{2,1,0:T(8,128)(2,1)S(1)} %fusion.2, s32[]{:T(128)S(6)} %select_n.29), kind=kLoop, calls=%fused_computation.13 | loop fusion | flops 1048576 | bytes 1572868 | tf_op jit(solution)/shard_map/convert_element_type | solution.py:426
  141.7 25.5 %all-to-all-done.1 = bf16[8,64,2048]{2,1,0:T(8,128)(2,1)} async-done(((bf16[8,64,2048]{2,1,0:T(8,128)(2,1)}), bf16[8,64,2048]{2,1,0:T(8,128)(2,1)}, u32[]{:S(2)}, u32[]{:S(2)}) %all-to-all-start.1) | async-done | bytes 2097184 | tf_op jit(solution)/shard_map/all_to_all | solution.py:523
  167.2 2.1 %convolution_multiply_fusion.1 = f32[128,2048]{1,0:T(8,128)S(1)} fusion(bf16[512,2048]{1,0:T(8,128)(2,1)} %bitcast.14, f32[128]{0:T(128)S(1)} %get-tuple-element.29, s32[128]{0:T(128)S(1)} %get-tuple-element.27), kind=kOutput, calls=%fused_computation.3 | convolution fusion | flops 268763136 | bytes 3146752 | tf_op jit(solution)/shard_map/dot_general | solution.py:535
  169.2 2.9 %fusion.1 = bf16[128,2048]{1,0:T(8,128)(2,1)} fusion(f32[128,2048]{1,0:T(8,128)S(1)} %convolution_multiply_fusion.1, bf16[512,2048]{1,0:T(8,128)(2,1)} %bitcast.14, f32[128]{0:T(128)S(1)} %get-tuple-element.28, s32[128]{0:T(128)S(1)} %get-tuple-element.26), kind=kOutput, calls=%fused_computation.4 | convolution fusion | flops 269287424 | bytes 3671040 | tf_op jit(solution)/shard_map/dot_general | solution.py:535
  (16 shorter events, 0.0 us)
Async XLA Ops:
  0.6 85.6 %copy-start = (bf16[512,2048]{1,0:T(8,128)(2,1)S(1)}, bf16[512,2048]{1,0:T(8,128)(2,1)}, u32[]{:S(2)}) copy-start(bf16[512,2048]{1,0:T(8,128)(2,1)} %param.24) | copy-start | bytes 6291460
  7.3 10.0 %copy-start.13 = (f32[512,8]{0,1:T(8,128)S(1)}, f32[512,8]{0,1:T(8,128)}, u32[]{:S(2)}) copy-start(f32[512,8]{0,1:T(8,128)} %param.22) | copy-start | bytes 49156
  7.3 10.1 %copy-start.9 = (f32[512]{0:T(512)S(1)}, f32[512]{0:T(512)}, u32[]{:S(2)}) copy-start(f32[512]{0:T(512)} %param.21) | copy-start | bytes 6148
  7.3 69.8 %all-to-all-start = ((bf16[8,64,2048]{2,1,0:T(8,128)(2,1)}), bf16[8,64,2048]{2,1,0:T(8,128)(2,1)}, u32[]{:S(2)}, u32[]{:S(2)}) async-start(bf16[8,64,2048]{2,1,0:T(8,128)(2,1)} %bitcast.43), calls=%async_computation | async-start | bytes 4194304 | tf_op jit(solution)/shard_map/all_to_all | solution.py:488
  14.7 38.1 %collective-permute-start = (bf16[2048,256]{1,0:T(8,128)(2,1)}, bf16[2048,256]{1,0:T(8,128)(2,1)S(1)}, u32[]{:S(2)}, u32[]{:S(2)}) collective-permute-start(bf16[2048,256]{1,0:T(8,128)(2,1)} %bitcast.35), channel_id=1, source_target_pairs={{0,2},{1,3},{2,0},{3,1},{4,6},{5,7},{6,4},{7,5},{8,10},{9,11},{10,... | collective-permute-start | bytes 3145736 | tf_op jit(solution)/shard_map/ppermute | solution.py:410
  16.2 60.8 %collective-permute-start.3 = (bf16[2048,256]{1,0:T(8,128)(2,1)}, bf16[2048,256]{1,0:T(8,128)(2,1)}, u32[]{:S(2)}, u32[]{:S(2)}) collective-permute-start(bf16[2048,256]{1,0:T(8,128)(2,1)} %bitcast.36), channel_id=1, source_target_pairs={{0,1},{1,0},{2,3},{3,2},{4,5},{5,4},{6,7},{7,6},{8,9},{9,8},{10,11... | collective-permute-start | bytes 3145736 | tf_op jit(solution)/shard_map/ppermute | solution.py:410
  16.2 60.8 %collective-permute-start.1 = (bf16[2048,256]{1,0:T(8,128)(2,1)}, bf16[2048,256]{1,0:T(8,128)(2,1)}, u32[]{:S(2)}, u32[]{:S(2)}) collective-permute-start(bf16[2048,256]{1,0:T(8,128)(2,1)} %bitcast.38), channel_id=1, source_target_pairs={{0,2},{1,3},{2,0},{3,1},{4,6},{5,7},{6,4},{7,5},{8,10},{9,11},{10,... | collective-permute-start | bytes 3145736 | tf_op jit(solution)/shard_map/ppermute | solution.py:410
  16.7 60.3 %collective-permute-start.4 = (bf16[2048,256]{1,0:T(8,128)(2,1)}, bf16[2048,256]{1,0:T(8,128)(2,1)}, u32[]{:S(2)}, u32[]{:S(2)}) collective-permute-start(bf16[2048,256]{1,0:T(8,128)(2,1)} %bitcast.39), channel_id=1, source_target_pairs={{0,1},{1,0},{2,3},{3,2},{4,5},{5,4},{6,7},{7,6},{8,9},{9,8},{10,11... | collective-permute-start | bytes 3145736 | tf_op jit(solution)/shard_map/ppermute | solution.py:410
  17.0 60.1 %collective-permute-start.5 = (bf16[256,2048]{1,0:T(8,128)(2,1)}, bf16[256,2048]{1,0:T(8,128)(2,1)}, u32[]{:S(2)}, u32[]{:S(2)}) collective-permute-start(bf16[256,2048]{1,0:T(8,128)(2,1)} %bitcast.6.refs_3_), channel_id=1, source_target_pairs={{0,1},{1,0},{2,3},{3,2},{4,5},{5,4},{6,7},{7,6},{8,9},{9,8},{10,11... | collective-permute-start | bytes 3145736 | tf_op jit(solution)/shard_map/ppermute | solution.py:410
  17.4 1.0 copy-start.4
  18.4 1.0 copy-start.5
  19.5 1.0 copy-start.6
  20.5 1.0 copy-start.7
  21.6 1.0 copy-start.8
  22.6 31.8 %copy-start.10 = (f32[512]{0:T(512)S(1)}, f32[512]{0:T(512)}, u32[]{:S(2)}) copy-start(f32[512]{0:T(512)} %param.23) | copy-start | bytes 6148
  52.8 36.0 %collective-permute-start.2 = (bf16[256,2048]{1,0:T(8,128)(2,1)}, bf16[256,2048]{1,0:T(8,128)(2,1)}, u32[]{:S(2)}, u32[]{:S(2)}) collective-permute-start(bf16[256,2048]{1,0:T(8,128)(2,1)} %bitcast.6.refs_3_), channel_id=1, source_target_pairs={{0,2},{1,3},{2,0},{3,1},{4,6},{5,7},{6,4},{7,5},{8,10},{9,11},{10,... | collective-permute-start | bytes 3145736 | tf_op jit(solution)/shard_map/ppermute | solution.py:410
  76.3 0.8 copy-start.11
  77.1 1.2 copy-start.2
  78.3 1.2 copy-start.3
  79.5 6.7 %copy-start.12 = (bf16[512,512]{1,0:T(8,128)(2,1)S(1)}, bf16[512,512]{1,0:T(8,128)(2,1)}, u32[]{:S(2)}) copy-start(bf16[512,512]{1,0:T(8,128)(2,1)} %copy-done.11) | copy-start | bytes 1572868
  88.8 2.9 %collective-permute-start.8 = (bf16[256,2048]{1,0:T(8,128)(2,1)}, bf16[256,2048]{1,0:T(8,128)(2,1)S(1)}, u32[]{:S(2)}, u32[]{:S(2)}) collective-permute-start(bf16[256,2048]{1,0:T(8,128)(2,1)} %collective-permute-done.2.refs_3_), channel_id=1, source_target_pairs={{0,1},{1,0},{2,3},{3,2},{4,5},{5,4},{6,7},{7,6},{8,9},{9,8},{10,11... | collective-permute-start | bytes 3145736 | tf_op jit(solution)/shard_map/ppermute | solution.py:410
  88.8 4.4 %collective-permute-start.6 = (bf16[2048,256]{1,0:T(8,128)(2,1)S(1)}, bf16[2048,256]{1,0:T(8,128)(2,1)S(1)}, u32[]{:S(2)}, u32[]{:S(2)}) collective-permute-start(bf16[2048,256]{1,0:T(8,128)(2,1)S(1)} %collective-permute-done.refs_1_), channel_id=1, source_target_pairs={{0,1},{1,0},{2,3},{3,2},{4,5},{5,4},{6,7},{7,6},{8,9},{9,8},{10,11... | collective-permute-start | bytes 3145736 | tf_op jit(solution)/shard_map/ppermute | solution.py:410
  89.3 5.4 %collective-permute-start.7 = (bf16[2048,256]{1,0:T(8,128)(2,1)}, bf16[2048,256]{1,0:T(8,128)(2,1)S(1)}, u32[]{:S(2)}, u32[]{:S(2)}) collective-permute-start(bf16[2048,256]{1,0:T(8,128)(2,1)} %collective-permute-done.1.refs_2_), channel_id=1, source_target_pairs={{0,1},{1,0},{2,3},{3,2},{4,5},{5,4},{6,7},{7,6},{8,9},{9,8},{10,11... | collective-permute-start | bytes 3145736 | tf_op jit(solution)/shard_map/ppermute | solution.py:410
  100.9 1.3 copy-start.1
  102.2 64.9 %all-to-all-start.1 = ((bf16[8,64,2048]{2,1,0:T(8,128)(2,1)}), bf16[8,64,2048]{2,1,0:T(8,128)(2,1)}, u32[]{:S(2)}, u32[]{:S(2)}) async-start(bf16[8,64,2048]{2,1,0:T(8,128)(2,1)} %bitcast.34), calls=%async_computation.1 | async-start | bytes 4194304 | tf_op jit(solution)/shard_map/all_to_all | solution.py:523
  119.8 2.9 %collective-permute-start.9 = (bf16[2,128,2048]{2,1,0:T(8,128)(2,1)S(1)}, bf16[2,128,2048]{2,1,0:T(8,128)(2,1)}, u32[]{:S(2)}, u32[]{:S(2)}) collective-permute-start(bf16[2,128,2048]{2,1,0:T(8,128)(2,1)S(1)} %dynamic-slice_bitcast_fusion), channel_id=1, source_target_pairs={{0,1},{1,0},{2,3},{3,2},{4,5},{5,4},{6,7},{7,6},{8,9},{9,8},{10,11... | collective-permute-start | bytes 3145736 | tf_op jit(solution)/shard_map/ppermute | solution.py:410
  119.9 7.0 %copy-start.14 = (f32[128,2]{0,1:T(2,128)S(1)}, f32[128,2]{0,1:T(2,128)}, u32[]{:S(2)}) copy-start(f32[128,2]{0,1:T(2,128)} %param.28) | copy-start | bytes 3076
  125.4 14.3 %collective-permute-start.10 = (bf16[128,2048]{1,0:T(8,128)(2,1)}, bf16[128,2048]{1,0:T(8,128)(2,1)}, u32[]{:S(2)}, u32[]{:S(2)}) collective-permute-start(bf16[128,2048]{1,0:T(8,128)(2,1)} %dynamic-slice_bitcast_fusion.1), channel_id=1, source_target_pairs={{0,2},{1,3},{2,0},{3,1},{4,6},{5,7},{6,4},{7,5},{8,10},{9,11},{10,... | collective-permute-start | bytes 1572872 | tf_op jit(solution)/shard_map/ppermute | solution.py:410

commit v2 on v1

--- a/solution.py
+++ b/solution.py
@@ -230,6 +230,10 @@
     half = LANES // 2
     tile = pl.BlockSpec((rows, LANES), lambda p: (0, p))
     small = pl.BlockSpec((2, half, LANES), lambda p: (0, p, 0))
+    streams = [
+        pltpu.with_memory_space_constraint(array, pltpu.HBM)
+        for array in (receptance, keys, values, decay, learn)
+    ]
     return pl.pallas_call(
         functools.partial(local_kernel, head_size),
         grid=(pairs,),
@@ -252,7 +256,7 @@
             flops=20 * 10**9, bytes_accessed=6 * 2**20, transcendentals=10**6
         ),
         name="mixer_local",
-    )(receptance, keys, values, decay, learn, base.reshape(pairs, 1, LANES), shift)
+    )(*streams, base.reshape(pairs, 1, LANES), shift)
 
 
 def finish_kernel(
@@ -262,24 +266,28 @@
     local_ref,
     gain_ref,
     out_ref,
+    before,
+    sending,
     landed,
     send_sems,
     recv_sems,
 ):
     here = lax.axis_index("ep")
     count = lax.axis_size("ep")
+    rounds = landed.shape[0]
     half = LANES // 2
     _, channels = reader_ref.shape
     pairs = channels // LANES
     matched = same_head(head_size)
     block = matched.astype(BF16)
-
-    def transfer(distance, target):
+    diagonal = grid_index((LANES, LANES), 0) == grid_index((LANES, LANES), 1)
+
+    def transfer(level, distance, target):
         return pltpu.make_async_remote_copy(
-            src_ref=summary_ref,
-            dst_ref=landed.at[distance - 1],
+            src_ref=sending,
+            dst_ref=landed.at[level],
             send_sem=send_sems.at[distance - 1],
-            recv_sem=recv_sems.at[distance - 1],
+            recv_sem=recv_sems.at[level],
             device_id={"ep": target},
             device_id_type=pl.DeviceIdType.MESH,
         )
@@ -296,57 +304,87 @@
         return nothing
 
     lax.fori_loop(1, count, greet, 0)
+
+    def wide(part):
+        part = part.astype(F32)
+        return jnp.where(matched, jnp.concatenate([part, part], axis=0), 0.0)
+
+    def spot(p):
+        return slice(p * half, (p + 1) * half)
+
+    for p in range(pairs):
+        before[0, p] = jnp.where(diagonal, 1.0, 0.0)
+        before[1, p] = jnp.zeros((LANES, LANES), F32)
     pl.semaphore_wait(barrier, count - 1)
 
-    def launch(distance, nothing):
-        transfer(distance, here + distance).start()
-        return nothing
-
-    lax.fori_loop(1, count - here, launch, 0)
-
-    def wide(place, kind, p):
-        part = landed[place, kind, p * half : (p + 1) * half].astype(F32)
-        return jnp.where(matched, jnp.concatenate([part, part], axis=0), 0.0)
-
-    def turn(k, states):
-        distance = here - k
-        transfer(distance, k).wait_recv()
-        after = []
-        for p in range(pairs):
-            high, low = split_two(states[p])
-            moved = mm(jnp.concatenate([high, low], axis=0), wide(distance - 1, 0, p))
-            after.append(moved[:LANES] + moved[LANES:] + wide(distance - 1, 1, p))
-        return tuple(after)
-
-    nothing = tuple(jnp.zeros((LANES, LANES), F32) for _ in range(pairs))
-    entering = lax.fori_loop(0, here, turn, nothing)
+    for level in range(rounds):
+        reach = 2**level
+
+        @pl.when(lax.rem(here, 2 * reach) == reach - 1)
+        def _(level=level, reach=reach):
+            for p in range(pairs):
+                both = jnp.concatenate([before[0, p], before[1, p]], axis=0)
+                high, low = split_two(both)
+                step = wide(summary_ref[0, spot(p)])
+                moved = mm(high, step) + mm(low, step)
+                after = moved[LANES:] + wide(summary_ref[1, spot(p)])
+                sending[0, spot(p)] = (moved[:half] + moved[half:LANES]).astype(BF16)
+                sending[1, spot(p)] = (after[:half] + after[half:]).astype(BF16)
+
+            def launch(distance, nothing):
+                transfer(level, distance, here + distance).start()
+                return nothing
+
+            lax.fori_loop(1, reach + 1, launch, 0)
+
+        @pl.when(lax.rem(here // reach, 2) == 1)
+        def _(level=level, reach=reach):
+            transfer(level, 1, here).wait_recv()
+            for p in range(pairs):
+                both = jnp.concatenate(
+                    [wide(landed[level, 0, spot(p)]), wide(landed[level, 1, spot(p)])], axis=0
+                )
+                high, low = split_two(before[0, p])
+                moved = mm(both, high) + mm(both, low)
+                before[0, p] = moved[:LANES]
+                before[1, p] = moved[LANES:] + before[1, p]
+
     for p in range(pairs):
         lanes = slice(p * LANES, (p + 1) * LANES)
-        read = mm_nt(reader_ref[:, lanes], entering[p]) + local_ref[:, lanes]
+        read = mm_nt(reader_ref[:, lanes], before[1, p]) + local_ref[:, lanes]
         centred = read - head_sums(read, block) * (1.0 / head_size)
         variance = head_sums(centred * centred, block) * (1.0 / head_size)
         scaled = centred * lax.rsqrt(variance + GROUP_EPS) * gain_ref[:, lanes]
         out_ref[:, lanes] = scaled.astype(BF16)
 
-    def settle(distance, nothing):
-        transfer(distance, here + distance).wait_send()
-        return nothing
-
-    lax.fori_loop(1, count - here, settle, 0)
+    for level in range(rounds):
+        reach = 2**level
+
+        @pl.when(lax.rem(here, 2 * reach) == reach - 1)
+        def _(level=level, reach=reach):
+            def settle(distance, nothing):
+                transfer(level, distance, here + distance).wait_send()
+                return nothing
+
+            lax.fori_loop(1, reach + 1, settle, 0)
 
 
 def mixer_finish(summary, reader, local_read, gain, head_size):
     rows, channels = reader.shape
+    pairs = channels // LANES
     count = lax.axis_size("ep")
+    rounds = (count - 1).bit_length()
     return pl.pallas_call(
         functools.partial(finish_kernel, head_size),
         in_specs=[pl.BlockSpec(memory_space=pltpu.VMEM)] * 4,
         out_specs=pl.BlockSpec(memory_space=pltpu.VMEM),
         out_shape=jax.ShapeDtypeStruct((rows, channels), BF16),
         scratch_shapes=[
-            pltpu.VMEM((count - 1,) + summary.shape, BF16),
-            pltpu.SemaphoreType.DMA((count - 1,)),
-            pltpu.SemaphoreType.DMA((count - 1,)),
+            pltpu.VMEM((2, pairs, LANES, LANES), F32),
+            pltpu.VMEM(summary.shape, BF16),
+            pltpu.VMEM((rounds,) + summary.shape, BF16),
+            pltpu.SemaphoreType.DMA((count // 2,)),
+            pltpu.SemaphoreType.DMA((rounds,)),
         ],
         compiler_params=pltpu.CompilerParams(
             vmem_limit_bytes=32 * 2**20, collective_id=0, has_side_effects=True
@@ -358,72 +396,260 @@
     )(summary, reader, local_read, gain.reshape(1, channels))
 
 
-def part_kernel(shards, started, *refs):
-    x_ref = refs[0]
-    weights = refs[1 : 1 + 3 * shards]
-    total_ref = refs[1 + 3 * shards] if started else None
-    out_ref = refs[-1]
+def gated(x, gate, up):
+    gates = mm(x, gate)
+    uppers = mm(x, up)
+    return (gates / (1.0 + jnp.exp(-gates)) * uppers).astype(BF16)
+
+
+def part_kernel(x_ref, *refs):
+    weights, (total_ref, hidden_ref) = refs[:-2], refs[-2:]
     rows = x_ref.shape[0]
+    units = weights[0].shape[1]
     piece = min(rows, 256)
 
     def block(step, nothing):
         here = pl.ds(pl.multiple_of(step * piece, piece), piece)
         x = x_ref[here]
-        total = total_ref[here] if started else None
-        for s in range(shards):
+        total = None
+        for s in range(2):
             gate, up, down = weights[3 * s : 3 * s + 3]
-            gates = mm(x, gate[...])
-            uppers = mm(x, up[...])
-            hidden = (gates / (1.0 + jnp.exp(-gates)) * uppers).astype(BF16)
-            term = mm(hidden, down[...])
+            term = mm(gated(x, gate[...], up[...]), down[...])
             total = term if total is None else total + term
-        out_ref[here] = total.astype(out_ref.dtype)
+        total_ref[here] = total
+        for s in range(2):
+            gate, up = weights[6 + 2 * s : 8 + 2 * s]
+            hidden_ref[here, s * units : (s + 1) * units] = gated(x, gate[...], up[...])
         return nothing
 
     lax.fori_loop(0, rows // piece, block, 0)
 
 
-def expert_part(incoming, weights, total, out_type):
+def expert_part(incoming, full, partial):
     rows, width = incoming.shape
-    shards = len(weights)
-    units = weights[0][0].shape[1]
-    started = total is not None
-    flat = [array for shard in weights for array in shard]
-    operands = [incoming] + flat + ([total] if started else [])
+    units = full[0][0].shape[1]
+    flat = [array for shard in full + partial for array in shard]
+    operands = [incoming] + flat
     return pl.pallas_call(
-        functools.partial(part_kernel, shards, started),
+        part_kernel,
         in_specs=[pl.BlockSpec(memory_space=pltpu.VMEM)] * len(operands),
-        out_specs=pl.BlockSpec(memory_space=pltpu.VMEM),
-        out_shape=jax.ShapeDtypeStruct((rows, width), out_type),
+        out_specs=[pl.BlockSpec(memory_space=pltpu.VMEM)] * 2,
+        out_shape=[
+            jax.ShapeDtypeStruct((rows, width), F32),
+            jax.ShapeDtypeStruct((rows, 2 * units), BF16),
+        ],
         compiler_params=pltpu.CompilerParams(vmem_limit_bytes=32 * 2**20),
         cost_estimate=pl.CostEstimate(
-            flops=6 * rows * width * units * shards,
-            bytes_accessed=2 * (rows * width + 3 * shards * units * width),
-            transcendentals=rows * units * shards,
+            flops=20 * rows * width * units,
+            bytes_accessed=2 * (rows * width + 10 * units * width),
+            transcendentals=4 * rows * units,
         ),
         name="expert_part",
     )(*operands)
 
 
+def return_kernel(
+    capacity,
+    mixed_ref,
+    project_ref,
+    total_ref,
+    hidden_ref,
+    far_ref,
+    target_ref,
+    weight_ref,
+    mixer_ref,
+    expert_ref,
+    cross,
+    staged,
+    landed,
+    term,
+    near_in,
+    pair_out,
+    far_in,
+    combined,
+    send_sems,
+    recv_sems,
+    side_send,
+    side_recv,
+):
+    here = lax.axis_index("ep")
+    count = lax.axis_size("ep")
+    place = lax.axis_index("tp")
+    low, high = lax.rem(place, 2), place // 2
+    beside = place + 1 - 2 * low
+    across = place + 2 - 4 * high
+    units = far_ref.shape[0]
+    tokens = expert_ref.shape[0]
+
+    def side(src, dst, index, target):
+        return pltpu.make_async_remote_copy(
+            src_ref=src,
+            dst_ref=dst,
+            send_sem=side_send.at[index],
+            recv_sem=side_recv.at[index],
+            device_id={"tp": target},
+            device_id_type=pl.DeviceIdType.MESH,
+        )
+
+    def rows_of(member):
+        return pl.ds(pl.multiple_of(member * capacity, capacity), capacity)
+
+    def back(distance, member):
+        return pltpu.make_async_remote_copy(
+            src_ref=staged.at[rows_of(member)],
+            dst_ref=landed.at[rows_of(here)],
+            send_sem=send_sems.at[distance - 1],
+            recv_sem=recv_sems.at[distance - 1],
+            device_id={"ep": member},
+            device_id_type=pl.DeviceIdType.MESH,
+        )
+
+    barrier = pltpu.get_barrier_semaphore()
+
+    def greet(distance, nothing):
+        pl.semaphore_signal(
+            barrier,
+            inc=1,
+            device_id={"ep": lax.rem(here + distance, count)},
+            device_id_type=pl.DeviceIdType.MESH,
+        )
+        return nothing
+
+    lax.fori_loop(1, count, greet, 0)
+    for target in (beside, across):
+        pl.semaphore_signal(
+            barrier,
+            inc=1,
+            device_id={"tp": target},
+            device_id_type=pl.DeviceIdType.MESH,
+        )
+    pl.semaphore_wait(barrier, count + 1)
+
+    forward = side(far_ref, cross, 0, beside)
+    forward.start()
+    forward.wait_recv()
+
+    def finished(member):
+        rows = rows_of(member)
+        hidden = hidden_ref[rows]
+        row = total_ref[rows] + mm(hidden[:, :units], far_ref[...])
+        return (row + mm(hidden[:, units:], cross[...])).astype(BF16)
+
+    def far_first(k):
+        return count // 2 + ((k + 1) // 2) * (2 * lax.rem(k, 2) - 1)
+
+    def send_block(k, nothing):
+        distance = far_first(k)
+        member = lax.rem(here + distance, count)
+        staged[rows_of(member)] = finished(member)
+        back(distance, member).start()
+        return nothing
+
+    lax.fori_loop(0, count - 1, send_block, 0)
+    landed[rows_of(here)] = finished(here)
+
+    def project(b, nothing):
+        rows = pl.ds(pl.multiple_of(b * tokens, tokens), tokens)
+        term[rows] = mm(mixed_ref[rows], project_ref[...]).astype(BF16)
+        return nothing
+
+    def block_rows(b):
+        return pl.ds(pl.multiple_of(b * tokens, tokens), tokens)
+
+    lax.fori_loop(0, 4, project, 0)
+    nears = [
+        side(term.at[block_rows(2 * y + 1 - low)], near_in.at[y], 1 + y, beside)
+        for y in range(2)
+    ]
+    for copy in nears:
+        copy.start()
+
+    target = target_ref[...]
+    weight = weight_ref[...]
+    slot = grid_index((tokens, capacity), 1)
+
+    def taken(member):
+        table = jnp.zeros((tokens, capacity), F32)
+        scale = jnp.zeros((tokens, 1), F32)
+        for picked in range(target.shape[1]):
+            own = target[:, picked : picked + 1] - member * capacity
+            table = jnp.where(own == slot, 1.0, table)
+            inside = (own >= 0) & (own < capacity)
+            scale = jnp.where(inside, weight[:, picked : picked + 1], scale)
+        return mm(table, landed[rows_of(member)]) * scale
+
+    combined[...] = taken(here)
+
+    for copy in nears:
+        copy.wait_recv()
+    other = 1 - high
+    pair_out[...] = (
+        term[block_rows(2 * other + low)].astype(F32) + near_in[other].astype(F32)
+    ).astype(BF16)
+    cross_send = side(pair_out, far_in, 3, across)
+    cross_send.start()
+
+    def gather_block(k, nothing):
+        distance = far_first(count - 2 - k)
+        member = lax.rem(here + count - distance, count)
+        back(distance, member).wait_recv()
+        combined[...] += taken(member)
+        return nothing
+
+    lax.fori_loop(0, count // 2, gather_block, 0)
+    cross_send.wait_recv()
+    kept = term[block_rows(2 * high + low)].astype(F32) + near_in[high].astype(F32)
+    mixer_ref[...] = (kept + far_in[...].astype(F32)).astype(BF16)
+    lax.fori_loop(count // 2, count - 1, gather_block, 0)
+    expert_ref[...] = combined[...].astype(BF16)
+
+    def settle(k, nothing):
+        distance = far_first(k)
+        back(distance, lax.rem(here + distance, count)).wait_send()
+        return nothing
+
+    lax.fori_loop(0, count - 1, settle, 0)
+    for copy in [forward] + nears + [cross_send]:
+        copy.wait_send()
+
+
+def return_rows(mixed, out_weight, total, hidden, far_down, targets, route_weight, capacity):
+    count = lax.axis_size("ep")
+    rows, width = total.shape
+    tokens = targets.shape[0]
+    operands = (mixed, out_weight, total, hidden, far_down, targets, route_weight)
+    return pl.pallas_call(
+        functools.partial(return_kernel, capacity),
+        in_specs=[pl.BlockSpec(memory_space=pltpu.VMEM)] * len(operands),
+        out_specs=[pl.BlockSpec(memory_space=pltpu.VMEM)] * 2,
+        out_shape=[jax.ShapeDtypeStruct((tokens, width), BF16)] * 2,
+        scratch_shapes=[
+            pltpu.VMEM(far_down.shape, BF16),
+            pltpu.VMEM((rows, width), BF16),
+            pltpu.VMEM((rows, width), BF16),
+            pltpu.VMEM((mixed.shape[0], width), BF16),
+            pltpu.VMEM((2, tokens, width), BF16),
+            pltpu.VMEM((tokens, width), BF16),
+            pltpu.VMEM((tokens, width), BF16),
+            pltpu.VMEM((tokens, width), F32),
+            pltpu.SemaphoreType.DMA((count - 1,)),
+            pltpu.SemaphoreType.DMA((count - 1,)),
+            pltpu.SemaphoreType.DMA((4,)),
+            pltpu.SemaphoreType.DMA((4,)),
+        ],
+        compiler_params=pltpu.CompilerParams(
+            vmem_limit_bytes=40 * 2**20, collective_id=1, has_side_effects=True
+        ),
+        cost_estimate=pl.CostEstimate(
+            flops=6 * 10**9, bytes_accessed=12 * 2**20, transcendentals=0
+        ),
+        name="return_rows",
+    )(*operands)
+
+
 def swap(x, distance):
     count = lax.axis_size("tp")
     return lax.ppermute(x, "tp", [(i, i ^ distance) for i in range(count)])
-
-
-def spread_sum(term):
-    rows, width = term.shape
-    count = lax.axis_size("tp")
-    place = lax.axis_index("tp")
-    block = rows // count
-    parts = term.reshape(count // 2, 2, block, width)
-    low = place % 2
-    kept = lax.dynamic_index_in_dim(parts, low, 1, keepdims=False)
-    sent = lax.dynamic_index_in_dim(parts, 1 - low, 1, keepdims=False)
-    pair = (kept.astype(F32) + swap(sent, 1).astype(F32)).astype(BF16)
-    high = place // 2
-    kept = lax.dynamic_index_in_dim(pair, high, 0, keepdims=False)
-    sent = lax.dynamic_index_in_dim(pair, 1 - high, 0, keepdims=False)
-    return (kept.astype(F32) + swap(sent, 2).astype(F32)).astype(BF16)
 
 
 def slot_targets(block_routes, capacity):
@@ -503,38 +729,14 @@
         decay_shift,
         head_size,
     )
+    cross = tuple(swap(array, 1) for array in far[:2])
     mixed = mixer_finish(summary, reader, local_read, channel_gain, head_size)
-    far_gate, far_up, arrived, mixed = lax.optimization_barrier(
-        (far[0], far[1], arrived, mixed)
+    total, hidden = expert_part(arrived, (own, near), (far[:2], cross))
+    return tuple(
+        return_rows(
+            mixed, out_weight, total, hidden, far[2], own_targets, route_weight, capacity
+        )
     )
-    cross_gate, cross_up = swap(far_gate, 1), swap(far_up, 1)
-    mixer_term = jnp.dot(mixed, out_weight, preferred_element_type=F32)
-    first = expert_part(arrived, (own, near), None, F32)
-    far_down, first, mixer_term = lax.optimization_barrier((far[2], first, mixer_term))
-    cross_down = swap(far_down, 1)
-    total = expert_part(
-        arrived,
-        ((far_gate, far_up, far_down), (cross_gate, cross_up, cross_down)),
-        first,
-        BF16,
-    )
-    total, mixer_term = lax.optimization_barrier((total, mixer_term))
-    mixer_out = spread_sum(mixer_term.astype(BF16))
-    returned = lax.all_to_all(
-        total.reshape(ep_count, capacity, model_width),
-        "ep",
-        split_axis=0,
-        concat_axis=0,
-        tiled=True,
-    )
-    flat_rows = returned.reshape(experts * capacity, model_width)
-    places = jnp.arange(experts * capacity, dtype=jnp.int32)
-    combined = jnp.zeros((token_rows, model_width), F32)
-    for picked in range(top_count):
-        table = (own_targets[:, picked : picked + 1] == places[None, :]).astype(BF16)
-        chosen = jnp.dot(table, flat_rows, preferred_element_type=F32)
-        combined = combined + chosen * route_weight[:, picked : picked + 1]
-    return (mixer_out, combined.astype(BF16))
 
 
 def solution(mesh):

time: 173 us -> 186 us (1.075)
  the two profiles are of different devices: /device:TPU:0 before, /device:TPU:17 now
where the time goes in v2:
time: 186 us
  Pallas kernels  125 us (67%)
  waiting for transfers between devices  27.9 us (15%)
  starting transfers between devices  15 us (8%)
  local copies, waits for them, and re-layouts  11.9 us (6%)
  matrix products  3.19 us (2%)
  other arithmetic  2.2 us (1%)
    pallas_call x1, Pallas kernels, return_rows(): pl.pallas_call(functools.partial(return_kernel, capacity), in_specs=[pl.B...  64.1 us
    pallas_call x1, Pallas kernels, mixer_local(): pl.pallas_call(functools.partial(local_kernel, head_size), grid=(pairs,),...  31 us
    ppermute x8, waiting for transfers between devices, swap(): return lax.ppermute(x, 'tp', [(i, i ^ distance) for i in range(count)])  27.9 us
    pallas_call x1, Pallas kernels, mixer_finish(): pl.pallas_call(functools.partial(finish_kernel, head_size), in_specs=[pl....  20.5 us
    unnamed x37, local copies, waits for them, and re-layouts  11.5 us
    ppermute x8, starting transfers between devices, swap(): return lax.ppermute(x, 'tp', [(i, i ^ distance) for i in range(count)])  9.33 us
    pallas_call x1, Pallas kernels, expert_part(): pl.pallas_call(part_kernel, in_specs=[pl.BlockSpec(memory_space=pltpu.VME...  9.27 us
    all_to_all x1, starting transfers between devices, one_device(): lax.all_to_all(outgoing.reshape(experts, capacity, model_width), 'ep', sp...  5.71 us
  transfers between devices with their start and end apart: 9, of which 2 were waited for; matrix products, arithmetic and copies ran while one was open for 4% of the time, Pallas kernels for 33%

profile of v2, /device:TPU:17, one launch (start us, length us, event | category | flops | bytes accessed | tf_op | source)
XLA Modules:
  0.0 185.9 jit_solution(9697034770359086999)
XLA Ops:
  0.6 1.3 collective-permute-start.3
  1.9 0.2 collective-permute-start.4
  2.2 0.8 copy.34
  2.9 0.7 broadcast_multiply_fusion
  3.6 0.1 eq.29
  3.8 0.2 convert_reduce_fusion.1
  4.0 0.1 reshape.33
  4.1 0.1 copy.35
  4.2 0.1 copy.36
  4.3 0.1 convert_reduce_fusion
  4.4 1.2 fusion
  5.6 3.2 %convolution_convert_fusion = bf16[512,2048]{1,0:T(8,128)(2,1)} fusion(bf16[128,2048]{1,0:T(8,128)(2,1)} %param.25, f32[2048]{0:T(1024)} %param.26, f32[128]{0:T(128)S(1)} %add_rsqrt_fusion, s32[512,128]{1,0:T(8,128)S(1)} %convert_reduce_fusion), kind=kOutput, calls=%fused_computation | convolution fusion | flops 270598144 | bytes 2892288 | tf_op jit(solution)/shard_map/dot_general | solution.py:709
  8.8 0.0 copy-start.1
  8.8 0.0 copy-start.14
  8.8 0.0 copy-start.4
  8.8 5.7 %all-to-all-start = ((bf16[8,64,2048]{2,1,0:T(8,128)(2,1)}), bf16[8,64,2048]{2,1,0:T(8,128)(2,1)S(1)}, u32[]{:S(2)}, u32[]{:S(2)}) async-start(bf16[8,64,2048]{2,1,0:T(8,128)(2,1)} %bitcast.19), calls=%async_computation | async-start | bytes 4194304 | tf_op jit(solution)/shard_map/all_to_all | solution.py:714
  14.5 0.0 copy-done.1
  14.5 1.8 collective-permute-start
  16.3 0.1 collective-permute-start.1
  16.4 0.4 collective-permute-start.2
  16.8 0.0 copy-done.14
  16.8 0.1 copy.33.shift_ref
  17.0 8.1 %collective-permute-done.3.refs_6_ = bf16[2048,256]{1,0:T(8,128)(2,1)} collective-permute-done((bf16[2048,256]{1,0:T(8,128)(2,1)}, bf16[2048,256]{1,0:T(8,128)(2,1)}, u32[]{:S(2)}, u32[]{:S(2)}) %collective-permute-start.3) | collective-permute-done | bytes 1048608 | tf_op jit(solution)/shard_map/ppermute | solution.py:652
  25.1 2.7 %collective-permute-start.5 = (bf16[2048,256]{1,0:T(8,128)(2,1)}, bf16[2048,256]{1,0:T(8,128)(2,1)}, u32[]{:S(2)}, u32[]{:S(2)}) collective-permute-start(bf16[2048,256]{1,0:T(8,128)(2,1)} %collective-permute-done.3.refs_6_), channel_id=1, source_target_pairs={{0,1},{1,0},{2,3},{3,2},{4,5},{5,4},{6,7},{7,6},{8,9},{9,8},{10,11... | collective-permute-start | bytes 3145736 | tf_op jit(solution)/shard_map/ppermute | solution.py:652
  27.7 19.8 %collective-permute-done.4.refs_7_ = bf16[2048,256]{1,0:T(8,128)(2,1)} collective-permute-done((bf16[2048,256]{1,0:T(8,128)(2,1)}, bf16[2048,256]{1,0:T(8,128)(2,1)}, u32[]{:S(2)}, u32[]{:S(2)}) %collective-permute-start.4) | collective-permute-done | bytes 1048608 | tf_op jit(solution)/shard_map/ppermute | solution.py:652
  47.5 1.5 collective-permute-start.6
  49.1 0.0 copy-done.4
  49.1 0.0 copy-start.15
  49.1 0.0 copy-start.5
  49.1 31.0 %mixer_local.1 = (bf16[512,512]{1,0:T(8,128)(2,1)S(1)}, f32[512,512]{1,0:T(8,128)S(1)}, bf16[2,256,128]{2,1,0:T(8,128)(2,1)S(1)}) custom-call(bf16[512,512]{1,0:T(8,128)(2,1)} %r_ref.1, bf16[512,512]{1,0:T(8,128)(2,1)} %k_ref.1, bf16[512,512]{1,0:T(8,128)(2,1)} %v_ref.1, bf16[512,512]{1,0:T(8,128)(2,1)} %d_ref.1, bf16[512,512]{1,0:T(8,128)(2,1)} %l_ref.1, ...), custom_call_target="tpu_custom_call" | custom-call | flops 20000000000 | bytes 6291456 | tf_op jit(solution)/shard_map/mixer_local/pallas_call | solution.py:237
  80.0 0.0 copy-start.8
  80.1 1.0 copy-done.8
  81.0 0.0 copy-start.10
  81.0 0.8 copy-done.10
  81.8 0.0 copy-start.12
  81.8 0.7 copy-done.12
  82.5 0.0 copy-done.15
  82.5 0.1 copy.37.weight_ref
  82.6 0.0 collective-permute-done.refs_3_
  82.6 1.3 collective-permute-start.7
  83.9 0.0 copy-done.5
  83.9 0.0 copy-start.9
  83.9 1.2 copy-done.9
  85.1 0.0 copy-start.11
  85.1 1.0 copy-done.11
  86.2 0.9 copy-done.13
  87.1 20.5 %mixer_finish.1.mixed_ref = bf16[512,512]{1,0:T(8,128)(2,1)S(1)} custom-call(bf16[2,256,128]{2,1,0:T(8,128)(2,1)S(1)} %copy-done.13, bf16[512,512]{1,0:T(8,128)(2,1)S(1)} %copy-done.11, f32[512,512]{1,0:T(8,128)S(1)} %copy-done.9, f32[1,512]{1,0:T(1,128)S(1)} %bitcast.18), custom_call_target="tpu_custom_call" | custom-call | flops 10000000000 | bytes 4194304 | tf_op jit(solution)/shard_map/mixer_finish/pallas_call | solution.py:377
  107.6 0.0 copy-start.6
  107.6 0.8 copy-done.6
  108.3 0.0 collective-permute-done.1.refs_4_
  108.4 0.0 collective-permute-done.2.refs_5_
  108.4 0.0 collective-permute-done.5.refs_8_
  108.4 0.0 collective-permute-done.6.refs_9_
  108.4 0.0 all-to-all-done
  108.4 0.0 copy-start.2
  108.4 1.2 copy-done.2
  109.6 1.2 copy-done.3
  110.8 9.3 %expert_part.1 = (f32[512,2048]{1,0:T(8,128)S(1)}, bf16[512,512]{1,0:T(8,128)(2,1)S(1)}) custom-call(bf16[512,2048]{1,0:T(8,128)(2,1)S(1)} %bitcast.7, bf16[2048,256]{1,0:T(8,128)(2,1)S(1)} %bitcast.10, bf16[2048,256]{1,0:T(8,128)(2,1)S(1)} %bitcast.13, bf16[256,2048]{1,0:T(8,128)(2,1)S(1)} %bitcast.16, bf16[2048,256]{1,0:T(8,128)(2,1)} %collective-permute-done.refs_3_, ...), custom_call_target="tpu_custom_call" | custom-call | flops 5368709120 | bytes 12582912 | tf_op jit(solution)/shard_map/expert_part/pallas_call | solution.py:433
  120.1 0.0 collective-permute-done.7.far_ref
  120.1 0.0 copy-done
  120.1 0.0 copy-done.7
  120.2 64.1 %return_rows.1 = (bf16[128,2048]{1,0:T(8,128)(2,1)S(1)}, bf16[128,2048]{1,0:T(8,128)(2,1)S(1)}) custom-call(bf16[512,512]{1,0:T(8,128)(2,1)S(1)} %copy-done.7, bf16[512,2048]{1,0:T(8,128)(2,1)S(1)} %copy-done, f32[512,2048]{1,0:T(8,128)S(1)} %get-tuple-element.10.total_ref, bf16[512,512]{1,0:T(8,128)(2,1)S(1)} %get-tuple-element.11.hidden_ref, ...), custom_call_target="tpu_custom_call" | custom-call | flops 6000000000 | bytes 12582912 | tf_op jit(solution)/shard_map/return_rows/pallas_call | solution.py:621
  184.3 0.8 copy.40
  185.1 0.8 copy.41
  (6 shorter events, 0.0 us)
Async XLA Ops:
  0.6 24.4 %collective-permute-start.3 = (bf16[2048,256]{1,0:T(8,128)(2,1)}, bf16[2048,256]{1,0:T(8,128)(2,1)}, u32[]{:S(2)}, u32[]{:S(2)}) collective-permute-start(bf16[2048,256]{1,0:T(8,128)(2,1)} %bitcast.8), channel_id=1, source_target_pairs={{0,2},{1,3},{2,0},{3,1},{4,6},{5,7},{6,4},{7,5},{8,10},{9,11},{10,... | collective-permute-start | bytes 3145736 | tf_op jit(solution)/shard_map/ppermute | solution.py:652
  1.9 45.6 %collective-permute-start.4 = (bf16[2048,256]{1,0:T(8,128)(2,1)}, bf16[2048,256]{1,0:T(8,128)(2,1)}, u32[]{:S(2)}, u32[]{:S(2)}) collective-permute-start(bf16[2048,256]{1,0:T(8,128)(2,1)} %bitcast.11), channel_id=1, source_target_pairs={{0,2},{1,3},{2,0},{3,1},{4,6},{5,7},{6,4},{7,5},{8,10},{9,11},{10,... | collective-permute-start | bytes 3145736 | tf_op jit(solution)/shard_map/ppermute | solution.py:652
  8.8 5.7 %copy-start.1 = (bf16[1,2048,256]{2,1,0:T(8,128)(2,1)S(1)}, bf16[1,2048,256]{2,1,0:T(8,128)(2,1)}, u32[]{:S(2)}) copy-start(bf16[1,2048,256]{2,1,0:T(8,128)(2,1)} %param.29) | copy-start | bytes 3145732
  8.8 8.0 %copy-start.14 = (f32[512,8]{0,1:T(8,128)S(1)}, f32[512,8]{0,1:T(8,128)}, u32[]{:S(2)}) copy-start(f32[512,8]{0,1:T(8,128)} %param.22) | copy-start | bytes 49156
  8.8 40.3 %copy-start.4 = (f32[512]{0:T(512)S(1)}, f32[512]{0:T(512)}, u32[]{:S(2)}) copy-start(f32[512]{0:T(512)} %param.21) | copy-start | bytes 6148
  8.8 99.6 %all-to-all-start = ((bf16[8,64,2048]{2,1,0:T(8,128)(2,1)}), bf16[8,64,2048]{2,1,0:T(8,128)(2,1)S(1)}, u32[]{:S(2)}, u32[]{:S(2)}) async-start(bf16[8,64,2048]{2,1,0:T(8,128)(2,1)} %bitcast.19), calls=%async_computation | async-start | bytes 4194304 | tf_op jit(solution)/shard_map/all_to_all | solution.py:714
  14.5 68.1 %collective-permute-start = (bf16[2048,256]{1,0:T(8,128)(2,1)S(1)}, bf16[2048,256]{1,0:T(8,128)(2,1)}, u32[]{:S(2)}, u32[]{:S(2)}) collective-permute-start(bf16[2048,256]{1,0:T(8,128)(2,1)S(1)} %bitcast.9), channel_id=1, source_target_pairs={{0,1},{1,0},{2,3},{3,2},{4,5},{5,4},{6,7},{7,6},{8,9},{9,8},{10,11... | collective-permute-start | bytes 3145736 | tf_op jit(solution)/shard_map/ppermute | solution.py:652
  16.3 92.0 %collective-permute-start.1 = (bf16[2048,256]{1,0:T(8,128)(2,1)}, bf16[2048,256]{1,0:T(8,128)(2,1)}, u32[]{:S(2)}, u32[]{:S(2)}) collective-permute-start(bf16[2048,256]{1,0:T(8,128)(2,1)} %bitcast.12), channel_id=1, source_target_pairs={{0,1},{1,0},{2,3},{3,2},{4,5},{5,4},{6,7},{7,6},{8,9},{9,8},{10,11... | collective-permute-start | bytes 3145736 | tf_op jit(solution)/shard_map/ppermute | solution.py:652
  16.4 92.0 %collective-permute-start.2 = (bf16[256,2048]{1,0:T(8,128)(2,1)}, bf16[256,2048]{1,0:T(8,128)(2,1)}, u32[]{:S(2)}, u32[]{:S(2)}) collective-permute-start(bf16[256,2048]{1,0:T(8,128)(2,1)} %bitcast.14), channel_id=1, source_target_pairs={{0,1},{1,0},{2,3},{3,2},{4,5},{5,4},{6,7},{7,6},{8,9},{9,8},{10,11... | collective-permute-start | bytes 3145736 | tf_op jit(solution)/shard_map/ppermute | solution.py:652
  25.1 83.3 %collective-permute-start.5 = (bf16[2048,256]{1,0:T(8,128)(2,1)}, bf16[2048,256]{1,0:T(8,128)(2,1)}, u32[]{:S(2)}, u32[]{:S(2)}) collective-permute-start(bf16[2048,256]{1,0:T(8,128)(2,1)} %collective-permute-done.3.refs_6_), channel_id=1, source_target_pairs={{0,1},{1,0},{2,3},{3,2},{4,5},{5,4},{6,7},{7,6},{8,9},{9,8},{10,11... | collective-permute-start | bytes 3145736 | tf_op jit(solution)/shard_map/ppermute | solution.py:652
  47.5 60.8 %collective-permute-start.6 = (bf16[2048,256]{1,0:T(8,128)(2,1)}, bf16[2048,256]{1,0:T(8,128)(2,1)}, u32[]{:S(2)}, u32[]{:S(2)}) collective-permute-start(bf16[2048,256]{1,0:T(8,128)(2,1)} %collective-permute-done.4.refs_7_), channel_id=1, source_target_pairs={{0,1},{1,0},{2,3},{3,2},{4,5},{5,4},{6,7},{7,6},{8,9},{9,8},{10,11... | collective-permute-start | bytes 3145736 | tf_op jit(solution)/shard_map/ppermute | solution.py:652
  49.1 33.4 %copy-start.15 = (f32[128,2]{0,1:T(2,128)S(1)}, f32[128,2]{0,1:T(2,128)}, u32[]{:S(2)}) copy-start(f32[128,2]{0,1:T(2,128)} %param.28) | copy-start | bytes 3076
  49.1 34.8 %copy-start.5 = (f32[512]{0:T(512)S(1)}, f32[512]{0:T(512)}, u32[]{:S(2)}) copy-start(f32[512]{0:T(512)} %param.23) | copy-start | bytes 6148
  80.0 1.0 copy-start.8
  81.0 0.8 copy-start.10
  81.8 0.7 copy-start.12
  82.6 37.5 %collective-permute-start.7 = (bf16[256,2048]{1,0:T(8,128)(2,1)}, bf16[256,2048]{1,0:T(8,128)(2,1)}, u32[]{:S(2)}, u32[]{:S(2)}) collective-permute-start(bf16[256,2048]{1,0:T(8,128)(2,1)} %bitcast.15), channel_id=1, source_target_pairs={{0,2},{1,3},{2,0},{3,1},{4,6},{5,7},{6,4},{7,5},{8,10},{9,11},{10,... | collective-permute-start | bytes 3145736 | tf_op jit(solution)/shard_map/ppermute | solution.py:652
  83.9 1.2 copy-start.9
  85.1 1.0 copy-start.11
  86.2 0.9 copy-start.13
  107.6 0.8 copy-start.6
  108.4 1.2 copy-start.2
  109.6 1.2 copy-start.3
  110.8 9.3 %copy-start = (bf16[512,2048]{1,0:T(8,128)(2,1)S(1)}, bf16[512,2048]{1,0:T(8,128)(2,1)}, u32[]{:S(2)}) copy-start(bf16[512,2048]{1,0:T(8,128)(2,1)} %project_ref.1) | copy-start | bytes 6291460
  110.8 9.3 %copy-start.7 = (bf16[512,512]{1,0:T(8,128)(2,1)S(1)}, bf16[512,512]{1,0:T(8,128)(2,1)}, u32[]{:S(2)}) copy-start(bf16[512,512]{1,0:T(8,128)(2,1)} %copy-done.6) | copy-start | bytes 1572868

commit v3 on v2

--- a/solution.py
+++ b/solution.py
@@ -230,10 +230,7 @@
     half = LANES // 2
     tile = pl.BlockSpec((rows, LANES), lambda p: (0, p))
     small = pl.BlockSpec((2, half, LANES), lambda p: (0, p, 0))
-    streams = [
-        pltpu.with_memory_space_constraint(array, pltpu.HBM)
-        for array in (receptance, keys, values, decay, learn)
-    ]
+    streams = [in_hbm(array) for array in (receptance, keys, values, decay, learn)]
     return pl.pallas_call(
         functools.partial(local_kernel, head_size),
         grid=(pairs,),
@@ -259,41 +256,24 @@
     )(*streams, base.reshape(pairs, 1, LANES), shift)
 
 
-def finish_kernel(
-    head_size,
-    summary_ref,
-    reader_ref,
-    local_ref,
-    gain_ref,
-    out_ref,
-    before,
-    sending,
-    landed,
-    send_sems,
-    recv_sems,
-):
-    here = lax.axis_index("ep")
-    count = lax.axis_size("ep")
-    rounds = landed.shape[0]
-    half = LANES // 2
-    _, channels = reader_ref.shape
-    pairs = channels // LANES
-    matched = same_head(head_size)
-    block = matched.astype(BF16)
-    diagonal = grid_index((LANES, LANES), 0) == grid_index((LANES, LANES), 1)
-
-    def transfer(level, distance, target):
-        return pltpu.make_async_remote_copy(
-            src_ref=sending,
-            dst_ref=landed.at[level],
-            send_sem=send_sems.at[distance - 1],
-            recv_sem=recv_sems.at[level],
-            device_id={"ep": target},
-            device_id_type=pl.DeviceIdType.MESH,
-        )
-
-    barrier = pltpu.get_barrier_semaphore()
-
+def gated(x, gate, up):
+    gates = mm(x, gate)
+    uppers = mm(x, up)
+    return (gates / (1.0 + jnp.exp(-gates)) * uppers).astype(BF16)
+
+
+def send_to(src, dst, send_sem, recv_sem, target):
+    return pltpu.make_async_remote_copy(
+        src_ref=src,
+        dst_ref=dst,
+        send_sem=send_sem,
+        recv_sem=recv_sem,
+        device_id=target,
+        device_id_type=pl.DeviceIdType.MESH,
+    )
+
+
+def greet_all(barrier, here, count, others):
     def greet(distance, nothing):
         pl.semaphore_signal(
             barrier,
@@ -304,6 +284,80 @@
         return nothing
 
     lax.fori_loop(1, count, greet, 0)
+    for target in others:
+        pl.semaphore_signal(
+            barrier, inc=1, device_id={"tp": target}, device_id_type=pl.DeviceIdType.MESH
+        )
+
+
+def part_kernel(
+    head_size,
+    x_ref,
+    summary_ref,
+    own_gate,
+    own_up,
+    own_down,
+    near_gate,
+    near_up,
+    near_down,
+    far_gate,
+    far_up,
+    total_ref,
+    hidden_ref,
+    entering_ref,
+    held,
+    held_down,
+    cross,
+    before,
+    sending,
+    landed,
+    load_sems,
+    send_sems,
+    recv_sems,
+    side_send,
+    side_recv,
+):
+    here = lax.axis_index("ep")
+    count = lax.axis_size("ep")
+    place = lax.axis_index("tp")
+    beside = place + 1 - 2 * lax.rem(place, 2)
+    rounds = landed.shape[0]
+    half = LANES // 2
+    pairs = before.shape[1]
+    rows = x_ref.shape[0]
+    units = own_gate.shape[1]
+    piece = min(rows, 256)
+    matched = same_head(head_size)
+    diagonal = grid_index((LANES, LANES), 0) == grid_index((LANES, LANES), 1)
+
+    loads = [
+        pltpu.make_async_copy(src, dst, load_sems.at[i])
+        for i, (src, dst) in enumerate(
+            [
+                (own_gate, held.at[0]),
+                (own_up, held.at[1]),
+                (own_down, held_down.at[0]),
+                (near_gate, held.at[2]),
+                (near_up, held.at[3]),
+                (near_down, held_down.at[1]),
+                (far_gate, held.at[4]),
+                (far_up, held.at[5]),
+            ]
+        )
+    ]
+    for load in loads:
+        load.start()
+    barrier = pltpu.get_barrier_semaphore()
+    greet_all(barrier, here, count, (beside,))
+
+    def transfer(level, distance, target):
+        return send_to(
+            sending,
+            landed.at[level],
+            send_sems.at[distance - 1],
+            recv_sems.at[level],
+            {"ep": target},
+        )
 
     def wide(part):
         part = part.astype(F32)
@@ -315,13 +369,19 @@
     for p in range(pairs):
         before[0, p] = jnp.where(diagonal, 1.0, 0.0)
         before[1, p] = jnp.zeros((LANES, LANES), F32)
-    pl.semaphore_wait(barrier, count - 1)
-
-    for level in range(rounds):
+    pl.semaphore_wait(barrier, count)
+    forwards = [
+        send_to(src, cross.at[i], side_send.at[i], side_recv.at[i], {"tp": beside})
+        for i, src in enumerate((far_gate, far_up))
+    ]
+    for forward in forwards:
+        forward.start()
+
+    def send_round(level):
         reach = 2**level
 
         @pl.when(lax.rem(here, 2 * reach) == reach - 1)
-        def _(level=level, reach=reach):
+        def _():
             for p in range(pairs):
                 both = jnp.concatenate([before[0, p], before[1, p]], axis=0)
                 high, low = split_two(both)
@@ -337,8 +397,11 @@
 
             lax.fori_loop(1, reach + 1, launch, 0)
 
+    def take_round(level):
+        reach = 2**level
+
         @pl.when(lax.rem(here // reach, 2) == 1)
-        def _(level=level, reach=reach):
+        def _():
             transfer(level, 1, here).wait_recv()
             for p in range(pairs):
                 both = jnp.concatenate(
@@ -349,13 +412,44 @@
                 before[0, p] = moved[:LANES]
                 before[1, p] = moved[LANES:] + before[1, p]
 
+    def over_rows(body):
+        def step(i, nothing):
+            body(pl.ds(pl.multiple_of(i * piece, piece), piece))
+            return nothing
+
+        lax.fori_loop(0, rows // piece, step, 0)
+
+    def first_part(at):
+        hidden = gated(x_ref[at], held[0], held[1])
+        total_ref[at] = mm(hidden, held_down[0])
+
+    def second_part(at):
+        hidden = gated(x_ref[at], held[2], held[3])
+        total_ref[at] += mm(hidden, held_down[1])
+
+    def third_part(at):
+        hidden_ref[at, :units] = gated(x_ref[at], held[4], held[5])
+
+    def fourth_part(at):
+        hidden_ref[at, units:] = gated(x_ref[at], cross[0], cross[1])
+
+    send_round(0)
+    bodies = (first_part, second_part, third_part, fourth_part)
+    needs = (loads[:3], loads[3:6], loads[6:], ())
+    for turn in range(max(len(bodies), rounds)):
+        if turn < len(bodies):
+            for load in needs[turn]:
+                load.wait()
+            if turn == len(bodies) - 1:
+                for forward in forwards:
+                    forward.wait_recv()
+            over_rows(bodies[turn])
+        if turn < rounds:
+            take_round(turn)
+            if turn + 1 < rounds:
+                send_round(turn + 1)
     for p in range(pairs):
-        lanes = slice(p * LANES, (p + 1) * LANES)
-        read = mm_nt(reader_ref[:, lanes], before[1, p]) + local_ref[:, lanes]
-        centred = read - head_sums(read, block) * (1.0 / head_size)
-        variance = head_sums(centred * centred, block) * (1.0 / head_size)
-        scaled = centred * lax.rsqrt(variance + GROUP_EPS) * gain_ref[:, lanes]
-        out_ref[:, lanes] = scaled.astype(BF16)
+        entering_ref[p * LANES : (p + 1) * LANES] = before[1, p]
 
     for level in range(rounds):
         reach = 2**level
@@ -368,90 +462,64 @@
 
             lax.fori_loop(1, reach + 1, settle, 0)
 
-
-def mixer_finish(summary, reader, local_read, gain, head_size):
-    rows, channels = reader.shape
-    pairs = channels // LANES
+    for forward in forwards:
+        forward.wait_send()
+
+
+def in_hbm(array):
+    return pltpu.with_memory_space_constraint(array, pltpu.HBM)
+
+
+def expert_part(incoming, summary, own, near, far, head_size):
+    rows, width = incoming.shape
+    units = own[0].shape[1]
+    pairs = summary.shape[1] * 2 // LANES
     count = lax.axis_size("ep")
     rounds = (count - 1).bit_length()
+    weights = [in_hbm(array) for array in own + near + far]
     return pl.pallas_call(
-        functools.partial(finish_kernel, head_size),
-        in_specs=[pl.BlockSpec(memory_space=pltpu.VMEM)] * 4,
-        out_specs=pl.BlockSpec(memory_space=pltpu.VMEM),
-        out_shape=jax.ShapeDtypeStruct((rows, channels), BF16),
+        functools.partial(part_kernel, head_size),
+        in_specs=[pl.BlockSpec(memory_space=pltpu.VMEM)] * 2
+        + [pl.BlockSpec(memory_space=pl.ANY)] * len(weights),
+        out_specs=[pl.BlockSpec(memory_space=pltpu.VMEM)] * 3,
+        out_shape=[
+            jax.ShapeDtypeStruct((rows, width), F32),
+            jax.ShapeDtypeStruct((rows, 2 * units), BF16),
+            jax.ShapeDtypeStruct((pairs * LANES, LANES), F32),
+        ],
         scratch_shapes=[
+            pltpu.VMEM((6, width, units), BF16),
+            pltpu.VMEM((2, units, width), BF16),
+            pltpu.VMEM((2, width, units), BF16),
             pltpu.VMEM((2, pairs, LANES, LANES), F32),
             pltpu.VMEM(summary.shape, BF16),
             pltpu.VMEM((rounds,) + summary.shape, BF16),
+            pltpu.SemaphoreType.DMA((8,)),
             pltpu.SemaphoreType.DMA((count // 2,)),
             pltpu.SemaphoreType.DMA((rounds,)),
+            pltpu.SemaphoreType.DMA((2,)),
+            pltpu.SemaphoreType.DMA((2,)),
         ],
         compiler_params=pltpu.CompilerParams(
             vmem_limit_bytes=32 * 2**20, collective_id=0, has_side_effects=True
         ),
-        cost_estimate=pl.CostEstimate(
-            flops=10 * 10**9, bytes_accessed=4 * 2**20, transcendentals=10**5
-        ),
-        name="mixer_finish",
-    )(summary, reader, local_read, gain.reshape(1, channels))
-
-
-def gated(x, gate, up):
-    gates = mm(x, gate)
-    uppers = mm(x, up)
-    return (gates / (1.0 + jnp.exp(-gates)) * uppers).astype(BF16)
-
-
-def part_kernel(x_ref, *refs):
-    weights, (total_ref, hidden_ref) = refs[:-2], refs[-2:]
-    rows = x_ref.shape[0]
-    units = weights[0].shape[1]
-    piece = min(rows, 256)
-
-    def block(step, nothing):
-        here = pl.ds(pl.multiple_of(step * piece, piece), piece)
-        x = x_ref[here]
-        total = None
-        for s in range(2):
-            gate, up, down = weights[3 * s : 3 * s + 3]
-            term = mm(gated(x, gate[...], up[...]), down[...])
-            total = term if total is None else total + term
-        total_ref[here] = total
-        for s in range(2):
-            gate, up = weights[6 + 2 * s : 8 + 2 * s]
-            hidden_ref[here, s * units : (s + 1) * units] = gated(x, gate[...], up[...])
-        return nothing
-
-    lax.fori_loop(0, rows // piece, block, 0)
-
-
-def expert_part(incoming, full, partial):
-    rows, width = incoming.shape
-    units = full[0][0].shape[1]
-    flat = [array for shard in full + partial for array in shard]
-    operands = [incoming] + flat
-    return pl.pallas_call(
-        part_kernel,
-        in_specs=[pl.BlockSpec(memory_space=pltpu.VMEM)] * len(operands),
-        out_specs=[pl.BlockSpec(memory_space=pltpu.VMEM)] * 2,
-        out_shape=[
-            jax.ShapeDtypeStruct((rows, width), F32),
-            jax.ShapeDtypeStruct((rows, 2 * units), BF16),
-        ],
-        compiler_params=pltpu.CompilerParams(vmem_limit_bytes=32 * 2**20),
         cost_estimate=pl.CostEstimate(
             flops=20 * rows * width * units,
             bytes_accessed=2 * (rows * width + 10 * units * width),
             transcendentals=4 * rows * units,
         ),
         name="expert_part",
-    )(*operands)
+    )(incoming, summary, *weights)
 
 
 def return_kernel(
     capacity,
-    mixed_ref,
+    head_size,
+    reader_ref,
+    local_ref,
     project_ref,
+    gain_ref,
+    entering_ref,
     total_ref,
     hidden_ref,
     far_ref,
@@ -459,6 +527,10 @@
     weight_ref,
     mixer_ref,
     expert_ref,
+    reader,
+    local,
+    project,
+    mixed,
     cross,
     staged,
     landed,
@@ -467,6 +539,7 @@
     pair_out,
     far_in,
     combined,
+    load_sems,
     send_sems,
     recv_sems,
     side_send,
@@ -480,53 +553,38 @@
     across = place + 2 - 4 * high
     units = far_ref.shape[0]
     tokens = expert_ref.shape[0]
+    pairs = reader.shape[1] // LANES
+    block = same_head(head_size).astype(BF16)
 
     def side(src, dst, index, target):
-        return pltpu.make_async_remote_copy(
-            src_ref=src,
-            dst_ref=dst,
-            send_sem=side_send.at[index],
-            recv_sem=side_recv.at[index],
-            device_id={"tp": target},
-            device_id_type=pl.DeviceIdType.MESH,
-        )
+        return send_to(src, dst, side_send.at[index], side_recv.at[index], {"tp": target})
 
     def rows_of(member):
         return pl.ds(pl.multiple_of(member * capacity, capacity), capacity)
 
     def back(distance, member):
-        return pltpu.make_async_remote_copy(
-            src_ref=staged.at[rows_of(member)],
-            dst_ref=landed.at[rows_of(here)],
-            send_sem=send_sems.at[distance - 1],
-            recv_sem=recv_sems.at[distance - 1],
-            device_id={"ep": member},
-            device_id_type=pl.DeviceIdType.MESH,
+        return send_to(
+            staged.at[rows_of(member)],
+            landed.at[rows_of(here)],
+            send_sems.at[distance - 1],
+            recv_sems.at[distance - 1],
+            {"ep": member},
         )
 
     barrier = pltpu.get_barrier_semaphore()
-
-    def greet(distance, nothing):
-        pl.semaphore_signal(
-            barrier,
-            inc=1,
-            device_id={"ep": lax.rem(here + distance, count)},
-            device_id_type=pl.DeviceIdType.MESH,
-        )
-        return nothing
-
-    lax.fori_loop(1, count, greet, 0)
-    for target in (beside, across):
-        pl.semaphore_signal(
-            barrier,
-            inc=1,
-            device_id={"tp": target},
-            device_id_type=pl.DeviceIdType.MESH,
-        )
+    greet_all(barrier, here, count, (beside, across))
     pl.semaphore_wait(barrier, count + 1)
 
     forward = side(far_ref, cross, 0, beside)
     forward.start()
+    loads = [
+        pltpu.make_async_copy(src, dst, load_sems.at[i])
+        for i, (src, dst) in enumerate(
+            [(reader_ref, reader), (local_ref, local), (project_ref, project)]
+        )
+    ]
+    for load in loads:
+        load.start()
     forward.wait_recv()
 
     def finished(member):
@@ -548,15 +606,26 @@
     lax.fori_loop(0, count - 1, send_block, 0)
     landed[rows_of(here)] = finished(here)
 
-    def project(b, nothing):
-        rows = pl.ds(pl.multiple_of(b * tokens, tokens), tokens)
-        term[rows] = mm(mixed_ref[rows], project_ref[...]).astype(BF16)
-        return nothing
+    for load in loads:
+        load.wait()
+    for p in range(pairs):
+        lanes = slice(p * LANES, (p + 1) * LANES)
+        entering = entering_ref[p * LANES : (p + 1) * LANES]
+        read = mm_nt(reader[:, lanes], entering) + local[:, lanes]
+        centred = read - head_sums(read, block) * (1.0 / head_size)
+        variance = head_sums(centred * centred, block) * (1.0 / head_size)
+        scaled = centred * lax.rsqrt(variance + GROUP_EPS) * gain_ref[:, lanes]
+        mixed[:, lanes] = scaled.astype(BF16)
 
     def block_rows(b):
         return pl.ds(pl.multiple_of(b * tokens, tokens), tokens)
 
-    lax.fori_loop(0, 4, project, 0)
+    def project_block(b, nothing):
+        rows = block_rows(b)
+        term[rows] = mm(mixed[rows], project[...]).astype(BF16)
+        return nothing
+
+    lax.fori_loop(0, 4, project_block, 0)
     nears = [
         side(term.at[block_rows(2 * y + 1 - low)], near_in.at[y], 1 + y, beside)
         for y in range(2)
@@ -613,25 +682,53 @@
         copy.wait_send()
 
 
-def return_rows(mixed, out_weight, total, hidden, far_down, targets, route_weight, capacity):
+def return_rows(
+    reader,
+    local_read,
+    out_weight,
+    gain,
+    entering,
+    total,
+    hidden,
+    far_down,
+    targets,
+    route_weight,
+    capacity,
+    head_size,
+):
     count = lax.axis_size("ep")
     rows, width = total.shape
     tokens = targets.shape[0]
-    operands = (mixed, out_weight, total, hidden, far_down, targets, route_weight)
+    streamed = [in_hbm(array) for array in (reader, local_read, out_weight)]
+    operands = (
+        gain.reshape(1, gain.shape[0]),
+        entering,
+        total,
+        hidden,
+        far_down,
+        targets,
+        route_weight,
+    )
     return pl.pallas_call(
-        functools.partial(return_kernel, capacity),
-        in_specs=[pl.BlockSpec(memory_space=pltpu.VMEM)] * len(operands),
+        functools.partial(return_kernel, capacity, head_size),
+        in_specs=[pl.BlockSpec(memory_space=pl.ANY)] * 3
+        + [pl.BlockSpec(memory_space=pltpu.VMEM)] * len(operands),
         out_specs=[pl.BlockSpec(memory_space=pltpu.VMEM)] * 2,
         out_shape=[jax.ShapeDtypeStruct((tokens, width), BF16)] * 2,
         scratch_shapes=[
+            pltpu.VMEM(reader.shape, BF16),
+            pltpu.VMEM(local_read.shape, F32),
+            pltpu.VMEM(out_weight.shape, BF16),
+            pltpu.VMEM(reader.shape, BF16),
             pltpu.VMEM(far_down.shape, BF16),
             pltpu.VMEM((rows, width), BF16),
             pltpu.VMEM((rows, width), BF16),
-            pltpu.VMEM((mixed.shape[0], width), BF16),
+            pltpu.VMEM((reader.shape[0], width), BF16),
             pltpu.VMEM((2, tokens, width), BF16),
             pltpu.VMEM((tokens, width), BF16),
             pltpu.VMEM((tokens, width), BF16),
             pltpu.VMEM((tokens, width), F32),
+            pltpu.SemaphoreType.DMA((3,)),
             pltpu.SemaphoreType.DMA((count - 1,)),
             pltpu.SemaphoreType.DMA((count - 1,)),
             pltpu.SemaphoreType.DMA((4,)),
@@ -644,7 +741,7 @@
             flops=6 * 10**9, bytes_accessed=12 * 2**20, transcendentals=0
         ),
         name="return_rows",
-    )(*operands)
+    )(*streamed, *operands)
 
 
 def swap(x, distance):
@@ -729,12 +826,21 @@
         decay_shift,
         head_size,
     )
-    cross = tuple(swap(array, 1) for array in far[:2])
-    mixed = mixer_finish(summary, reader, local_read, channel_gain, head_size)
-    total, hidden = expert_part(arrived, (own, near), (far[:2], cross))
+    total, hidden, entering = expert_part(arrived, summary, own, near, far[:2], head_size)
     return tuple(
         return_rows(
-            mixed, out_weight, total, hidden, far[2], own_targets, route_weight, capacity
+            reader,
+            local_read,
+            out_weight,
+            channel_gain,
+            entering,
+            total,
+            hidden,
+            far[2],
+            own_targets,
+            route_weight,
+            capacity,
+            head_size,
         )
     )
 

time: 186 us -> 146 us (0.78)
  Pallas kernels: 125 us -> 110 us
  waiting for transfers between devices: 27.9 us -> 13.2 us
  local copies, waits for them, and re-layouts: 11.9 us -> 6.41 us
  starting transfers between devices: 15 us -> 10.4 us
    pallas_call x3 -> x2, Pallas kernels: 93.9 us -> 78.7 us  [the longest x1 60.1 us: return_rows(): pl.pallas_call(functools.partial(return_kernel, capacity, head_size), in_...]
    ppermute x8 -> x6, waiting for transfers between devices: 27.9 us -> 13.2 us  [swap(): return lax.ppermute(x, 'tp', [(i, i ^ distance) for i in range(count)])]
    unnamed x37 -> x21, local copies, waits for them, and re-layouts: 11.5 us -> 5.95 us
    ppermute x8 -> x6, starting transfers between devices: 9.33 us -> 4.73 us  [swap(): return lax.ppermute(x, 'tp', [(i, i ^ distance) for i in range(count)])]
  transfers between devices with their start and end apart: 9 -> 7, of which waited for: 2 -> 3; matrix products, arithmetic and copies ran while one was open for 4% -> 0% of each run, Pallas kernels for 33% -> 34%
where the time goes in v3:
time: 146 us
  Pallas kernels  110 us (75%)
  waiting for transfers between devices  13.2 us (9%)
  starting transfers between devices  10.4 us (7%)
  local copies, waits for them, and re-layouts  6.41 us (4%)
  matrix products  3.18 us (2%)
  other arithmetic  2.2 us (2%)
    pallas_call x1, Pallas kernels, return_rows(): pl.pallas_call(functools.partial(return_kernel, capacity, head_size), in_...  60.1 us
    pallas_call x1, Pallas kernels, mixer_local(): pl.pallas_call(functools.partial(local_kernel, head_size), grid=(pairs,),...  31 us
    pallas_call x1, Pallas kernels, expert_part(): pl.pallas_call(functools.partial(part_kernel, head_size), in_specs=[pl.Bl...  18.6 us
    ppermute x6, waiting for transfers between devices, swap(): return lax.ppermute(x, 'tp', [(i, i ^ distance) for i in range(count)])  13.2 us
    unnamed x21, local copies, waits for them, and re-layouts  5.95 us
    all_to_all x1, starting transfers between devices, one_device(): lax.all_to_all(outgoing.reshape(experts, capacity, model_width), 'ep', sp...  5.71 us
    ppermute x6, starting transfers between devices, swap(): return lax.ppermute(x, 'tp', [(i, i ^ distance) for i in range(count)])  4.73 us
    dot_general x1, matrix products, one_device(): jnp.dot(dispersal_table(own_targets, experts * capacity), expert_normed,...  3.18 us
  transfers between devices with their start and end apart: 7, of which 3 were waited for; matrix products, arithmetic and copies ran while one was open for 0% of the time, Pallas kernels for 34%

profile of v3, /device:TPU:17, one launch (start us, length us, event | category | flops | bytes accessed | tf_op | source)
XLA Modules:
  0.0 145.8 jit_solution(3128474937429509462)
XLA Ops:
  0.6 0.7 broadcast_multiply_fusion
  1.3 0.8 copy.34
  2.1 1.2 fusion
  3.3 0.1 copy.35
  3.4 0.1 eq.29
  3.6 0.2 convert_reduce_fusion.1
  3.8 0.1 reshape.33
  3.9 0.1 copy.36
  4.0 0.1 convert_reduce_fusion
  4.1 3.2 %convolution_convert_fusion = bf16[512,2048]{1,0:T(8,128)(2,1)} fusion(bf16[128,2048]{1,0:T(8,128)(2,1)} %param.25, f32[2048]{0:T(1024)} %param.26, f32[128]{0:T(128)S(1)} %add_rsqrt_fusion, s32[512,128]{1,0:T(8,128)S(1)} %convert_reduce_fusion), kind=kOutput, calls=%fused_computation | convolution fusion | flops 270598144 | bytes 2892288 | tf_op jit(solution)/shard_map/dot_general | solution.py:806
  7.3 0.0 copy-start.6
  7.3 0.0 copy-start
  7.3 5.7 %all-to-all-start = ((bf16[8,64,2048]{2,1,0:T(8,128)(2,1)}), bf16[8,64,2048]{2,1,0:T(8,128)(2,1)S(1)}, u32[]{:S(2)}, u32[]{:S(2)}) async-start(bf16[8,64,2048]{2,1,0:T(8,128)(2,1)} %bitcast.10), calls=%async_computation | async-start | bytes 4194304 | tf_op jit(solution)/shard_map/all_to_all | solution.py:811
  13.0 1.2 collective-permute-start
  14.2 1.2 collective-permute-start.3
  15.5 0.3 collective-permute-start.1
  15.7 0.2 collective-permute-start.4
  16.0 0.5 collective-permute-start.2
  16.5 0.0 copy-done.6
  16.5 0.1 copy.33.shift_ref
  16.6 0.2 collective-permute-done.near_gate
  16.9 1.2 collective-permute-start.5
  18.1 0.0 copy-done
  18.1 0.0 copy-start.7
  18.1 31.0 %mixer_local.1 = (bf16[512,512]{1,0:T(8,128)(2,1)S(1)}, f32[512,512]{1,0:T(8,128)S(1)}, bf16[2,256,128]{2,1,0:T(8,128)(2,1)S(1)}) custom-call(bf16[512,512]{1,0:T(8,128)(2,1)} %r_ref.1, bf16[512,512]{1,0:T(8,128)(2,1)} %k_ref.1, bf16[512,512]{1,0:T(8,128)(2,1)} %v_ref.1, bf16[512,512]{1,0:T(8,128)(2,1)} %d_ref.1, bf16[512,512]{1,0:T(8,128)(2,1)} %l_ref.1, ...), custom_call_target="tpu_custom_call" | custom-call | flops 20000000000 | bytes 6291456 | tf_op jit(solution)/shard_map/mixer_local/pallas_call | solution.py:234
  49.1 0.0 copy-start.2
  49.1 1.0 copy-done.2
  50.1 0.0 copy-start.3
  50.1 0.8 copy-done.3
  50.9 0.0 copy-start.4
  50.9 0.7 copy-done.4
  51.5 0.0 copy-done.7
  51.5 0.1 copy.37.weight_ref
  51.6 0.0 collective-permute-done.1.near_up
  51.6 0.0 collective-permute-done.2.near_down
  51.6 0.0 collective-permute-done.3.far_gate
  51.6 10.1 %collective-permute-done.4.far_up = bf16[2048,256]{1,0:T(8,128)(2,1)} collective-permute-done((bf16[2048,256]{1,0:T(8,128)(2,1)}, bf16[2048,256]{1,0:T(8,128)(2,1)}, u32[]{:S(2)}, u32[]{:S(2)}) %collective-permute-start.4) | collective-permute-done | bytes 1048608 | tf_op jit(solution)/shard_map/ppermute | solution.py:749
  61.7 0.0 all-to-all-done
  61.7 0.0 copy-start.5
  61.7 0.9 copy-done.5
  62.6 0.0 copy-start.1
  62.6 18.6 %expert_part.1 = (f32[512,2048]{1,0:T(8,128)S(1)}, bf16[512,512]{1,0:T(8,128)(2,1)S(1)}, f32[512,128]{1,0:T(8,128)S(1)}) custom-call(bf16[512,2048]{1,0:T(8,128)(2,1)S(1)} %bitcast.7, bf16[2,256,128]{2,1,0:T(8,128)(2,1)S(1)} %copy-done.5, bf16[2048,256]{1,0:T(8,128)(2,1)} %bitcast.13, bf16[2048,256]{1,0:T(8,128)(2,1)} %bitcast.16, ...), custom_call_target="tpu_custom_call" | custom-call | flops 5368709120 | bytes 12582912 | tf_op jit(solution)/shard_map/expert_part/pallas_call | solution.py:480
  81.2 2.9 %collective-permute-done.5.far_ref = bf16[256,2048]{1,0:T(8,128)(2,1)S(1)} collective-permute-done((bf16[256,2048]{1,0:T(8,128)(2,1)}, bf16[256,2048]{1,0:T(8,128)(2,1)S(1)}, u32[]{:S(2)}, u32[]{:S(2)}) %collective-permute-start.5) | collective-permute-done | bytes 1048608 | tf_op jit(solution)/shard_map/ppermute | solution.py:749
  84.1 0.0 copy-done.1
  84.1 60.1 %return_rows.1 = (bf16[128,2048]{1,0:T(8,128)(2,1)S(1)}, bf16[128,2048]{1,0:T(8,128)(2,1)S(1)}) custom-call(bf16[512,512]{1,0:T(8,128)(2,1)} %copy-done.3, f32[512,512]{1,0:T(8,128)} %copy-done.2, bf16[512,2048]{1,0:T(8,128)(2,1)} %project_ref.1, f32[1,512]{1,0:T(1,128)S(1)} %bitcast.9, f32[512,128]{1,0:T(8,128)S(1)} %get-tuple-element.11.entering_ref, ...), custom_call_target="tpu_custom_call" | custom-call | flops 6000000000 | bytes 12582912 | tf_op jit(solution)/shard_map/return_rows/pallas_call | solution.py:712
  144.2 0.8 copy.40
  145.0 0.8 copy.41
  (2 shorter events, 0.0 us)
Async XLA Ops:
  7.3 9.2 %copy-start.6 = (f32[512,8]{0,1:T(8,128)S(1)}, f32[512,8]{0,1:T(8,128)}, u32[]{:S(2)}) copy-start(f32[512,8]{0,1:T(8,128)} %param.22) | copy-start | bytes 49156
  7.3 10.8 %copy-start = (f32[512]{0:T(512)S(1)}, f32[512]{0:T(512)}, u32[]{:S(2)}) copy-start(f32[512]{0:T(512)} %param.21) | copy-start | bytes 6148
  7.3 54.5 %all-to-all-start = ((bf16[8,64,2048]{2,1,0:T(8,128)(2,1)}), bf16[8,64,2048]{2,1,0:T(8,128)(2,1)S(1)}, u32[]{:S(2)}, u32[]{:S(2)}) async-start(bf16[8,64,2048]{2,1,0:T(8,128)(2,1)} %bitcast.10), calls=%async_computation | async-start | bytes 4194304 | tf_op jit(solution)/shard_map/all_to_all | solution.py:811
  13.0 3.9 %collective-permute-start = (bf16[2048,256]{1,0:T(8,128)(2,1)}, bf16[2048,256]{1,0:T(8,128)(2,1)}, u32[]{:S(2)}, u32[]{:S(2)}) collective-permute-start(bf16[2048,256]{1,0:T(8,128)(2,1)} %bitcast.11), channel_id=1, source_target_pairs={{0,1},{1,0},{2,3},{3,2},{4,5},{5,4},{6,7},{7,6},{8,9},{9,8},{10,11... | collective-permute-start | bytes 3145736 | tf_op jit(solution)/shard_map/ppermute | solution.py:749
  14.2 37.4 %collective-permute-start.3 = (bf16[2048,256]{1,0:T(8,128)(2,1)}, bf16[2048,256]{1,0:T(8,128)(2,1)}, u32[]{:S(2)}, u32[]{:S(2)}) collective-permute-start(bf16[2048,256]{1,0:T(8,128)(2,1)} %bitcast.12), channel_id=1, source_target_pairs={{0,2},{1,3},{2,0},{3,1},{4,6},{5,7},{6,4},{7,5},{8,10},{9,11},{10,... | collective-permute-start | bytes 3145736 | tf_op jit(solution)/shard_map/ppermute | solution.py:749
  15.5 36.2 %collective-permute-start.1 = (bf16[2048,256]{1,0:T(8,128)(2,1)}, bf16[2048,256]{1,0:T(8,128)(2,1)}, u32[]{:S(2)}, u32[]{:S(2)}) collective-permute-start(bf16[2048,256]{1,0:T(8,128)(2,1)} %bitcast.14), channel_id=1, source_target_pairs={{0,1},{1,0},{2,3},{3,2},{4,5},{5,4},{6,7},{7,6},{8,9},{9,8},{10,11... | collective-permute-start | bytes 3145736 | tf_op jit(solution)/shard_map/ppermute | solution.py:749
  15.7 46.0 %collective-permute-start.4 = (bf16[2048,256]{1,0:T(8,128)(2,1)}, bf16[2048,256]{1,0:T(8,128)(2,1)}, u32[]{:S(2)}, u32[]{:S(2)}) collective-permute-start(bf16[2048,256]{1,0:T(8,128)(2,1)} %bitcast.15), channel_id=1, source_target_pairs={{0,2},{1,3},{2,0},{3,1},{4,6},{5,7},{6,4},{7,5},{8,10},{9,11},{10,... | collective-permute-start | bytes 3145736 | tf_op jit(solution)/shard_map/ppermute | solution.py:749
  16.0 35.7 %collective-permute-start.2 = (bf16[256,2048]{1,0:T(8,128)(2,1)}, bf16[256,2048]{1,0:T(8,128)(2,1)}, u32[]{:S(2)}, u32[]{:S(2)}) collective-permute-start(bf16[256,2048]{1,0:T(8,128)(2,1)} %bitcast.17), channel_id=1, source_target_pairs={{0,1},{1,0},{2,3},{3,2},{4,5},{5,4},{6,7},{7,6},{8,9},{9,8},{10,11... | collective-permute-start | bytes 3145736 | tf_op jit(solution)/shard_map/ppermute | solution.py:749
  16.9 67.2 %collective-permute-start.5 = (bf16[256,2048]{1,0:T(8,128)(2,1)}, bf16[256,2048]{1,0:T(8,128)(2,1)S(1)}, u32[]{:S(2)}, u32[]{:S(2)}) collective-permute-start(bf16[256,2048]{1,0:T(8,128)(2,1)} %bitcast.18), channel_id=1, source_target_pairs={{0,2},{1,3},{2,0},{3,1},{4,6},{5,7},{6,4},{7,5},{8,10},{9,11},{10,... | collective-permute-start | bytes 3145736 | tf_op jit(solution)/shard_map/ppermute | solution.py:749
  18.1 33.4 %copy-start.7 = (f32[128,2]{0,1:T(2,128)S(1)}, f32[128,2]{0,1:T(2,128)}, u32[]{:S(2)}) copy-start(f32[128,2]{0,1:T(2,128)} %param.28) | copy-start | bytes 3076
  49.1 1.0 copy-start.2
  50.1 0.8 copy-start.3
  50.9 0.7 copy-start.4
  61.7 0.9 copy-start.5
  62.6 21.5 %copy-start.1 = (f32[512]{0:T(512)S(1)}, f32[512]{0:T(512)}, u32[]{:S(2)}) copy-start(f32[512]{0:T(512)} %param.23) | copy-start | bytes 6148

commit v4 on v3

--- a/solution.py
+++ b/solution.py
@@ -75,8 +75,70 @@
     return inverses
 
 
+def send_to(src, dst, send_sem, recv_sem, target):
+    return pltpu.make_async_remote_copy(
+        src_ref=src,
+        dst_ref=dst,
+        send_sem=send_sem,
+        recv_sem=recv_sem,
+        device_id=target,
+        device_id_type=pl.DeviceIdType.MESH,
+    )
+
+
+def greet_all(barrier, here, count, others):
+    def greet(distance, nothing):
+        pl.semaphore_signal(
+            barrier,
+            inc=1,
+            device_id={"ep": lax.rem(here + distance, count)},
+            device_id_type=pl.DeviceIdType.MESH,
+        )
+        return nothing
+
+    lax.fori_loop(1, count, greet, 0)
+    for target in others:
+        pl.semaphore_signal(
+            barrier, inc=1, device_id={"tp": target}, device_id_type=pl.DeviceIdType.MESH
+        )
+
+
+def in_hbm(array):
+    return pltpu.with_memory_space_constraint(array, pltpu.HBM)
+
+
+def far_first(k, count):
+    return count // 2 + ((k + 1) // 2) * (2 * lax.rem(k, 2) - 1)
+
+
+def pack_rows(tokens_ref, scale_ref, routes_ref, outgoing, count, capacity):
+    inputs = tokens_ref[...].astype(F32)
+    square = jnp.sum(inputs * inputs, axis=1, keepdims=True) * (1.0 / inputs.shape[1])
+    normed = (inputs * lax.rsqrt(square + NORM_EPS) * scale_ref[...]).astype(BF16)
+    rows = inputs.shape[0]
+    members = grid_index((count, rows), 0)
+    named = jnp.zeros((count, rows), F32)
+    for picked in range(routes_ref.shape[0]):
+        named = jnp.where(routes_ref[picked : picked + 1] == members, 1.0, named)
+    earlier = grid_index((rows, rows), 0) < grid_index((rows, rows), 1)
+    slots = mm(named, earlier.astype(F32))
+    slots = jnp.where(named > 0.5, slots, -1.0).astype(jnp.int32)
+    wanted = grid_index((capacity, rows), 0)
+    group = max(1, min(count, 256 // capacity))
+    for begin in range(0, count, group):
+        table = jnp.concatenate(
+            [
+                jnp.where(slots[e : e + 1] == wanted, 1.0, 0.0)
+                for e in range(begin, begin + group)
+            ],
+            axis=0,
+        )
+        outgoing[begin * capacity : (begin + group) * capacity] = mm(table, normed).astype(BF16)
+
+
 def local_kernel(
     head_size,
+    capacity,
     r_ref,
     k_ref,
     v_ref,
@@ -84,13 +146,72 @@
     l_ref,
     base_ref,
     shift_ref,
+    tokens_ref,
+    scale_ref,
+    routes_ref,
+    own_gate,
+    own_up,
+    own_down,
     reader_ref,
     local_ref,
     summary_ref,
+    arrived,
+    near_gate,
+    near_up,
+    near_down,
     state,
+    outgoing,
+    keep_sem,
+    send_sems,
+    recv_sems,
+    side_send,
+    side_recv,
 ):
     pair = pl.program_id(0)
     half = LANES // 2
+    here = lax.axis_index("ep")
+    count = lax.axis_size("ep")
+    place = lax.axis_index("tp")
+    beside = place + 1 - 2 * lax.rem(place, 2)
+
+    def rows_of(member):
+        return pl.ds(pl.multiple_of(member * capacity, capacity), capacity)
+
+    def post(distance, member):
+        return send_to(
+            outgoing.at[rows_of(member)],
+            arrived.at[rows_of(here)],
+            send_sems.at[distance - 1],
+            recv_sems.at[distance - 1],
+            {"ep": member},
+        )
+
+    keep = pltpu.make_async_copy(
+        outgoing.at[rows_of(here)], arrived.at[rows_of(here)], keep_sem
+    )
+    nears = [
+        send_to(src, dst, side_send.at[i], side_recv.at[i], {"tp": beside})
+        for i, (src, dst) in enumerate(
+            [(own_gate, near_gate), (own_up, near_up), (own_down, near_down)]
+        )
+    ]
+
+    @pl.when(pair == 0)
+    def _():
+        barrier = pltpu.get_barrier_semaphore()
+        greet_all(barrier, here, count, (beside,))
+        pack_rows(tokens_ref, scale_ref, routes_ref, outgoing, count, capacity)
+        pl.semaphore_wait(barrier, count)
+
+        def launch(k, nothing):
+            distance = far_first(k, count)
+            post(distance, lax.rem(here + distance, count)).start()
+            return nothing
+
+        lax.fori_loop(0, count - 1, launch, 0)
+        keep.start()
+        for copy in nears:
+            copy.start()
 
     rows = grid_index((SPAN, SPAN), 0)
     cols = grid_index((SPAN, SPAN), 1)
@@ -222,38 +343,96 @@
     summary_ref[1] = (state[:half] + state[half:LANES]).astype(BF16)
     summary_ref[0] = (state[LANES : LANES + half] + state[LANES + half :]).astype(BF16)
 
-
-def mixer_local(receptance, keys, values, decay, learn, base, shift, head_size):
+    @pl.when(pair == pl.num_programs(0) - 1)
+    def _():
+        def collect(k, nothing):
+            distance = far_first(k, count)
+            copy = post(distance, lax.rem(here + distance, count))
+            copy.wait_send()
+            copy.wait_recv()
+            return nothing
+
+        lax.fori_loop(0, count - 1, collect, 0)
+        keep.wait()
+        for copy in nears:
+            copy.wait()
+
+
+def mixer_local(
+    receptance,
+    keys,
+    values,
+    decay,
+    learn,
+    base,
+    shift,
+    tokens,
+    scale,
+    routes,
+    own,
+    head_size,
+    capacity,
+):
     rows, channels = receptance.shape
     pairs = channels // LANES
     heads = shift.shape[1]
     half = LANES // 2
+    count = lax.axis_size("ep")
+    token_rows, width = tokens.shape
+    picks = routes.shape[1]
     tile = pl.BlockSpec((rows, LANES), lambda p: (0, p))
     small = pl.BlockSpec((2, half, LANES), lambda p: (0, p, 0))
+    anywhere = pl.BlockSpec(memory_space=pl.ANY)
     streams = [in_hbm(array) for array in (receptance, keys, values, decay, learn)]
+    shards = [in_hbm(array) for array in own]
     return pl.pallas_call(
-        functools.partial(local_kernel, head_size),
+        functools.partial(local_kernel, head_size, capacity),
         grid=(pairs,),
         in_specs=[tile] * 5
         + [
             pl.BlockSpec((1, 1, LANES), lambda p: (p, 0, 0)),
             pl.BlockSpec((rows, heads), lambda p: (0, 0)),
-        ],
-        out_specs=[tile, tile, small],
+            pl.BlockSpec((token_rows, width), lambda p: (0, 0)),
+            pl.BlockSpec((1, width), lambda p: (0, 0)),
+            pl.BlockSpec((picks, token_rows), lambda p: (0, 0)),
+        ]
+        + [anywhere] * 3,
+        out_specs=[tile, tile, small] + [anywhere] * 4,
         out_shape=[
             jax.ShapeDtypeStruct((rows, channels), BF16),
             jax.ShapeDtypeStruct((rows, channels), F32),
             jax.ShapeDtypeStruct((2, pairs * half, LANES), BF16),
+            jax.ShapeDtypeStruct((count * capacity, width), BF16),
+        ]
+        + [jax.ShapeDtypeStruct(array.shape, BF16) for array in own],
+        scratch_shapes=[
+            pltpu.VMEM((2 * LANES, LANES), F32),
+            pltpu.VMEM((count * capacity, width), BF16),
+            pltpu.SemaphoreType.DMA,
+            pltpu.SemaphoreType.DMA((count - 1,)),
+            pltpu.SemaphoreType.DMA((count - 1,)),
+            pltpu.SemaphoreType.DMA((3,)),
+            pltpu.SemaphoreType.DMA((3,)),
         ],
-        scratch_shapes=[pltpu.VMEM((2 * LANES, LANES), F32)],
         compiler_params=pltpu.CompilerParams(
-            dimension_semantics=("arbitrary",), vmem_limit_bytes=24 * 2**20
+            dimension_semantics=("arbitrary",),
+            vmem_limit_bytes=24 * 2**20,
+            collective_id=2,
+            has_side_effects=True,
         ),
         cost_estimate=pl.CostEstimate(
             flops=20 * 10**9, bytes_accessed=6 * 2**20, transcendentals=10**6
         ),
         name="mixer_local",
-    )(*streams, base.reshape(pairs, 1, LANES), shift)
+    )(
+        *streams,
+        base.reshape(pairs, 1, LANES),
+        shift,
+        tokens,
+        scale.reshape(1, width),
+        routes.T,
+        *shards,
+    )
 
 
 def gated(x, gate, up):
@@ -262,41 +441,13 @@
     return (gates / (1.0 + jnp.exp(-gates)) * uppers).astype(BF16)
 
 
-def send_to(src, dst, send_sem, recv_sem, target):
-    return pltpu.make_async_remote_copy(
-        src_ref=src,
-        dst_ref=dst,
-        send_sem=send_sem,
-        recv_sem=recv_sem,
-        device_id=target,
-        device_id_type=pl.DeviceIdType.MESH,
-    )
-
-
-def greet_all(barrier, here, count, others):
-    def greet(distance, nothing):
-        pl.semaphore_signal(
-            barrier,
-            inc=1,
-            device_id={"ep": lax.rem(here + distance, count)},
-            device_id_type=pl.DeviceIdType.MESH,
-        )
-        return nothing
-
-    lax.fori_loop(1, count, greet, 0)
-    for target in others:
-        pl.semaphore_signal(
-            barrier, inc=1, device_id={"tp": target}, device_id_type=pl.DeviceIdType.MESH
-        )
-
-
 def part_kernel(
     head_size,
-    x_ref,
-    summary_ref,
     own_gate,
     own_up,
     own_down,
+    summary_ref,
+    x_ref,
     near_gate,
     near_up,
     near_down,
@@ -336,12 +487,7 @@
             [
                 (own_gate, held.at[0]),
                 (own_up, held.at[1]),
-                (own_down, held_down.at[0]),
-                (near_gate, held.at[2]),
-                (near_up, held.at[3]),
-                (near_down, held_down.at[1]),
-                (far_gate, held.at[4]),
-                (far_up, held.at[5]),
+                (own_down, held_down),
             ]
         )
     ]
@@ -358,6 +504,18 @@
             recv_sems.at[level],
             {"ep": target},
         )
+
+    def transfer_state(level, distance, target):
+        return send_to(
+            sending.at[1],
+            landed.at[level, 1],
+            send_sems.at[distance - 1],
+            recv_sems.at[level],
+            {"ep": target},
+        )
+
+    def sends_all(reach):
+        return (lax.rem(here, 2 * reach) == reach - 1) & (here >= 2 * reach)
 
     def wide(part):
         part = part.astype(F32)
@@ -391,16 +549,20 @@
                 sending[0, spot(p)] = (moved[:half] + moved[half:LANES]).astype(BF16)
                 sending[1, spot(p)] = (after[:half] + after[half:]).astype(BF16)
 
+        def launch_with(transfer):
             def launch(distance, nothing):
                 transfer(level, distance, here + distance).start()
                 return nothing
 
             lax.fori_loop(1, reach + 1, launch, 0)
 
+        pl.when(sends_all(reach))(lambda: launch_with(transfer))
+        pl.when(here == reach - 1)(lambda: launch_with(transfer_state))
+
     def take_round(level):
         reach = 2**level
 
-        @pl.when(lax.rem(here // reach, 2) == 1)
+        @pl.when((lax.rem(here // reach, 2) == 1) & (here >= 2 * reach))
         def _():
             transfer(level, 1, here).wait_recv()
             for p in range(pairs):
@@ -412,6 +574,14 @@
                 before[0, p] = moved[:LANES]
                 before[1, p] = moved[LANES:] + before[1, p]
 
+        @pl.when((here >= reach) & (here < 2 * reach))
+        def _():
+            transfer_state(level, 1, here).wait_recv()
+            for p in range(pairs):
+                state = wide(landed[level, 1, spot(p)])
+                high, low = split_two(before[0, p])
+                before[1, p] = mm(state, high) + mm(state, low) + before[1, p]
+
     def over_rows(body):
         def step(i, nothing):
             body(pl.ds(pl.multiple_of(i * piece, piece), piece))
@@ -421,21 +591,21 @@
 
     def first_part(at):
         hidden = gated(x_ref[at], held[0], held[1])
-        total_ref[at] = mm(hidden, held_down[0])
+        total_ref[at] = mm(hidden, held_down[...])
 
     def second_part(at):
-        hidden = gated(x_ref[at], held[2], held[3])
-        total_ref[at] += mm(hidden, held_down[1])
+        hidden = gated(x_ref[at], near_gate[...], near_up[...])
+        total_ref[at] += mm(hidden, near_down[...])
 
     def third_part(at):
-        hidden_ref[at, :units] = gated(x_ref[at], held[4], held[5])
+        hidden_ref[at, :units] = gated(x_ref[at], far_gate[...], far_up[...])
 
     def fourth_part(at):
         hidden_ref[at, units:] = gated(x_ref[at], cross[0], cross[1])
 
     send_round(0)
     bodies = (first_part, second_part, third_part, fourth_part)
-    needs = (loads[:3], loads[3:6], loads[6:], ())
+    needs = (loads, (), (), ())
     for turn in range(max(len(bodies), rounds)):
         if turn < len(bodies):
             for load in needs[turn]:
@@ -451,23 +621,22 @@
     for p in range(pairs):
         entering_ref[p * LANES : (p + 1) * LANES] = before[1, p]
 
+    def settle_with(transfer, level, reach):
+        def settle(distance, nothing):
+            transfer(level, distance, here + distance).wait_send()
+            return nothing
+
+        lax.fori_loop(1, reach + 1, settle, 0)
+
     for level in range(rounds):
         reach = 2**level
-
-        @pl.when(lax.rem(here, 2 * reach) == reach - 1)
-        def _(level=level, reach=reach):
-            def settle(distance, nothing):
-                transfer(level, distance, here + distance).wait_send()
-                return nothing
-
-            lax.fori_loop(1, reach + 1, settle, 0)
+        pl.when(sends_all(reach))(functools.partial(settle_with, transfer, level, reach))
+        pl.when(here == reach - 1)(
+            functools.partial(settle_with, transfer_state, level, reach)
+        )
 
     for forward in forwards:
         forward.wait_send()
-
-
-def in_hbm(array):
-    return pltpu.with_memory_space_constraint(array, pltpu.HBM)
 
 
 def expert_part(incoming, summary, own, near, far, head_size):
@@ -476,11 +645,12 @@
     pairs = summary.shape[1] * 2 // LANES
     count = lax.axis_size("ep")
     rounds = (count - 1).bit_length()
-    weights = [in_hbm(array) for array in own + near + far]
+    shards = [in_hbm(array) for array in own]
+    operands = (summary, incoming) + near + far
     return pl.pallas_call(
         functools.partial(part_kernel, head_size),
-        in_specs=[pl.BlockSpec(memory_space=pltpu.VMEM)] * 2
-        + [pl.BlockSpec(memory_space=pl.ANY)] * len(weights),
+        in_specs=[pl.BlockSpec(memory_space=pl.ANY)] * 3
+        + [pl.BlockSpec(memory_space=pltpu.VMEM)] * len(operands),
         out_specs=[pl.BlockSpec(memory_space=pltpu.VMEM)] * 3,
         out_shape=[
             jax.ShapeDtypeStruct((rows, width), F32),
@@ -488,13 +658,13 @@
             jax.ShapeDtypeStruct((pairs * LANES, LANES), F32),
         ],
         scratch_shapes=[
-            pltpu.VMEM((6, width, units), BF16),
-            pltpu.VMEM((2, units, width), BF16),
+            pltpu.VMEM((2, width, units), BF16),
+            pltpu.VMEM((units, width), BF16),
             pltpu.VMEM((2, width, units), BF16),
             pltpu.VMEM((2, pairs, LANES, LANES), F32),
             pltpu.VMEM(summary.shape, BF16),
             pltpu.VMEM((rounds,) + summary.shape, BF16),
-            pltpu.SemaphoreType.DMA((8,)),
+            pltpu.SemaphoreType.DMA((3,)),
             pltpu.SemaphoreType.DMA((count // 2,)),
             pltpu.SemaphoreType.DMA((rounds,)),
             pltpu.SemaphoreType.DMA((2,)),
@@ -509,26 +679,24 @@
             transcendentals=4 * rows * units,
         ),
         name="expert_part",
-    )(incoming, summary, *weights)
+    )(*shards, *operands)
 
 
 def return_kernel(
     capacity,
     head_size,
-    reader_ref,
-    local_ref,
     project_ref,
+    reader,
+    local,
     gain_ref,
     entering_ref,
     total_ref,
     hidden_ref,
     far_ref,
-    target_ref,
+    routes_ref,
     weight_ref,
     mixer_ref,
     expert_ref,
-    reader,
-    local,
     project,
     mixed,
     cross,
@@ -539,7 +707,7 @@
     pair_out,
     far_in,
     combined,
-    load_sems,
+    load_sem,
     send_sems,
     recv_sems,
     side_send,
@@ -577,14 +745,8 @@
 
     forward = side(far_ref, cross, 0, beside)
     forward.start()
-    loads = [
-        pltpu.make_async_copy(src, dst, load_sems.at[i])
-        for i, (src, dst) in enumerate(
-            [(reader_ref, reader), (local_ref, local), (project_ref, project)]
-        )
-    ]
-    for load in loads:
-        load.start()
+    load = pltpu.make_async_copy(project_ref, project, load_sem)
+    load.start()
     forward.wait_recv()
 
     def finished(member):
@@ -593,11 +755,8 @@
         row = total_ref[rows] + mm(hidden[:, :units], far_ref[...])
         return (row + mm(hidden[:, units:], cross[...])).astype(BF16)
 
-    def far_first(k):
-        return count // 2 + ((k + 1) // 2) * (2 * lax.rem(k, 2) - 1)
-
     def send_block(k, nothing):
-        distance = far_first(k)
+        distance = far_first(k, count)
         member = lax.rem(here + distance, count)
         staged[rows_of(member)] = finished(member)
         back(distance, member).start()
@@ -606,8 +765,7 @@
     lax.fori_loop(0, count - 1, send_block, 0)
     landed[rows_of(here)] = finished(here)
 
-    for load in loads:
-        load.wait()
+    load.wait()
     for p in range(pairs):
         lanes = slice(p * LANES, (p + 1) * LANES)
         entering = entering_ref[p * LANES : (p + 1) * LANES]
@@ -633,8 +791,29 @@
     for copy in nears:
         copy.start()
 
-    target = target_ref[...]
-    weight = weight_ref[...]
+    picks = routes_ref.shape[0]
+    packed = jnp.concatenate(
+        [routes_ref[...].astype(F32), weight_ref[...], jnp.zeros((8 - 2 * picks, tokens), F32)],
+        axis=0,
+    ).T
+    lane = grid_index((tokens, LANES), 1)
+    routes = [packed[:, i : i + 1].astype(jnp.int32) for i in range(picks)]
+    weight = packed[:, picks : 2 * picks]
+    named = jnp.zeros((tokens, LANES), F32)
+    for route in routes:
+        named = jnp.where(route == lane, 1.0, named)
+    earlier = grid_index((tokens, tokens), 0) > grid_index((tokens, tokens), 1)
+    slots = mm(earlier.astype(F32), named)
+    target = jnp.concatenate(
+        [
+            route * capacity
+            + jnp.sum(jnp.where(route == lane, slots, 0.0), axis=1, keepdims=True).astype(
+                jnp.int32
+            )
+            for route in routes
+        ],
+        axis=1,
+    )
     slot = grid_index((tokens, capacity), 1)
 
     def taken(member):
@@ -659,7 +838,7 @@
     cross_send.start()
 
     def gather_block(k, nothing):
-        distance = far_first(count - 2 - k)
+        distance = far_first(count - 2 - k, count)
         member = lax.rem(here + count - distance, count)
         back(distance, member).wait_recv()
         combined[...] += taken(member)
@@ -673,7 +852,7 @@
     expert_ref[...] = combined[...].astype(BF16)
 
     def settle(k, nothing):
-        distance = far_first(k)
+        distance = far_first(k, count)
         back(distance, lax.rem(here + distance, count)).wait_send()
         return nothing
 
@@ -691,33 +870,32 @@
     total,
     hidden,
     far_down,
-    targets,
+    routes,
     route_weight,
     capacity,
     head_size,
 ):
     count = lax.axis_size("ep")
     rows, width = total.shape
-    tokens = targets.shape[0]
-    streamed = [in_hbm(array) for array in (reader, local_read, out_weight)]
+    tokens = routes.shape[0]
     operands = (
+        reader,
+        local_read,
         gain.reshape(1, gain.shape[0]),
         entering,
         total,
         hidden,
         far_down,
-        targets,
-        route_weight,
+        routes.T,
+        route_weight.T,
     )
     return pl.pallas_call(
         functools.partial(return_kernel, capacity, head_size),
-        in_specs=[pl.BlockSpec(memory_space=pl.ANY)] * 3
+        in_specs=[pl.BlockSpec(memory_space=pl.ANY)]
         + [pl.BlockSpec(memory_space=pltpu.VMEM)] * len(operands),
         out_specs=[pl.BlockSpec(memory_space=pltpu.VMEM)] * 2,
         out_shape=[jax.ShapeDtypeStruct((tokens, width), BF16)] * 2,
         scratch_shapes=[
-            pltpu.VMEM(reader.shape, BF16),
-            pltpu.VMEM(local_read.shape, F32),
             pltpu.VMEM(out_weight.shape, BF16),
             pltpu.VMEM(reader.shape, BF16),
             pltpu.VMEM(far_down.shape, BF16),
@@ -728,7 +906,7 @@
             pltpu.VMEM((tokens, width), BF16),
             pltpu.VMEM((tokens, width), BF16),
             pltpu.VMEM((tokens, width), F32),
-            pltpu.SemaphoreType.DMA((3,)),
+            pltpu.SemaphoreType.DMA,
             pltpu.SemaphoreType.DMA((count - 1,)),
             pltpu.SemaphoreType.DMA((count - 1,)),
             pltpu.SemaphoreType.DMA((4,)),
@@ -741,28 +919,12 @@
             flops=6 * 10**9, bytes_accessed=12 * 2**20, transcendentals=0
         ),
         name="return_rows",
-    )(*streamed, *operands)
+    )(in_hbm(out_weight), *operands)
 
 
 def swap(x, distance):
     count = lax.axis_size("tp")
     return lax.ppermute(x, "tp", [(i, i ^ distance) for i in range(count)])
-
-
-def slot_targets(block_routes, capacity):
-    flat_routes = block_routes.reshape(-1)
-    count = flat_routes.shape[0]
-    order = jnp.arange(count, dtype=jnp.int32)
-    before = (order[:, None] > order[None, :]) & (flat_routes[:, None] == flat_routes[None, :])
-    slots = jnp.sum(before.astype(jnp.int32), axis=1).reshape(block_routes.shape)
-    return block_routes * capacity + slots
-
-
-def dispersal_table(targets, places):
-    marks = (jnp.arange(places, dtype=jnp.int32)[:, None, None] == targets[None, :, :]).astype(
-        jnp.int32
-    )
-    return jnp.sum(marks, axis=2).astype(jnp.bfloat16)
 
 
 def one_device(
@@ -786,37 +948,12 @@
     ep_count = lax.axis_size("ep")
     channels = receptance.shape[1]
     head_size = channels // decay_shift.shape[1]
-    token_rows, model_width = expert_input.shape
-    top_count = routes.shape[1]
     experts = gate_weight.shape[0] * ep_count
-    capacity = max(2, 2 * token_rows * top_count // experts)
-    slab_rows = ep_count * capacity
+    capacity = max(2, 2 * expert_input.shape[0] * routes.shape[1] // experts)
 
     own = (gate_weight[0], up_weight[0], down_weight[0])
     far = tuple(swap(array, 2) for array in own)
-    near = tuple(swap(array, 1) for array in own)
-
-    inputs = expert_input.astype(F32)
-    expert_normed = (
-        inputs
-        * lax.rsqrt(jnp.mean(inputs * inputs, axis=1, keepdims=True) + NORM_EPS)
-        * expert_gain
-    ).astype(BF16)
-    own_targets = slot_targets(routes, capacity)
-    outgoing = jnp.dot(
-        dispersal_table(own_targets, experts * capacity),
-        expert_normed,
-        preferred_element_type=F32,
-    ).astype(BF16)
-    arrived = lax.all_to_all(
-        outgoing.reshape(experts, capacity, model_width),
-        "ep",
-        split_axis=0,
-        concat_axis=0,
-        tiled=True,
-    ).reshape(slab_rows, model_width)
-
-    reader, local_read, summary = mixer_local(
+    reader, local_read, summary, arrived, *near = mixer_local(
         receptance,
         key_rows,
         value_rows,
@@ -824,8 +961,14 @@
         learn_input,
         decay_base,
         decay_shift,
+        expert_input,
+        expert_gain,
+        routes,
+        own,
         head_size,
-    )
+        capacity,
+    )
+    near = tuple(near)
     total, hidden, entering = expert_part(arrived, summary, own, near, far[:2], head_size)
     return tuple(
         return_rows(
@@ -837,7 +980,7 @@
             total,
             hidden,
             far[2],
-            own_targets,
+            routes,
             route_weight,
             capacity,
             head_size,

time: 146 us -> 132 us (0.904)
  waiting for transfers between devices: 13.2 us -> 0.01 us
  Pallas kernels: 110 us -> 122 us
  starting transfers between devices: 10.4 us -> 2.77 us
  matrix products: 3.18 us -> 0 us
  other arithmetic: 2.2 us -> 0 us
    pallas_call x1, Pallas kernels: 31 us -> 50.1 us  [mixer_local(): pl.pallas_call(functools.partial(local_kernel, head_size, capacity), grid...]
    ppermute x6 -> x3, waiting for transfers between devices: 13.2 us -> 0.01 us  [swap(): return lax.ppermute(x, 'tp', [(i, i ^ distance) for i in range(count)])]
    all_to_all x1 -> x0, starting transfers between devices: 5.71 us -> none  [one_device(): lax.all_to_all(outgoing.reshape(experts, capacity, model_width), 'ep', sp...]
    pallas_call x1, Pallas kernels: 18.6 us -> 13.9 us  [expert_part(): pl.pallas_call(functools.partial(part_kernel, head_size), in_specs=[pl.Bl...]
    dot_general x1 -> x0, matrix products: 3.18 us -> none  [one_device(): jnp.dot(dispersal_table(own_targets, experts * capacity), expert_normed,...]
    ppermute x6 -> x3, starting transfers between devices: 4.73 us -> 2.77 us  [swap(): return lax.ppermute(x, 'tp', [(i, i ^ distance) for i in range(count)])]
    pallas_call x1, Pallas kernels: 60.1 us -> 58.3 us  [return_rows(): pl.pallas_call(functools.partial(return_kernel, capacity, head_size), in_...]
    reduce_sum x3 -> x0, other arithmetic: 1.5 us -> none  [the longest x1 1.23 us: one_device(): jnp.mean(inputs * inputs, axis=1, keepdims=True) + NORM_EPS]
  transfers between devices with their start and end apart: 7 -> 3, of which waited for: 3 -> 0; matrix products, arithmetic and copies ran while one was open for 0% -> 1% of each run, Pallas kernels for 34% -> 49%
where the time goes in v4:
time: 132 us; the launch traced here: 131 us
  Pallas kernels  122 us (92%)
  local copies, waits for them, and re-layouts  5.54 us (4%)
  starting transfers between devices  2.77 us (2%)
    pallas_call x1, Pallas kernels, return_rows(): pl.pallas_call(functools.partial(return_kernel, capacity, head_size), in_...  58.3 us
    pallas_call x1, Pallas kernels, mixer_local(): pl.pallas_call(functools.partial(local_kernel, head_size, capacity), grid...  50.1 us
    pallas_call x1, Pallas kernels, expert_part(): pl.pallas_call(functools.partial(part_kernel, head_size), in_specs=[pl.Bl...  13.9 us
    unnamed x17, local copies, waits for them, and re-layouts  5.54 us
    ppermute x3, starting transfers between devices, swap(): return lax.ppermute(x, 'tp', [(i, i ^ distance) for i in range(count)])  2.77 us
  transfers between devices with their start and end apart: 3, of which 0 were waited for; matrix products, arithmetic and copies ran while one was open for 1% of the time, Pallas kernels for 49%

profile of v4, /device:TPU:17, one launch (start us, length us, event | category | flops | bytes accessed | tf_op | source)
XLA Modules:
  0.0 131.4 jit_solution(6462007780187894201)
XLA Ops:
  0.6 1.3 collective-permute-start
  1.9 0.2 collective-permute-start.1
  2.2 1.2 collective-permute-start.2
  3.4 0.8 copy.18.shift_ref
  4.2 0.0 copy-start
  4.3 1.0 copy-done
  5.3 0.0 copy-start.1
  5.3 0.7 copy-done.1
  6.0 0.0 copy-start.2
  6.0 0.7 copy-done.2
  6.7 0.0 copy-start.4
  6.7 0.7 copy-done.4
  7.4 50.1 %mixer_local.1 = (bf16[512,512]{1,0:T(8,128)(2,1)S(1)}, f32[512,512]{1,0:T(8,128)S(1)}, bf16[2,256,128]{2,1,0:T(8,128)(2,1)S(1)}, bf16[512,2048]{1,0:T(8,128)(2,...) custom-call(bf16[512,512]{1,0:T(8,128)(2,1)} %r_ref.1, ...), custom_call_target="tpu_custom_call" | custom-call | flops 20000000000 | bytes 6291456 | tf_op jit(solution)/shard_map/mixer_local/pallas_call | solution.py:388
  57.5 0.0 collective-permute-done.far_gate
  57.5 0.0 collective-permute-done.1.far_up
  57.5 0.0 copy-start.3
  57.5 0.0 copy-start.5
  57.5 0.0 copy-start.6
  57.5 13.9 %expert_part.1 = (f32[512,2048]{1,0:T(8,128)S(1)}, bf16[512,512]{1,0:T(8,128)(2,1)S(1)}, f32[512,128]{1,0:T(8,128)S(1)}) custom-call(bf16[2048,256]{1,0:T(8,128)(2,1)} %bitcast.16, bf16[2048,256]{1,0:T(8,128)(2,1)} %bitcast.19, bf16[256,2048]{1,0:T(8,128)(2,1)} %bitcast.22, bf16[2,256,128]{2,1,0:T(8,128)(2,1)S(1)} %get-tuple-element.14.summary_ref, ...), custom_call_target="tpu_custom_call" | custom-call | flops 5368709120 | bytes 12582912 | tf_op jit(solution)/shard_map/expert_part/pallas_call | solution.py:650
  71.4 0.0 collective-permute-done.2.far_ref
  71.5 0.0 copy-done.3
  71.5 0.0 copy-done.5
  71.5 0.0 copy-done.6
  71.5 58.3 %return_rows.1 = (bf16[128,2048]{1,0:T(8,128)(2,1)S(1)}, bf16[128,2048]{1,0:T(8,128)(2,1)S(1)}) custom-call(bf16[512,2048]{1,0:T(8,128)(2,1)} %project_ref.1, bf16[512,512]{1,0:T(8,128)(2,1)S(1)} %get-tuple-element.12.reader, f32[512,512]{1,0:T(8,128)S(1)} %get-tuple-element.13.local, f32[1,512]{1,0:T(1,128)S(1)} %bitcast.10, ...), custom_call_target="tpu_custom_call" | custom-call | flops 6000000000 | bytes 12582912 | tf_op jit(solution)/shard_map/return_rows/pallas_call | solution.py:892
  129.8 0.8 copy.21
  130.6 0.8 copy.22
Async XLA Ops:
  0.6 56.8 %collective-permute-start = (bf16[2048,256]{1,0:T(8,128)(2,1)}, bf16[2048,256]{1,0:T(8,128)(2,1)S(1)}, u32[]{:S(2)}, u32[]{:S(2)}) collective-permute-start(bf16[2048,256]{1,0:T(8,128)(2,1)} %bitcast.14), channel_id=1, source_target_pairs={{0,2},{1,3},{2,0},{3,1},{4,6},{5,7},{6,4},{7,5},{8,10},{9,11},{10,... | collective-permute-start | bytes 3145736 | tf_op jit(solution)/shard_map/ppermute | solution.py:927
  1.9 55.5 %collective-permute-start.1 = (bf16[2048,256]{1,0:T(8,128)(2,1)}, bf16[2048,256]{1,0:T(8,128)(2,1)S(1)}, u32[]{:S(2)}, u32[]{:S(2)}) collective-permute-start(bf16[2048,256]{1,0:T(8,128)(2,1)} %bitcast.17), channel_id=1, source_target_pairs={{0,2},{1,3},{2,0},{3,1},{4,6},{5,7},{6,4},{7,5},{8,10},{9,11},{10,... | collective-permute-start | bytes 3145736 | tf_op jit(solution)/shard_map/ppermute | solution.py:927
  2.2 69.3 %collective-permute-start.2 = (bf16[256,2048]{1,0:T(8,128)(2,1)}, bf16[256,2048]{1,0:T(8,128)(2,1)S(1)}, u32[]{:S(2)}, u32[]{:S(2)}) collective-permute-start(bf16[256,2048]{1,0:T(8,128)(2,1)} %bitcast.20), channel_id=1, source_target_pairs={{0,2},{1,3},{2,0},{3,1},{4,6},{5,7},{6,4},{7,5},{8,10},{9,11},{10,... | collective-permute-start | bytes 3145736 | tf_op jit(solution)/shard_map/ppermute | solution.py:927
  4.2 1.0 copy-start
  5.3 0.7 copy-start.1
  6.0 0.7 copy-start.2
  6.7 0.7 copy-start.4
  57.5 14.0 %copy-start.3 = (f32[512]{0:T(512)S(1)}, f32[512]{0:T(512)}, u32[]{:S(2)}) copy-start(f32[512]{0:T(512)} %param.23) | copy-start | bytes 6148
  57.5 14.0 %copy-start.5 = (s32[128,2]{0,1:T(2,128)S(1)}, s32[128,2]{0,1:T(2,128)}, u32[]{:S(2)}) copy-start(s32[128,2]{0,1:T(2,128)} %param.27) | copy-start | bytes 3076
  57.5 14.0 %copy-start.6 = (f32[128,2]{0,1:T(2,128)S(1)}, f32[128,2]{0,1:T(2,128)}, u32[]{:S(2)}) copy-start(f32[128,2]{0,1:T(2,128)} %param.28) | copy-start | bytes 3076

commit v5 on v0

v5 whole, which is shorter than its diff:
```python
import functools

import jax
import jax.numpy as jnp
from jax import lax
from jax.experimental import pallas as pl
from jax.experimental.pallas import tpu as pltpu
from jax.sharding import PartitionSpec as P

SPAN = 128
STACK = 2
LANES = 128

NORM_EPS = 1e-06
GROUP_EPS = 0.00064
KEY_EPS = 1e-06
F32 = jnp.float32
BF16 = jnp.bfloat16


def mm(a, b):
    return lax.dot_general(
        a.astype(BF16), b.astype(BF16), (((1,), (0,)), ((), ())), preferred_element_type=F32
    )


def mm_nt(a, b):
    return lax.dot_general(
        a.astype(BF16), b.astype(BF16), (((1,), (1,)), ((), ())), preferred_element_type=F32
    )


def mm_tn(a, b):
    return lax.dot_general(
        a.astype(BF16), b.astype(BF16), (((0,), (0,)), ((), ())), preferred_element_type=F32
    )


def split_two(x):
    high = x.astype(BF16)
    return high, (x - high.astype(F32)).astype(BF16)


def grid_index(shape, axis):
    return lax.broadcasted_iota(jnp.int32, shape, axis)


def same_head(head_size):
    rows = grid_index((LANES, LANES), 0) // head_size
    cols = grid_index((LANES, LANES), 1) // head_size
    return rows == cols


def head_sums(x, block):
    high, low = split_two(x)
    return mm(
        jnp.concatenate([high, low], axis=1), jnp.concatenate([block, block], axis=0)
    )


def lower_inverses(strict_parts, rows, cols):
    eye = jnp.where(rows == cols, 1.0, 0.0)
    size = 1
    inverses = None
    while size < SPAN:
        off = (rows // (2 * size) == cols // (2 * size)) & (rows // size != cols // size)
        parts = [jnp.where(off, part, 0.0) for part in strict_parts]
        if inverses is None:
            inverses = [eye - part for part in parts]
        else:
            firsts = [mm(part, inv) for part, inv in zip(parts, inverses)]
            inverses = [inv - mm(inv, first) for inv, first in zip(inverses, firsts)]
        size *= 2
    return inverses


def send_to(src, dst, send_sem, recv_sem, target):
    return pltpu.make_async_remote_copy(
        src_ref=src,
        dst_ref=dst,
        send_sem=send_sem,
        recv_sem=recv_sem,
        device_id=target,
        device_id_type=pl.DeviceIdType.MESH,
    )


def greet_all(barrier, here, count, others):
    def greet(distance, nothing):
        pl.semaphore_signal(
            barrier,
            inc=1,
            device_id={"ep": lax.rem(here + distance, count)},
            device_id_type=pl.DeviceIdType.MESH,
        )
        return nothing

    lax.fori_loop(1, count, greet, 0)
    for target in others:
        pl.semaphore_signal(
            barrier, inc=1, device_id={"tp": target}, device_id_type=pl.DeviceIdType.MESH
        )


def in_hbm(array):
    return pltpu.with_memory_space_constraint(array, pltpu.HBM)


def pack_rows(tokens_ref, scale_ref, routes_ref, outgoing, count, capacity):
    inputs = tokens_ref[...].astype(F32)
    square = jnp.sum(inputs * inputs, axis=1, keepdims=True) * (1.0 / inputs.shape[1])
    normed = (inputs * lax.rsqrt(square + NORM_EPS) * scale_ref[...]).astype(BF16)
    rows = inputs.shape[0]
    members = grid_index((count, rows), 0)
    named = jnp.zeros((count, rows), F32)
    for picked in range(routes_ref.shape[0]):
        named = jnp.where(routes_ref[picked : picked + 1] == members, 1.0, named)
    earlier = grid_index((rows, rows), 0) < grid_index((rows, rows), 1)
    slots = mm(named, earlier.astype(F32))
    slots = jnp.where(named > 0.5, slots, -1.0).astype(jnp.int32)
    wanted = grid_index((capacity, rows), 0)
    group = max(1, min(count, 256 // capacity))
    for begin in range(0, count, group):
        table = jnp.concatenate(
            [
                jnp.where(slots[e : e + 1] == wanted, 1.0, 0.0)
                for e in range(begin, begin + group)
            ],
            axis=0,
        )
        outgoing[begin * capacity : (begin + group) * capacity] = mm(table, normed).astype(BF16)


def scan_pair(
    pair,
    head_size,
    r_ref,
    k_ref,
    v_ref,
    d_ref,
    l_ref,
    base_ref,
    shift_ref,
    reader_ref,
    local_ref,
    summary_ref,
    state,
):
    half = LANES // 2
    lanes = pl.ds(pl.multiple_of(pair * LANES, LANES), LANES)
    spot = pl.ds(pl.multiple_of(pair * half, half), half)

    rows = grid_index((SPAN, SPAN), 0)
    cols = grid_index((SPAN, SPAN), 1)
    strict = rows > cols
    inclusive = rows >= cols
    first = grid_index((SPAN, LANES), 1) < half
    matched = same_head(head_size)
    block = matched.astype(BF16)
    diagonal = grid_index((LANES, LANES), 0) == grid_index((LANES, LANES), 1)
    tri = inclusive.astype(BF16)
    tri_two = jnp.concatenate([tri, tri], axis=1)

    state[:LANES] = jnp.zeros((LANES, LANES), F32)
    state[LANES:] = jnp.where(diagonal, 1.0, 0.0)

    heads = shift_ref.shape[1]
    chosen = grid_index((heads, LANES), 0) == 2 * pair + grid_index((heads, LANES), 1) // half
    def advance(step, nothing):
        start = pl.multiple_of(step * (STACK * SPAN), STACK * SPAN)
        rows_here = pl.ds(start, STACK * SPAN)
        shift = lax.dot_general(
            shift_ref[rows_here],
            chosen.astype(F32),
            (((1,), (0,)), ((), ())),
            precision=lax.Precision.HIGHEST,
            preferred_element_type=F32,
        )
        pre = d_ref[rows_here, lanes].astype(F32) + base_ref[:, lanes] + shift
        log_all = -0.6065306597126334 / (1.0 + jnp.exp(-pre))
        rates = 1.0 / (1.0 + jnp.exp(-l_ref[rows_here, lanes].astype(F32)))
        key_all = k_ref[rows_here, lanes].astype(F32)
        unit_all = key_all * lax.rsqrt(head_sums(key_all * key_all, block) + KEY_EPS)
        removal_all = unit_all * rates

        spans = STACK
        items = []
        strict_parts = []
        for j in range(spans):
            here = slice(j * SPAN, (j + 1) * SPAN)
            log_decay = log_all[here]
            high, low = split_two(log_decay)
            cum = mm(tri_two, jnp.concatenate([high, low], axis=0))
            middle = cum[SPAN // 2 - 1 : SPAN // 2]
            ending = cum[SPAN - 1 :]
            e_cm = jnp.exp(cum - middle)
            e_pm = jnp.exp(cum - log_decay - middle)
            shrink = jnp.exp(middle - cum)
            e_mid = jnp.exp(middle)
            e_tail = jnp.exp(ending - middle)
            unit, key = unit_all[here], key_all[here]
            value = v_ref[pl.ds(start + j * SPAN, SPAN), lanes]
            turned = jnp.concatenate([value[:, half:], value[:, :half]], axis=1)
            recept = r_ref[pl.ds(start + j * SPAN, SPAN), lanes].astype(F32)
            probes = unit * e_pm
            queries = recept * e_cm
            back_removal = removal_all[here] * shrink
            back_keys = key * shrink
            left = jnp.concatenate(
                [
                    jnp.where(first, probes, 0.0),
                    jnp.where(first, 0.0, probes),
                    jnp.where(first, queries, 0.0),
                    jnp.where(first, 0.0, queries),
                ],
                axis=0,
            )
            products = mm_nt(left, jnp.concatenate([back_removal, back_keys], axis=0))
            for h in range(2):
                strict_parts.append(
                    jnp.where(strict, products[h * SPAN : (h + 1) * SPAN, :SPAN], 0.0)
                )
            items.append(
                dict(
                    products=products,
                    turned=turned,
                    carrying=probes * e_mid,
                    reading=queries * e_mid,
                    removal_tail=back_removal * e_tail,
                    key_tail=back_keys * e_tail,
                    fade=jnp.exp(ending),
                )
            )
        inverses = lower_inverses(strict_parts, rows, cols)
        for j in range(spans):
            item = items[j]
            products, turned = item["products"], item["turned"]
            solved, removed, kept = [], [], []
            for h in range(2):
                top = slice(h * SPAN, (h + 1) * SPAN)
                bottom = slice((2 + h) * SPAN, (3 + h) * SPAN)
                pair_keys = jnp.where(strict, products[top, SPAN:], 0.0)
                read_removal = jnp.where(inclusive, products[bottom, :SPAN], 0.0)
                read_keys = jnp.where(inclusive, products[bottom, SPAN:], 0.0)
                both = mm(jnp.concatenate([pair_keys, read_keys], axis=0), turned)
                own = first if h == 0 else jnp.logical_not(first)
                right = jnp.where(own, item["carrying"], both[:SPAN])
                answer = mm(inverses[2 * j + h], right)
                solved.append(answer)
                removed.append(mm(read_removal, answer))
                kept.append(both[SPAN:])
            carried = jnp.where(first, solved[0], solved[1])
            local_turned = jnp.where(first, solved[1], solved[0])
            reader = item["reading"] - jnp.where(first, removed[0], removed[1])
            read_turned = jnp.where(first, kept[1] - removed[1], kept[0] - removed[0])
            local_read = jnp.concatenate([read_turned[:, half:], read_turned[:, :half]], axis=1)
            taken = mm_tn(
                jnp.concatenate([carried, local_turned], axis=1), item["removal_tail"]
            )
            offset_turned = mm_tn(turned, item["key_tail"]) - taken[LANES:]
            offset = jnp.concatenate([offset_turned[half:], offset_turned[:half]], axis=0)
            offset = jnp.where(matched, offset, 0.0)
            transition = jnp.where(diagonal, item["fade"], 0.0) - jnp.where(
                matched, taken[:LANES], 0.0
            )
            now = state[...]
            reads = mm_nt(reader, now)
            here = pl.ds(start + j * SPAN, SPAN)
            local_ref[here, lanes] = local_read + reads[:, :LANES]
            reader_ref[pl.ds(start + j * SPAN, SPAN), lanes] = reads[:, LANES:].astype(BF16)
            now_high, now_low = split_two(now)
            step_high, step_low = split_two(transition)
            moved = mm(now_high, step_high) + mm(now_low, step_high) + mm(now_high, step_low)
            state[:LANES] = moved[:LANES] + offset
            state[LANES:] = moved[LANES:]
        return nothing

    lax.fori_loop(0, r_ref.shape[0] // (STACK * SPAN), advance, 0)
    summary_ref[1, spot] = (state[:half] + state[half:LANES]).astype(BF16)
    summary_ref[0, spot] = (state[LANES : LANES + half] + state[LANES + half :]).astype(BF16)


def gated(x, gate, up):
    gates = mm(x, gate)
    uppers = mm(x, up)
    return (gates / (1.0 + jnp.exp(-gates)) * uppers).astype(BF16)


def layer_kernel(capacity, head_size, *refs):
    (
        r_hbm,
        k_hbm,
        v_hbm,
        d_hbm,
        l_hbm,
        base_hbm,
        shift_hbm,
        gain_hbm,
        project_hbm,
        tokens_hbm,
        scale_hbm,
        routes_hbm,
        weight_hbm,
        gate_hbm,
        up_hbm,
        down_hbm,
        mixer_ref,
        expert_ref,
        r_ref,
        k_ref,
        v_ref,
        d_ref,
        l_ref,
        base_ref,
        shift_in,
        gain_ref,
        project,
        tokens_ref,
        scale_ref,
        routes_ref,
        weight_ref,
        own_gate,
        own_up,
        own_down,
        near_gate,
        near_up,
        near_down,
        far_gate,
        far_up,
        far_down,
        cross_gate,
        cross_up,
        cross_down,
        shift_ref,
        reader,
        local,
        summary,
        state,
        outgoing,
        x_ref,
        total,
        hidden_ref,
        before,
        sending,
        passed,
        mixed,
        staged,
        landed,
        term,
        near_in,
        pair_out,
        far_in,
        combined,
        load_sems,
        post_send,
        post_recv,
        back_send,
        back_recv,
        round_send,
        round_recv,
        side_send,
        side_recv,
    ) = refs
    here = lax.axis_index("ep")
    count = lax.axis_size("ep")
    place = lax.axis_index("tp")
    low, high = lax.rem(place, 2), place // 2
    beside = place + 1 - 2 * low
    across = place + 2 - 4 * high
    reach_half = count // 2
    local_index, own_half = lax.rem(here, reach_half), here // reach_half
    rounds = passed.shape[0]
    half = LANES // 2
    pairs = before.shape[1]
    rows = x_ref.shape[0]
    units = own_gate.shape[1]
    tokens = expert_ref.shape[0]
    matched = same_head(head_size)
    block = matched.astype(BF16)
    diagonal = grid_index((LANES, LANES), 0) == grid_index((LANES, LANES), 1)

    pieces = [
        (tokens_hbm, tokens_ref),
        (scale_hbm, scale_ref),
        (routes_hbm, routes_ref),
        (weight_hbm, weight_ref),
        (base_hbm, base_ref),
        (shift_hbm, shift_in),
        (gain_hbm, gain_ref),
        (r_hbm, r_ref),
        (k_hbm, k_ref),
        (v_hbm, v_ref),
        (d_hbm, d_ref),
        (l_hbm, l_ref),
        (gate_hbm, own_gate),
        (up_hbm, own_up),
        (down_hbm, own_down),
        (project_hbm, project),
    ]
    loads = [
        pltpu.make_async_copy(src, dst, load_sems.at[i]) for i, (src, dst) in enumerate(pieces)
    ]
    keep_sem = load_sems.at[len(pieces)]
    barrier = pltpu.get_barrier_semaphore()
    greet_all(barrier, here, count, (beside, across))
    for load in loads:
        load.start()

    def side(src, dst, index, target):
        return send_to(src, dst, side_send.at[index], side_recv.at[index], {"tp": target})

    def rows_of(member):
        return pl.ds(pl.multiple_of(member * capacity, capacity), capacity)

    def partner(k, sign):
        crossing, shift = (k + 1) // reach_half, lax.rem(k + 1, reach_half)
        member = lax.rem(local_index + reach_half + sign * shift, reach_half)
        return member + reach_half * (own_half + crossing * (1 - 2 * own_half))

    def post(k, member):
        return send_to(
            outgoing.at[rows_of(member)],
            x_ref.at[rows_of(here)],
            post_send.at[k],
            post_recv.at[k],
            {"ep": member},
        )

    def back(k, member):
        return send_to(
            staged.at[rows_of(member)],
            landed.at[rows_of(here)],
            back_send.at[k],
            back_recv.at[k],
            {"ep": member},
        )

    cut = units // 2
    fars = [side(gate_hbm, far_gate, 0, across), side(up_hbm, far_up, 1, across)] + [
        side(down_hbm.at[i * cut : (i + 1) * cut], far_down.at[i * cut : (i + 1) * cut], 2 + i, across)
        for i in range(2)
    ]
    nears = [
        side(gate_hbm, near_gate, 4, beside),
        side(up_hbm, near_up, 5, beside),
        side(down_hbm, near_down, 6, beside),
    ]
    forwards = [side(far_gate, cross_gate, 7, beside), side(far_up, cross_up, 8, beside)] + [
        side(
            far_down.at[i * cut : (i + 1) * cut], cross_down.at[i * cut : (i + 1) * cut], 9 + i, beside
        )
        for i in range(2)
    ]

    pl.semaphore_wait(barrier, count + 1)
    for copy in fars + nears:
        copy.start()
    for load in loads[:3]:
        load.wait()
    pack_rows(tokens_ref, scale_ref, routes_ref, outgoing, count, capacity)

    def launch_post(k, nothing):
        post(k, partner(k, 1)).start()
        return nothing

    lax.fori_loop(0, count - 1, launch_post, 0)
    keep = pltpu.make_async_copy(outgoing.at[rows_of(here)], x_ref.at[rows_of(here)], keep_sem)
    keep.start()

    for load in loads[3:12]:
        load.wait()
    shift_ref[...] = shift_in[...].T

    def scan(p, nothing):
        scan_pair(
            p,
            head_size,
            r_ref,
            k_ref,
            v_ref,
            d_ref,
            l_ref,
            base_ref,
            shift_ref,
            reader,
            local,
            summary,
            state,
        )
        return nothing

    lax.fori_loop(0, pairs, scan, 0)

    def transfer(level, distance, target):
        return send_to(
            sending,
            passed.at[level],
            round_send.at[distance - 1],
            round_recv.at[level],
            {"ep": target},
        )

    def transfer_state(level, distance, target):
        return send_to(
            sending.at[1],
            passed.at[level, 1],
            round_send.at[distance - 1],
            round_recv.at[level],
            {"ep": target},
        )

    def sends_all(reach):
        return (lax.rem(here, 2 * reach) == reach - 1) & (here >= 2 * reach)

    def wide(part):
        part = part.astype(F32)
        return jnp.where(matched, jnp.concatenate([part, part], axis=0), 0.0)

    def spot(p):
        return slice(p * half, (p + 1) * half)

    for p in range(pairs):
        before[0, p] = jnp.where(diagonal, 1.0, 0.0)
        before[1, p] = jnp.zeros((LANES, LANES), F32)

    def send_round(level):
        reach = 2**level

        @pl.when(lax.rem(here, 2 * reach) == reach - 1)
        def _():
            for p in range(pairs):
                both = jnp.concatenate([before[0, p], before[1, p]], axis=0)
                upper, lower = split_two(both)
                step = wide(summary[0, spot(p)])
                moved = mm(upper, step) + mm(lower, step)
                after = moved[LANES:] + wide(summary[1, spot(p)])
                sending[0, spot(p)] = (moved[:half] + moved[half:LANES]).astype(BF16)
                sending[1, spot(p)] = (after[:half] + after[half:]).astype(BF16)

        def launch_with(transfer):
            def launch(distance, nothing):
                transfer(level, distance, here + distance).start()
                return nothing

            lax.fori_loop(1, reach + 1, launch, 0)

        pl.when(sends_all(reach))(lambda: launch_with(transfer))
        pl.when(here == reach - 1)(lambda: launch_with(transfer_state))

    def take_round(level):
        reach = 2**level

        @pl.when((lax.rem(here // reach, 2) == 1) & (here >= 2 * reach))
        def _():
            transfer(level, 1, here).wait_recv()
            for p in range(pairs):
                both = jnp.concatenate(
                    [wide(passed[level, 0, spot(p)]), wide(passed[level, 1, spot(p)])], axis=0
                )
                upper, lower = split_two(before[0, p])
                moved = mm(both, upper) + mm(both, lower)
                before[0, p] = moved[:LANES]
                before[1, p] = moved[LANES:] + before[1, p]

        @pl.when((here >= reach) & (here < 2 * reach))
        def _():
            transfer_state(level, 1, here).wait_recv()
            for p in range(pairs):
                entering = wide(passed[level, 1, spot(p)])
                upper, lower = split_two(before[0, p])
                before[1, p] = mm(entering, upper) + mm(entering, lower) + before[1, p]

    def settle_with(transfer, level, reach):
        def settle(distance, nothing):
            transfer(level, distance, here + distance).wait_send()
            return nothing

        lax.fori_loop(1, reach + 1, settle, 0)

    def at_half(which):
        return pl.ds(pl.multiple_of(which * (rows // 2), rows // 2), rows // 2)

    def full_parts(at):
        x = x_ref[at]
        total[at] = mm(gated(x, own_gate[...], own_up[...]), own_down[...])
        total[at] += mm(gated(x, near_gate[...], near_up[...]), near_down[...])

    def far_parts(at):
        x = x_ref[at]
        hidden_ref[at, :units] = gated(x, far_gate[...], far_up[...])
        hidden_ref[at, units:] = gated(x, cross_gate[...], cross_up[...])

    def take_post(k, nothing):
        post(k, partner(k, -1)).wait_recv()
        return nothing

    send_round(0)
    for load in loads[12:15]:
        load.wait()
    keep.wait()
    for copy in nears:
        copy.wait_recv()
    lax.fori_loop(0, reach_half - 1, take_post, 0)
    full_parts(at_half(own_half))
    fars[0].wait_recv()
    forwards[0].start()
    take_round(0)
    if rounds > 1:
        send_round(1)
    fars[1].wait_recv()
    forwards[1].start()
    lax.fori_loop(reach_half - 1, count - 1, take_post, 0)
    full_parts(at_half(1 - own_half))
    for level in range(1, min(rounds, 2)):
        take_round(level)
        if level + 1 < rounds:
            send_round(level + 1)
    for copy in forwards[:2]:
        copy.wait_recv()

    def far_step(i, nothing):
        far_parts(at_half(i))
        return nothing

    lax.fori_loop(0, 2, far_step, 0)
    for level in range(2, rounds):
        take_round(level)
        if level + 1 < rounds:
            send_round(level + 1)

    for i in range(2):
        fars[2 + i].wait_recv()
        forwards[2 + i].start()
    for copy in forwards[2:]:
        copy.wait_recv()

    def finished(member):
        at = rows_of(member)
        hidden = hidden_ref[at]
        row = total[at] + mm(hidden[:, :units], far_down[...])
        return (row + mm(hidden[:, units:], cross_down[...])).astype(BF16)

    def send_back(k, nothing):
        k = lax.rem(k + reach_half - 1, count - 1)
        member = partner(k, 1)
        staged[rows_of(member)] = finished(member)
        back(k, member).start()
        return nothing

    lax.fori_loop(0, count - 1, send_back, 0)
    landed[rows_of(here)] = finished(here)

    loads[15].wait()
    for p in range(pairs):
        lanes = slice(p * LANES, (p + 1) * LANES)
        read = mm_nt(reader[:, lanes], before[1, p]) + local[:, lanes]
        centred = read - head_sums(read, block) * (1.0 / head_size)
        variance = head_sums(centred * centred, block) * (1.0 / head_size)
        scaled = centred * lax.rsqrt(variance + GROUP_EPS) * gain_ref[:, lanes]
        mixed[:, lanes] = scaled.astype(BF16)

    def block_rows(b):
        return pl.ds(pl.multiple_of(b * tokens, tokens), tokens)

    def project_block(b, nothing):
        at = block_rows(b)
        term[at] = mm(mixed[at], project[...]).astype(BF16)
        return nothing

    lax.fori_loop(0, 4, project_block, 0)
    sums = [
        side(term.at[block_rows(2 * y + 1 - low)], near_in.at[y], 11 + y, beside)
        for y in range(2)
    ]
    for copy in sums:
        copy.start()

    picks = routes_ref.shape[0]
    packed = jnp.concatenate(
        [routes_ref[...].astype(F32), weight_ref[...], jnp.zeros((8 - 2 * picks, tokens), F32)],
        axis=0,
    ).T
    lane = grid_index((tokens, LANES), 1)
    routes = [packed[:, i : i + 1].astype(jnp.int32) for i in range(picks)]
    weight = packed[:, picks : 2 * picks]
    named = jnp.zeros((tokens, LANES), F32)
    for route in routes:
        named = jnp.where(route == lane, 1.0, named)
    earlier = grid_index((tokens, tokens), 0) > grid_index((tokens, tokens), 1)
    slots = mm(earlier.astype(F32), named)
    target = jnp.concatenate(
        [
            route * capacity
            + jnp.sum(jnp.where(route == lane, slots, 0.0), axis=1, keepdims=True).astype(
                jnp.int32
            )
            for route in routes
        ],
        axis=1,
    )
    slot = grid_index((tokens, capacity), 1)

    def taken(member):
        table = jnp.zeros((tokens, capacity), F32)
        scale = jnp.zeros((tokens, 1), F32)
        for picked in range(target.shape[1]):
            own = target[:, picked : picked + 1] - member * capacity
            table = jnp.where(own == slot, 1.0, table)
            inside = (own >= 0) & (own < capacity)
            scale = jnp.where(inside, weight[:, picked : picked + 1], scale)
        return mm(table, landed[rows_of(member)]) * scale

    combined[...] = taken(here)

    for copy in sums:
        copy.wait_recv()
    other = 1 - high
    pair_out[...] = (
        term[block_rows(2 * other + low)].astype(F32) + near_in[other].astype(F32)
    ).astype(BF16)
    last_sum = side(pair_out, far_in, 13, across)
    last_sum.start()

    def gather_block(k, nothing):
        member = partner(k, -1)
        back(k, member).wait_recv()
        combined[...] += taken(member)
        return nothing

    lax.fori_loop(0, reach_half - 1, gather_block, 0)
    last_sum.wait_recv()
    kept = term[block_rows(2 * high + low)].astype(F32) + near_in[high].astype(F32)
    mixer_ref[...] = (kept + far_in[...].astype(F32)).astype(BF16)
    lax.fori_loop(reach_half - 1, count - 1, gather_block, 0)
    expert_ref[...] = combined[...].astype(BF16)

    def settle_rows(k, nothing):
        post(k, partner(k, 1)).wait_send()
        back(k, partner(k, 1)).wait_send()
        return nothing

    lax.fori_loop(0, count - 1, settle_rows, 0)
    for level in range(rounds):
        reach = 2**level
        pl.when(sends_all(reach))(functools.partial(settle_with, transfer, level, reach))
        pl.when(here == reach - 1)(
            functools.partial(settle_with, transfer_state, level, reach)
        )
    for copy in fars + nears + forwards + sums + [last_sum]:
        copy.wait_send()


def whole_layer(streams, base, shift, gain, out_weight, tokens, scale, routes, weights, own, head_size, capacity):
    rows, channels = streams[0].shape
    pairs = channels // LANES
    half = LANES // 2
    count = lax.axis_size("ep")
    rounds = (count - 1).bit_length()
    token_rows, width = tokens.shape
    slots = count * capacity
    units = own[0].shape[1]
    inputs = list(streams) + [
        base.reshape(1, channels),
        shift.T,
        gain.reshape(1, channels),
        out_weight,
        tokens,
        scale.reshape(1, width),
        routes.T,
        weights.T,
    ]
    operands = [in_hbm(array) for array in inputs + list(own)]
    block = (token_rows, width)
    wide, tall = (width, units), (units, width)
    held = [pltpu.VMEM(array.shape, array.dtype) for array in inputs]
    shards = [pltpu.VMEM(shape, BF16) for shape in (wide, wide, tall) * 4]
    dma = pltpu.SemaphoreType.DMA
    return pl.pallas_call(
        functools.partial(layer_kernel, capacity, head_size),
        in_specs=[pl.BlockSpec(memory_space=pl.ANY)] * len(operands),
        out_specs=[pl.BlockSpec(memory_space=pltpu.VMEM)] * 2,
        out_shape=[jax.ShapeDtypeStruct(block, BF16)] * 2,
        scratch_shapes=held
        + shards
        + [
            pltpu.VMEM(shift.shape, F32),
            pltpu.VMEM((rows, channels), BF16),
            pltpu.VMEM((rows, channels), F32),
            pltpu.VMEM((2, pairs * half, LANES), BF16),
            pltpu.VMEM((2 * LANES, LANES), F32),
            pltpu.VMEM((slots, width), BF16),
            pltpu.VMEM((slots, width), BF16),
            pltpu.VMEM((slots, width), F32),
            pltpu.VMEM((slots, 2 * units), BF16),
            pltpu.VMEM((2, pairs, LANES, LANES), F32),
            pltpu.VMEM((2, pairs * half, LANES), BF16),
            pltpu.VMEM((rounds, 2, pairs * half, LANES), BF16),
            pltpu.VMEM((rows, channels), BF16),
            pltpu.VMEM((slots, width), BF16),
            pltpu.VMEM((slots, width), BF16),
            pltpu.VMEM((rows, width), BF16),
            pltpu.VMEM((2,) + block, BF16),
            pltpu.VMEM(block, BF16),
            pltpu.VMEM(block, BF16),
            pltpu.VMEM(block, F32),
            dma((len(operands) + 1,)),
            dma((count - 1,)),
            dma((count - 1,)),
            dma((count - 1,)),
            dma((count - 1,)),
            dma((count // 2,)),
            dma((rounds,)),
            dma((14,)),
            dma((14,)),
        ],
        compiler_params=pltpu.CompilerParams(
            vmem_limit_bytes=48 * 2**20, collective_id=0, has_side_effects=True
        ),
        cost_estimate=pl.CostEstimate(
            flops=40 * 10**9, bytes_accessed=20 * 2**20, transcendentals=2 * 10**6
        ),
        name="whole_layer",
    )(*operands)


def on_device(
    receptance,
    key_rows,
    value_rows,
    decay_input,
    learn_input,
    decay_base,
    decay_shift,
    channel_gain,
    out_weight,
    expert_input,
    expert_gain,
    routes,
    route_weight,
    gate_weight,
    up_weight,
    down_weight,
):
    head_size = receptance.shape[1] // decay_shift.shape[1]
    experts = gate_weight.shape[0] * lax.axis_size("ep")
    capacity = max(2, 2 * expert_input.shape[0] * routes.shape[1] // experts)
    return tuple(
        whole_layer(
            (receptance, key_rows, value_rows, decay_input, learn_input),
            decay_base,
            decay_shift,
            channel_gain,
            out_weight,
            expert_input,
            expert_gain,
            routes,
            route_weight,
            (gate_weight[0], up_weight[0], down_weight[0]),
            head_size,
            capacity,
        )
    )


def solution(mesh):
    return jax.shard_map(
        on_device,
        mesh=mesh,
        in_specs=(
            P("ep", "tp"),
            P("ep", "tp"),
            P("ep", "tp"),
            P("ep", "tp"),
            P("ep", "tp"),
            P("tp"),
            P("ep", "tp"),
            P("tp"),
            P("tp", None),
            P(("ep", "tp"), None),
            P(),
            P(("ep", "tp"), None),
            P(("ep", "tp"), None),
            P("ep", None, "tp"),
            P("ep", None, "tp"),
            P("ep", "tp", None),
        ),
        out_specs=(P(("ep", "tp"), None), P(("ep", "tp"), None)),
        check_vma=False,
    )
```

time: 192 us -> 127 us (0.66)
  waiting for transfers between devices: 79.5 us -> 0 us
  Pallas kernels: 58.3 us -> 125 us
  matrix products: 15.8 us -> 0 us
  between operations: 14 us -> 0.65 us
  starting transfers between devices: 13.1 us -> 0 us
  local copies, waits for them, and re-layouts: 9.78 us -> 1.59 us
    pallas_call x3 -> x1, Pallas kernels: 58.3 us -> 125 us  [whole_layer(): pl.pallas_call(functools.partial(layer_kernel, capacity, head_size), in_s...]
    all_to_all x2 -> x0, waiting for transfers between devices: 45.5 us -> none  [the longest x1 45.5 us: on_device(): lax.all_to_all(total.astype(BF16).reshape(ep_count, capacity, model_width...]
    all_gather x3 -> x0, waiting for transfers between devices: 32 us -> none  [the longest x1 24 us: on_device(): all_down = lax.all_gather(down_weight[0], 'tp')]
    dot_general x5 -> x0, matrix products: 15.8 us -> none  [the longest x1 6.19 us: on_device(): jnp.dot(hidden, all_down.reshape(hidden.shape[1], model_width), preferred...]
    all_to_all x2 -> x0, starting transfers between devices: 12.9 us -> none  [the longest x1 7.43 us: on_device(): lax.all_to_all(outgoing.reshape(experts, capacity, model_width), 'ep', sp...]
    unnamed x34 -> x2, local copies, waits for them, and re-layouts: 9.44 us -> 1.59 us
    unnamed x4 -> x0, waiting for transfers between devices: 2.07 us -> none
  transfers between devices with their start and end apart: 6 -> 0, of which waited for: 3 -> 0; matrix products, arithmetic and copies ran while one was open for 6% -> 0% of each run, Pallas kernels for 31% -> 0%
where the time goes in v5:
time: 127 us
  Pallas kernels  125 us (98%)
  local copies, waits for them, and re-layouts  1.59 us (1%)
    pallas_call x1, Pallas kernels, whole_layer(): pl.pallas_call(functools.partial(layer_kernel, capacity, head_size), in_s...  125 us

profile of v5, /device:TPU:0, one launch (start us, length us, event | category | flops | bytes accessed | tf_op | source)
XLA Modules:
  0.0 127.1 jit_solution(3612944184691168934)
XLA Ops:
  0.6 124.9 %whole_layer.1 = (bf16[128,2048]{1,0:T(8,128)(2,1)S(1)}, bf16[128,2048]{1,0:T(8,128)(2,1)S(1)}) custom-call(bf16[512,512]{1,0:T(8,128)(2,1)} %refs_0_.1, bf16[512,512]{1,0:T(8,128)(2,1)} %refs_1_.1, bf16[512,512]{1,0:T(8,128)(2,1)} %refs_2_.1, bf16[512,512]{1,0:T(8,128)(2,1)} %refs_3_.1, bf16[512,512]{1,0:T(8,128)(2,1)} %refs_4_.1, f32[1,512]{1,0:T(1,128)} %bitcast.14, ...), custom_call_target="tpu_custom_call" | custom-call | flops 40000000000 | bytes 20971520 | tf_op jit(solution)/shard_map/whole_layer/pallas_call | solution.py:778
  125.5 0.8 copy.20
  126.3 0.8 copy.21

commit v6 on v5

--- a/solution.py
+++ b/solution.py
@@ -10,6 +10,7 @@
 SPAN = 128
 STACK = 2
 LANES = 128
+EARLY = 3
 
 NORM_EPS = 1e-06
 GROUP_EPS = 0.00064
@@ -286,7 +287,7 @@
     return (gates / (1.0 + jnp.exp(-gates)) * uppers).astype(BF16)
 
 
-def layer_kernel(capacity, head_size, *refs):
+def layer_kernel(capacity, head_size, early, *refs):
     (
         r_hbm,
         k_hbm,
@@ -344,8 +345,13 @@
         sending,
         passed,
         mixed,
-        staged,
-        landed,
+        theirs,
+        part_out,
+        part_in,
+        staged_early,
+        staged_late,
+        landed_early,
+        landed_late,
         term,
         near_in,
         pair_out,
@@ -356,6 +362,8 @@
         post_recv,
         back_send,
         back_recv,
+        part_send,
+        part_recv,
         round_send,
         round_recv,
         side_send,
@@ -426,18 +434,42 @@
             {"ep": member},
         )
 
-    def back(k, member):
+    def back(k, member, late):
+        staged, landed = (staged_late, landed_late) if late else (staged_early, landed_early)
         return send_to(
             staged.at[rows_of(member)],
             landed.at[rows_of(here)],
-            back_send.at[k],
-            back_recv.at[k],
+            back_send.at[late, k],
+            back_recv.at[late, k],
             {"ep": member},
         )
+
+    def part(member):
+        return send_to(
+            part_out.at[rows_of(member)],
+            part_in.at[rows_of(member)],
+            part_send.at[member],
+            part_recv.at[member],
+            {"tp": across},
+        )
+
+    def at_half(which):
+        return pl.ds(pl.multiple_of(which * (rows // 2), rows // 2), rows // 2)
+
+    halves = (1 - own_half, own_half)
+    asks = [
+        side(hidden_ref.at[at_half(which)], theirs.at[at_half(which)], 14 + i, across)
+        for i, which in enumerate(halves)
+    ]
 
     cut = units // 2
     fars = [side(gate_hbm, far_gate, 0, across), side(up_hbm, far_up, 1, across)] + [
-        side(down_hbm.at[i * cut : (i + 1) * cut], far_down.at[i * cut : (i + 1) * cut], 2 + i, across)
+        side(
+            down_hbm.at[i * cut : (i + 1) * cut, :early],
+            far_down.at[i * cut : (i + 1) * cut],
+            2 + i,
+            across,
+        )
         for i in range(2)
     ]
     nears = [
@@ -576,9 +608,6 @@
             return nothing
 
         lax.fori_loop(1, reach + 1, settle, 0)
-
-    def at_half(which):
-        return pl.ds(pl.multiple_of(which * (rows // 2), rows // 2), rows // 2)
 
     def full_parts(at):
         x = x_ref[at]
@@ -611,19 +640,13 @@
     forwards[1].start()
     lax.fori_loop(reach_half - 1, count - 1, take_post, 0)
     full_parts(at_half(1 - own_half))
-    for level in range(1, min(rounds, 2)):
-        take_round(level)
-        if level + 1 < rounds:
-            send_round(level + 1)
     for copy in forwards[:2]:
         copy.wait_recv()
 
-    def far_step(i, nothing):
-        far_parts(at_half(i))
-        return nothing
-
-    lax.fori_loop(0, 2, far_step, 0)
-    for level in range(2, rounds):
+    for i in range(2):
+        far_parts(at_half(halves[i]))
+        asks[i].start()
+    for level in range(1, min(rounds, 2)):
         take_round(level)
         if level + 1 < rounds:
             send_round(level + 1)
@@ -637,19 +660,39 @@
     def finished(member):
         at = rows_of(member)
         hidden = hidden_ref[at]
-        row = total[at] + mm(hidden[:, :units], far_down[...])
+        row = total[at, :early] + mm(hidden[:, :units], far_down[...])
         return (row + mm(hidden[:, units:], cross_down[...])).astype(BF16)
 
     def send_back(k, nothing):
         k = lax.rem(k + reach_half - 1, count - 1)
         member = partner(k, 1)
-        staged[rows_of(member)] = finished(member)
-        back(k, member).start()
+        staged_early[rows_of(member)] = finished(member)
+        back(k, member, 0).start()
         return nothing
 
     lax.fori_loop(0, count - 1, send_back, 0)
-    landed[rows_of(here)] = finished(here)
-
+    landed_early[rows_of(here)] = finished(here)
+
+    def answer(i):
+        asks[i].wait_recv()
+        at = at_half(halves[i])
+        asked = theirs[at]
+        product = mm(asked[:, :units], own_down[:, early:])
+        product += mm(asked[:, units:], near_down[:, early:])
+        part_out[at] = product.astype(BF16)
+
+        def launch(j, nothing):
+            part(halves[i] * reach_half + lax.rem(local_index + j, reach_half)).start()
+            return nothing
+
+        lax.fori_loop(0, reach_half, launch, 0)
+
+    answer(0)
+    answer(1)
+    for level in range(2, rounds):
+        take_round(level)
+        if level + 1 < rounds:
+            send_round(level + 1)
     loads[15].wait()
     for p in range(pairs):
         lanes = slice(p * LANES, (p + 1) * LANES)
@@ -700,7 +743,7 @@
     )
     slot = grid_index((tokens, capacity), 1)
 
-    def taken(member):
+    def taken(member, late):
         table = jnp.zeros((tokens, capacity), F32)
         scale = jnp.zeros((tokens, 1), F32)
         for picked in range(target.shape[1]):
@@ -708,9 +751,10 @@
             table = jnp.where(own == slot, 1.0, table)
             inside = (own >= 0) & (own < capacity)
             scale = jnp.where(inside, weight[:, picked : picked + 1], scale)
+        landed = landed_late if late else landed_early
         return mm(table, landed[rows_of(member)]) * scale
 
-    combined[...] = taken(here)
+    combined[:, :early] = taken(here, 0)
 
     for copy in sums:
         copy.wait_recv()
@@ -721,32 +765,61 @@
     last_sum = side(pair_out, far_in, 13, across)
     last_sum.start()
 
-    def gather_block(k, nothing):
+    def late_rows(member):
+        part(member).wait_recv()
+        at = rows_of(member)
+        return (total[at, early:] + part_in[at].astype(F32)).astype(BF16)
+
+    def send_late(k, nothing):
+        k = lax.rem(k + reach_half - 1, count - 1)
+        member = partner(k, 1)
+        staged_late[rows_of(member)] = late_rows(member)
+        back(k, member, 1).start()
+        return nothing
+
+    def gather_early(k, nothing):
         member = partner(k, -1)
-        back(k, member).wait_recv()
-        combined[...] += taken(member)
-        return nothing
-
-    lax.fori_loop(0, reach_half - 1, gather_block, 0)
+        back(k, member, 0).wait_recv()
+        combined[:, :early] += taken(member, 0)
+        return nothing
+
+    def gather_late(k, nothing):
+        member = partner(k, -1)
+        back(k, member, 1).wait_recv()
+        combined[:, early:] += taken(member, 1)
+        return nothing
+
+    lax.fori_loop(0, reach_half, send_late, 0)
+    landed_late[rows_of(here)] = late_rows(here)
+    combined[:, early:] = taken(here, 1)
+    lax.fori_loop(reach_half, count - 1, send_late, 0)
+    lax.fori_loop(0, count - 1, gather_early, 0)
+    lax.fori_loop(0, reach_half - 1, gather_late, 0)
     last_sum.wait_recv()
     kept = term[block_rows(2 * high + low)].astype(F32) + near_in[high].astype(F32)
     mixer_ref[...] = (kept + far_in[...].astype(F32)).astype(BF16)
-    lax.fori_loop(reach_half - 1, count - 1, gather_block, 0)
+    lax.fori_loop(reach_half - 1, count - 1, gather_late, 0)
     expert_ref[...] = combined[...].astype(BF16)
 
     def settle_rows(k, nothing):
         post(k, partner(k, 1)).wait_send()
-        back(k, partner(k, 1)).wait_send()
+        back(k, partner(k, 1), 0).wait_send()
+        back(k, partner(k, 1), 1).wait_send()
+        return nothing
+
+    def settle_part(member, nothing):
+        part(member).wait_send()
         return nothing
 
     lax.fori_loop(0, count - 1, settle_rows, 0)
+    lax.fori_loop(0, count, settle_part, 0)
     for level in range(rounds):
         reach = 2**level
         pl.when(sends_all(reach))(functools.partial(settle_with, transfer, level, reach))
         pl.when(here == reach - 1)(
             functools.partial(settle_with, transfer_state, level, reach)
         )
-    for copy in fars + nears + forwards + sums + [last_sum]:
+    for copy in fars + nears + forwards + asks + sums + [last_sum]:
         copy.wait_send()
 
 
@@ -759,6 +832,8 @@
     token_rows, width = tokens.shape
     slots = count * capacity
     units = own[0].shape[1]
+    early = width * EARLY // (8 * LANES) * LANES
+    late = width - early
     inputs = list(streams) + [
         base.reshape(1, channels),
         shift.T,
@@ -773,10 +848,12 @@
     block = (token_rows, width)
     wide, tall = (width, units), (units, width)
     held = [pltpu.VMEM(array.shape, array.dtype) for array in inputs]
-    shards = [pltpu.VMEM(shape, BF16) for shape in (wide, wide, tall) * 4]
+    slim = (units, early)
+    shapes = (wide, wide, tall) * 2 + (wide, wide, slim) * 2
+    shards = [pltpu.VMEM(shape, BF16) for shape in shapes]
     dma = pltpu.SemaphoreType.DMA
     return pl.pallas_call(
-        functools.partial(layer_kernel, capacity, head_size),
+        functools.partial(layer_kernel, capacity, head_size, early),
         in_specs=[pl.BlockSpec(memory_space=pl.ANY)] * len(operands),
         out_specs=[pl.BlockSpec(memory_space=pltpu.VMEM)] * 2,
         out_shape=[jax.ShapeDtypeStruct(block, BF16)] * 2,
@@ -796,8 +873,13 @@
             pltpu.VMEM((2, pairs * half, LANES), BF16),
             pltpu.VMEM((rounds, 2, pairs * half, LANES), BF16),
             pltpu.VMEM((rows, channels), BF16),
-            pltpu.VMEM((slots, width), BF16),
-            pltpu.VMEM((slots, width), BF16),
+            pltpu.VMEM((slots, 2 * units), BF16),
+            pltpu.VMEM((slots, late), BF16),
+            pltpu.VMEM((slots, late), BF16),
+            pltpu.VMEM((slots, early), BF16),
+            pltpu.VMEM((slots, late), BF16),
+            pltpu.VMEM((slots, early), BF16),
+            pltpu.VMEM((slots, late), BF16),
             pltpu.VMEM((rows, width), BF16),
             pltpu.VMEM((2,) + block, BF16),
             pltpu.VMEM(block, BF16),
@@ -806,15 +888,17 @@
             dma((len(operands) + 1,)),
             dma((count - 1,)),
             dma((count - 1,)),
-            dma((count - 1,)),
-            dma((count - 1,)),
+            dma((2, count - 1)),
+            dma((2, count - 1)),
+            dma((count,)),
+            dma((count,)),
             dma((count // 2,)),
             dma((rounds,)),
-            dma((14,)),
-            dma((14,)),
+            dma((16,)),
+            dma((16,)),
         ],
         compiler_params=pltpu.CompilerParams(
-            vmem_limit_bytes=48 * 2**20, collective_id=0, has_side_effects=True
+            vmem_limit_bytes=52 * 2**20, collective_id=0, has_side_effects=True
         ),
         cost_estimate=pl.CostEstimate(
             flops=40 * 10**9, bytes_accessed=20 * 2**20, transcendentals=2 * 10**6

time: 127 us -> 117 us (0.921)
  Pallas kernels: 125 us -> 115 us
    pallas_call x1, Pallas kernels: 125 us -> 115 us  [whole_layer(): pl.pallas_call(functools.partial(layer_kernel, capacity, head_size, early...]
where the time goes in v6:
time: 117 us
  Pallas kernels  115 us (98%)
  local copies, waits for them, and re-layouts  1.59 us (1%)
    pallas_call x1, Pallas kernels, whole_layer(): pl.pallas_call(functools.partial(layer_kernel, capacity, head_size, early...  115 us

profile of v6, /device:TPU:0, one launch (start us, length us, event | category | flops | bytes accessed | tf_op | source)
XLA Modules:
  0.0 117.1 jit_solution(6855655884086049419)
XLA Ops:
  0.6 114.8 %whole_layer.1 = (bf16[128,2048]{1,0:T(8,128)(2,1)S(1)}, bf16[128,2048]{1,0:T(8,128)(2,1)S(1)}) custom-call(bf16[512,512]{1,0:T(8,128)(2,1)} %refs_0_.1, bf16[512,512]{1,0:T(8,128)(2,1)} %refs_1_.1, bf16[512,512]{1,0:T(8,128)(2,1)} %refs_2_.1, bf16[512,512]{1,0:T(8,128)(2,1)} %refs_3_.1, bf16[512,512]{1,0:T(8,128)(2,1)} %refs_4_.1, f32[1,512]{1,0:T(1,128)} %bitcast.14, ...), custom_call_target="tpu_custom_call" | custom-call | flops 40000000000 | bytes 20971520 | tf_op jit(solution)/shard_map/whole_layer/pallas_call | solution.py:855
  115.5 0.8 copy.20
  116.3 0.8 copy.21

commit v7 on v6

--- a/solution.py
+++ b/solution.py
@@ -10,7 +10,7 @@
 SPAN = 128
 STACK = 2
 LANES = 128
-EARLY = 3
+EARLY = 6
 
 NORM_EPS = 1e-06
 GROUP_EPS = 0.00064
@@ -345,6 +345,10 @@
         sending,
         passed,
         mixed,
+        far_rest_a,
+        far_rest_b,
+        cross_rest_a,
+        cross_rest_b,
         theirs,
         part_out,
         part_in,
@@ -425,6 +429,13 @@
         member = lax.rem(local_index + reach_half + sign * shift, reach_half)
         return member + reach_half * (own_half + crossing * (1 - 2 * own_half))
 
+    def crossing_step(j):
+        quarter = reach_half // 2
+        side_of = (1 - own_half) + (j // quarter) * (2 * own_half - 1)
+        index = side_of * quarter + lax.rem(local_index + j, quarter)
+        shift = lax.rem(index - local_index + reach_half, reach_half)
+        return reach_half - 1 + shift, (1 - own_half) * reach_half + index
+
     def post(k, member):
         return send_to(
             outgoing.at[rows_of(member)],
@@ -444,6 +455,21 @@
             {"ep": member},
         )
 
+    far_rest = (far_rest_a, far_rest_b)
+    cross_rest = (cross_rest_a, cross_rest_b)
+    middle = far_rest_a.shape[1]
+    spans = ((0, middle), (middle, middle + far_rest_b.shape[1]))
+
+    def back_piece(k, member, i):
+        columns = slice(*spans[i])
+        return send_to(
+            staged_late.at[rows_of(member), columns],
+            landed_late.at[rows_of(here), columns],
+            back_send.at[1 + i, k],
+            back_recv.at[1 + i, k],
+            {"ep": member},
+        )
+
     def part(member):
         return send_to(
             part_out.at[rows_of(member)],
@@ -456,11 +482,8 @@
     def at_half(which):
         return pl.ds(pl.multiple_of(which * (rows // 2), rows // 2), rows // 2)
 
-    halves = (1 - own_half, own_half)
-    asks = [
-        side(hidden_ref.at[at_half(which)], theirs.at[at_half(which)], 14 + i, across)
-        for i, which in enumerate(halves)
-    ]
+    crossing_rows = at_half(1 - own_half)
+    ask = side(hidden_ref.at[crossing_rows], theirs.at[crossing_rows], 14, across)
 
     cut = units // 2
     fars = [side(gate_hbm, far_gate, 0, across), side(up_hbm, far_up, 1, across)] + [
@@ -484,6 +507,12 @@
         for i in range(2)
     ]
 
+    rests = [
+        side(down_hbm.at[:, early + first : early + last], far_rest[i], 15 + i, across)
+        for i, (first, last) in enumerate(spans)
+    ]
+    onward = [side(far_rest[i], cross_rest[i], 17 + i, beside) for i in range(2)]
+
     pl.semaphore_wait(barrier, count + 1)
     for copy in fars + nears:
         copy.start()
@@ -495,7 +524,12 @@
         post(k, partner(k, 1)).start()
         return nothing
 
-    lax.fori_loop(0, count - 1, launch_post, 0)
+    def launch_crossing(j, nothing):
+        post(*crossing_step(j)).start()
+        return nothing
+
+    lax.fori_loop(0, reach_half - 1, launch_post, 0)
+    lax.fori_loop(0, reach_half, launch_crossing, 0)
     keep = pltpu.make_async_copy(outgoing.at[rows_of(here)], x_ref.at[rows_of(here)], keep_sem)
     keep.start()
 
@@ -643,9 +677,9 @@
     for copy in forwards[:2]:
         copy.wait_recv()
 
-    for i in range(2):
-        far_parts(at_half(halves[i]))
-        asks[i].start()
+    far_parts(crossing_rows)
+    ask.start()
+    far_parts(at_half(own_half))
     for level in range(1, min(rounds, 2)):
         take_round(level)
         if level + 1 < rounds:
@@ -663,32 +697,45 @@
         row = total[at, :early] + mm(hidden[:, :units], far_down[...])
         return (row + mm(hidden[:, units:], cross_down[...])).astype(BF16)
 
-    def send_back(k, nothing):
-        k = lax.rem(k + reach_half - 1, count - 1)
-        member = partner(k, 1)
+    def send_early(k, member):
         staged_early[rows_of(member)] = finished(member)
         back(k, member, 0).start()
-        return nothing
-
-    lax.fori_loop(0, count - 1, send_back, 0)
+
+    def send_back(j, nothing):
+        send_early(*crossing_step(j))
+        return nothing
+
+    def send_back_near(k, nothing):
+        send_early(k, partner(k, 1))
+        return nothing
+
+    lax.fori_loop(0, reach_half, send_back, 0)
+    lax.fori_loop(0, reach_half - 1, send_back_near, 0)
     landed_early[rows_of(here)] = finished(here)
 
-    def answer(i):
-        asks[i].wait_recv()
-        at = at_half(halves[i])
-        asked = theirs[at]
-        product = mm(asked[:, :units], own_down[:, early:])
-        product += mm(asked[:, units:], near_down[:, early:])
-        part_out[at] = product.astype(BF16)
-
-        def launch(j, nothing):
-            part(halves[i] * reach_half + lax.rem(local_index + j, reach_half)).start()
-            return nothing
-
-        lax.fori_loop(0, reach_half, launch, 0)
-
-    answer(0)
-    answer(1)
+    ask.wait_recv()
+    asked = theirs[crossing_rows]
+    product = mm(asked[:, :units], own_down[:, early:])
+    product += mm(asked[:, units:], near_down[:, early:])
+    part_out[crossing_rows] = product.astype(BF16)
+
+    def launch_part(j, nothing):
+        part(crossing_step(j)[1]).start()
+        return nothing
+
+    lax.fori_loop(0, reach_half, launch_part, 0)
+    for copy in rests:
+        copy.start()
+    def send_crossing(j, nothing):
+        k, member = crossing_step(j)
+        part(member).wait_recv()
+        at = rows_of(member)
+        staged_late[at] = (total[at, early:] + part_in[at].astype(F32)).astype(BF16)
+        back(k, member, 1).start()
+        return nothing
+
+    lax.fori_loop(0, reach_half, send_crossing, 0)
+
     for level in range(2, rounds):
         take_round(level)
         if level + 1 < rounds:
@@ -765,17 +812,28 @@
     last_sum = side(pair_out, far_in, 13, across)
     last_sum.start()
 
-    def late_rows(member):
-        part(member).wait_recv()
+    def late_rows(member, i):
         at = rows_of(member)
-        return (total[at, early:] + part_in[at].astype(F32)).astype(BF16)
-
-    def send_late(k, nothing):
-        k = lax.rem(k + reach_half - 1, count - 1)
-        member = partner(k, 1)
-        staged_late[rows_of(member)] = late_rows(member)
-        back(k, member, 1).start()
-        return nothing
+        hidden = hidden_ref[at]
+        first, last = spans[i]
+        row = total[at, early + first : early + last]
+        row += mm(hidden[:, :units], far_rest[i][...])
+        return (row + mm(hidden[:, units:], cross_rest[i][...])).astype(BF16)
+
+    def send_near(i):
+        columns = slice(*spans[i])
+        rests[i].wait_recv()
+        onward[i].start()
+        onward[i].wait_recv()
+
+        def send_piece(k, nothing):
+            member = partner(k, 1)
+            staged_late[rows_of(member), columns] = late_rows(member, i)
+            back_piece(k, member, i).start()
+            return nothing
+
+        lax.fori_loop(0, reach_half - 1, send_piece, 0)
+        landed_late[rows_of(here), columns] = late_rows(here, i)
 
     def gather_early(k, nothing):
         member = partner(k, -1)
@@ -783,43 +841,60 @@
         combined[:, :early] += taken(member, 0)
         return nothing
 
+    def gather_near(k, nothing):
+        member = partner(k, -1)
+        for i in range(2):
+            back_piece(k, member, i).wait_recv()
+        combined[:, early:] += taken(member, 1)
+        return nothing
+
     def gather_late(k, nothing):
         member = partner(k, -1)
         back(k, member, 1).wait_recv()
         combined[:, early:] += taken(member, 1)
         return nothing
 
-    lax.fori_loop(0, reach_half, send_late, 0)
-    landed_late[rows_of(here)] = late_rows(here)
+    lax.fori_loop(0, reach_half - 1, gather_early, 0)
+    for i in range(2):
+        send_near(i)
     combined[:, early:] = taken(here, 1)
-    lax.fori_loop(reach_half, count - 1, send_late, 0)
-    lax.fori_loop(0, count - 1, gather_early, 0)
-    lax.fori_loop(0, reach_half - 1, gather_late, 0)
+    lax.fori_loop(reach_half - 1, count - 1, gather_early, 0)
+    lax.fori_loop(0, reach_half - 1, gather_near, 0)
+    lax.fori_loop(reach_half - 1, count - 1, gather_late, 0)
+    expert_ref[...] = combined[...].astype(BF16)
     last_sum.wait_recv()
     kept = term[block_rows(2 * high + low)].astype(F32) + near_in[high].astype(F32)
     mixer_ref[...] = (kept + far_in[...].astype(F32)).astype(BF16)
-    lax.fori_loop(reach_half - 1, count - 1, gather_late, 0)
-    expert_ref[...] = combined[...].astype(BF16)
 
     def settle_rows(k, nothing):
         post(k, partner(k, 1)).wait_send()
         back(k, partner(k, 1), 0).wait_send()
+        return nothing
+
+    def settle_near(k, nothing):
+        for i in range(2):
+            back_piece(k, partner(k, 1), i).wait_send()
+        return nothing
+
+    def settle_crossing(k, nothing):
         back(k, partner(k, 1), 1).wait_send()
         return nothing
 
-    def settle_part(member, nothing):
-        part(member).wait_send()
+    def settle_part(j, nothing):
+        part(crossing_step(j)[1]).wait_send()
         return nothing
 
     lax.fori_loop(0, count - 1, settle_rows, 0)
-    lax.fori_loop(0, count, settle_part, 0)
+    lax.fori_loop(0, reach_half - 1, settle_near, 0)
+    lax.fori_loop(reach_half - 1, count - 1, settle_crossing, 0)
+    lax.fori_loop(0, reach_half, settle_part, 0)
     for level in range(rounds):
         reach = 2**level
         pl.when(sends_all(reach))(functools.partial(settle_with, transfer, level, reach))
         pl.when(here == reach - 1)(
             functools.partial(settle_with, transfer_state, level, reach)
         )
-    for copy in fars + nears + forwards + asks + sums + [last_sum]:
+    for copy in fars + nears + forwards + [ask] + rests + onward + sums + [last_sum]:
         copy.wait_send()
 
 
@@ -832,8 +907,9 @@
     token_rows, width = tokens.shape
     slots = count * capacity
     units = own[0].shape[1]
-    early = width * EARLY // (8 * LANES) * LANES
+    early = width * EARLY // (16 * LANES) * LANES
     late = width - early
+    late_end = late // (2 * LANES) * LANES
     inputs = list(streams) + [
         base.reshape(1, channels),
         shift.T,
@@ -873,6 +949,10 @@
             pltpu.VMEM((2, pairs * half, LANES), BF16),
             pltpu.VMEM((rounds, 2, pairs * half, LANES), BF16),
             pltpu.VMEM((rows, channels), BF16),
+            pltpu.VMEM((units, late - late_end), BF16),
+            pltpu.VMEM((units, late_end), BF16),
+            pltpu.VMEM((units, late - late_end), BF16),
+            pltpu.VMEM((units, late_end), BF16),
             pltpu.VMEM((slots, 2 * units), BF16),
             pltpu.VMEM((slots, late), BF16),
             pltpu.VMEM((slots, late), BF16),
@@ -888,14 +968,14 @@
             dma((len(operands) + 1,)),
             dma((count - 1,)),
             dma((count - 1,)),
-            dma((2, count - 1)),
-            dma((2, count - 1)),
+            dma((3, count - 1)),
+            dma((3, count - 1)),
             dma((count,)),
             dma((count,)),
             dma((count // 2,)),
             dma((rounds,)),
-            dma((16,)),
-            dma((16,)),
+            dma((19,)),
+            dma((19,)),
         ],
         compiler_params=pltpu.CompilerParams(
             vmem_limit_bytes=52 * 2**20, collective_id=0, has_side_effects=True
@@ -905,6 +985,32 @@
         ),
         name="whole_layer",
     )(*operands)
+
+
+def output_kernel(mixer_ref, expert_ref, mixer_out, expert_out, sems):
+    copies = [
+        pltpu.make_async_copy(mixer_ref, mixer_out, sems.at[0]),
+        pltpu.make_async_copy(expert_ref, expert_out, sems.at[1]),
+    ]
+    for copy in copies:
+        copy.start()
+    for copy in copies:
+        copy.wait()
+
+
+def write_outputs(mixer, expert):
+    return pl.pallas_call(
+        output_kernel,
+        in_specs=[pl.BlockSpec(memory_space=pltpu.VMEM)] * 2,
+        out_specs=[pl.BlockSpec(memory_space=pl.ANY)] * 2,
+        out_shape=[
+            jax.ShapeDtypeStruct(mixer.shape, BF16),
+            jax.ShapeDtypeStruct(expert.shape, BF16),
+        ],
+        scratch_shapes=[pltpu.SemaphoreType.DMA((2,))],
+        compiler_params=pltpu.CompilerParams(vmem_limit_bytes=4 * 2**20),
+        name="write_outputs",
+    )(mixer, expert)
 
 
 def on_device(
@@ -929,19 +1035,21 @@
     experts = gate_weight.shape[0] * lax.axis_size("ep")
     capacity = max(2, 2 * expert_input.shape[0] * routes.shape[1] // experts)
     return tuple(
-        whole_layer(
-            (receptance, key_rows, value_rows, decay_input, learn_input),
-            decay_base,
-            decay_shift,
-            channel_gain,
-            out_weight,
-            expert_input,
-            expert_gain,
-            routes,
-            route_weight,
-            (gate_weight[0], up_weight[0], down_weight[0]),
-            head_size,
-            capacity,
+        write_outputs(
+            *whole_layer(
+                (receptance, key_rows, value_rows, decay_input, learn_input),
+                decay_base,
+                decay_shift,
+                channel_gain,
+                out_weight,
+                expert_input,
+                expert_gain,
+                routes,
+                route_weight,
+                (gate_weight[0], up_weight[0], down_weight[0]),
+                head_size,
+                capacity,
+            )
         )
     )
 

time: 117 us -> 115 us (0.983); the launches traced: 117 us -> 112 us
  Pallas kernels: 115 us -> 112 us
  local copies, waits for them, and re-layouts: 1.59 us -> 0 us
    pallas_call x1, Pallas kernels: 115 us -> 111 us  [whole_layer(): pl.pallas_call(functools.partial(layer_kernel, capacity, head_size, early...]
    unnamed x2 -> x0, local copies, waits for them, and re-layouts: 1.59 us -> none
where the time goes in v7:
time: 115 us; the launch traced here: 112 us
  Pallas kernels  112 us (97%)
    pallas_call x1, Pallas kernels, whole_layer(): pl.pallas_call(functools.partial(layer_kernel, capacity, head_size, early...  111 us

profile of v7, /device:TPU:0, one launch (start us, length us, event | category | flops | bytes accessed | tf_op | source)
XLA Modules:
  0.0 112.4 jit_solution(9125139944890934579)
XLA Ops:
  0.6 110.6 %whole_layer.1 = (bf16[128,2048]{1,0:T(8,128)(2,1)S(1)}, bf16[128,2048]{1,0:T(8,128)(2,1)S(1)}) custom-call(bf16[512,512]{1,0:T(8,128)(2,1)} %refs_0_.1, bf16[512,512]{1,0:T(8,128)(2,1)} %refs_1_.1, bf16[512,512]{1,0:T(8,128)(2,1)} %refs_2_.1, bf16[512,512]{1,0:T(8,128)(2,1)} %refs_3_.1, bf16[512,512]{1,0:T(8,128)(2,1)} %refs_4_.1, f32[1,512]{1,0:T(1,128)} %bitcast.14, ...), custom_call_target="tpu_custom_call" | custom-call | flops 40000000000 | bytes 20971520 | tf_op jit(solution)/shard_map/whole_layer/pallas_call | solution.py:931
  111.3 1.0 write_outputs.1

commit v8 on v7

--- a/solution.py
+++ b/solution.py
@@ -673,17 +673,17 @@
     fars[1].wait_recv()
     forwards[1].start()
     lax.fori_loop(reach_half - 1, count - 1, take_post, 0)
-    full_parts(at_half(1 - own_half))
-    for copy in forwards[:2]:
-        copy.wait_recv()
-
-    far_parts(crossing_rows)
-    ask.start()
-    far_parts(at_half(own_half))
     for level in range(1, min(rounds, 2)):
         take_round(level)
         if level + 1 < rounds:
             send_round(level + 1)
+    full_parts(at_half(1 - own_half))
+    for copy in forwards[:2]:
+        copy.wait_recv()
+
+    far_parts(crossing_rows)
+    ask.start()
+    far_parts(at_half(own_half))
 
     for i in range(2):
         fars[2 + i].wait_recv()

time: 115 us -> 113 us (0.983); the launches traced: 112 us -> 112 us
  no operation moved by 1% of the time
where the time goes in v8:
time: 113 us; the launch traced here: 112 us
  Pallas kernels  112 us (99%)
    pallas_call x1, Pallas kernels, whole_layer(): pl.pallas_call(functools.partial(layer_kernel, capacity, head_size, early...  111 us

profile of v8, /device:TPU:0, one launch (start us, length us, event | category | flops | bytes accessed | tf_op | source)
XLA Modules:
  0.0 112.4 jit_solution(6521682270922405879)
XLA Ops:
  0.6 110.6 %whole_layer.1 = (bf16[128,2048]{1,0:T(8,128)(2,1)S(1)}, bf16[128,2048]{1,0:T(8,128)(2,1)S(1)}) custom-call(bf16[512,512]{1,0:T(8,128)(2,1)} %refs_0_.1, bf16[512,512]{1,0:T(8,128)(2,1)} %refs_1_.1, bf16[512,512]{1,0:T(8,128)(2,1)} %refs_2_.1, bf16[512,512]{1,0:T(8,128)(2,1)} %refs_3_.1, bf16[512,512]{1,0:T(8,128)(2,1)} %refs_4_.1, f32[1,512]{1,0:T(1,128)} %bitcast.14, ...), custom_call_target="tpu_custom_call" | custom-call | flops 40000000000 | bytes 20971520 | tf_op jit(solution)/shard_map/whole_layer/pallas_call | solution.py:931
  111.3 1.0 write_outputs.1

commit v9 on v8

--- a/solution.py
+++ b/solution.py
@@ -909,7 +909,7 @@
     units = own[0].shape[1]
     early = width * EARLY // (16 * LANES) * LANES
     late = width - early
-    late_end = late // (2 * LANES) * LANES
+    late_end = late // (3 * LANES) * LANES
     inputs = list(streams) + [
         base.reshape(1, channels),
         shift.T,

time: 113 us -> 115 us (1.018)
  Pallas kernels: 112 us -> 114 us
    pallas_call x1, Pallas kernels: 111 us -> 113 us  [whole_layer(): pl.pallas_call(functools.partial(layer_kernel, capacity, head_size, early...]
where the time goes in v9:
time: 115 us
  Pallas kernels  114 us (99%)
    pallas_call x1, Pallas kernels, whole_layer(): pl.pallas_call(functools.partial(layer_kernel, capacity, head_size, early...  113 us

profile of v9, /device:TPU:0, one launch (start us, length us, event | category | flops | bytes accessed | tf_op | source)
XLA Modules:
  0.0 114.7 jit_solution(16495023867447511397)
XLA Ops:
  0.6 112.9 %whole_layer.1 = (bf16[128,2048]{1,0:T(8,128)(2,1)S(1)}, bf16[128,2048]{1,0:T(8,128)(2,1)S(1)}) custom-call(bf16[512,512]{1,0:T(8,128)(2,1)} %refs_0_.1, bf16[512,512]{1,0:T(8,128)(2,1)} %refs_1_.1, bf16[512,512]{1,0:T(8,128)(2,1)} %refs_2_.1, bf16[512,512]{1,0:T(8,128)(2,1)} %refs_3_.1, bf16[512,512]{1,0:T(8,128)(2,1)} %refs_4_.1, f32[1,512]{1,0:T(1,128)} %bitcast.14, ...), custom_call_target="tpu_custom_call" | custom-call | flops 40000000000 | bytes 20971520 | tf_op jit(solution)/shard_map/whole_layer/pallas_call | solution.py:931
  113.5 1.0 write_outputs.1
